TPU v7x, 512 devices: a whole 4x8x8 slice. The times are simulated.
512 devices in a mesh: sp: 64 (over z, y), fs: 4 (over x), tp: 2 (over core).
Axes of the slice: x: 4, y: 8, z: 8, core: 2. Of those that a mesh axis runs over, the one named last changes fastest.
Arguments:
- tokens: bfloat16 [16384, 2048], P(('sp', 'fs', 'tp')), may hold values from -20 to 20
- norm_gain: float32 [2048], replicated, may hold values from 0.1 to 1.9
- query_weight: bfloat16 [2048, 1024], P(None, ('fs', 'tp')), may hold values from -0.5 to 0.5
- w_key: bfloat16 [2048, 256], P(None, 'tp'), may hold values from -0.5 to 0.5
- w_value: bfloat16 [2048, 256], P(None, 'tp'), may hold values from -0.125 to 0.125
- w_input: bfloat16 [2048, 1024], P(None, ('fs', 'tp')), may hold values from -0.125 to 0.125
- w_gate: bfloat16 [2048, 1024], P(None, ('fs', 'tp')), may hold values from -0.125 to 0.125
- conv_kernel: float32 [4, 1024], P(None, ('fs', 'tp')), may hold values from -3 to 3
- w_recur: bfloat16 [16, 64, 64], P(('fs', 'tp')), may hold values from -0.75 to 0.75
- w_admit: bfloat16 [16, 64, 64], P(('fs', 'tp')), may hold values from -0.75 to 0.75
- decay_param: float32 [1024], P(('fs', 'tp')), may hold values from 4 to 17
- decay_scale: float32 [16384, 1024], P('sp', ('fs', 'tp')), may hold values from 0.5 to 229376
- init_state: float32 [1024], P(('fs', 'tp')), may hold values from -6 to 6
- diff_lambda: float32 [8], P(('fs', 'tp')), may hold values from 0.3 to 0.8
- head_gain: float32 [128], replicated, may hold values from 0.1 to 1.9
- w_out_lru: bfloat16 [1024, 2048], P(('fs', 'tp')), may hold values from -1 to 1
- w_out_attn: bfloat16 [1024, 2048], P(('fs', 'tp')), may hold values from -0.1875 to 0.1875
Outputs:
- mixed: bfloat16 [16384, 2048], P(('sp', 'fs', 'tp'))
All inputs are finite; a program needn't handle non-finite values.
Results may differ from a plain program's by a relative error of at most 0.019.
Values may be sent and summed in bfloat16 or wider, within the bound.
No kernel may reach another device: no remote copies, remote signals or barrier semaphores. Data moves between devices by JAX's collectives and lax.ppermute only.
A program may use at most 64 MiB of HBM per device.

v0:
```python
import math

import jax
import jax.numpy as jnp
from jax import lax
from jax.sharding import Mesh
from jax.sharding import PartitionSpec as P

SP = ("sp_0", "sp_1")
SP_FS_TP = ("sp_0", "sp_1", "fs", "tp")


gate_scale = 8.0
input_eps = 1e-06
head_eps = 1e-05
far_below = -1e30


def joined_along(pieces, dim):
    dims = list(pieces.shape[1:])
    dims[dim] *= pieces.shape[0]
    return jnp.moveaxis(pieces, 0, dim).reshape(dims)


def from_everyone(value, axis):
    copies = jnp.broadcast_to(value, (lax.axis_size(axis), *value.shape))
    return lax.all_to_all(copies, axis, split_axis=0, concat_axis=0, tiled=True)


def gather_directly(value, axis, dim):
    return joined_along(from_everyone(value, axis), dim)


def passed_along(value, axis, by):
    devices = lax.axis_size(axis)
    pairs = [(i, i + by) for i in range(devices) if 0 <= i + by < devices]
    return lax.ppermute(value, axis, pairs)


def neutral_like(value, identity):
    return jax.tree.map(
        lambda part, zero: jnp.zeros_like(part) + jnp.asarray(zero, part.dtype), value, identity
    )


def prefix_by_axis(value, axes, combine, identity):
    before = start = neutral_like(value, identity)
    total = value
    for axis in reversed(axes):
        devices, here = (lax.axis_size(axis), lax.axis_index(axis))
        pieces = jax.tree.map(lambda part: lax.all_gather(part, axis), total)
        inside, total = (start, start)
        for k in range(devices):
            passed = k < here
            total = combine(total, jax.tree.map(lambda part: part[k], pieces))
            inside = jax.tree.map(lambda new, old: jnp.where(passed, new, old), total, inside)
        before = combine(inside, before)
    return before


def sent_together(arrays, axis, dim, along):
    ends, at = ([], 0)
    for a in arrays[:-1]:
        at += a.shape[along]
        ends.append(at)
    both = jnp.concatenate(arrays, axis=along)
    return tuple(jnp.split(lax.all_gather(both, axis, axis=dim, tiled=True), ends, axis=along))


def in_one_piece(arrays, axis, split_dim, concat_dim, along):
    columns = [a.reshape(*a.shape[:along], -1) for a in arrays]
    both = jnp.concatenate(columns, axis=along)
    whole, at, outs = (
        lax.all_to_all(both, axis, split_axis=split_dim, concat_axis=concat_dim, tiled=True),
        0,
        [],
    )
    for a, column in zip(arrays, columns):
        piece = whole[..., at : at + column.shape[along]]
        outs.append(piece.reshape(*piece.shape[:along], *a.shape[along:]))
        at += column.shape[along]
    return tuple(outs)


def cut_along(value, dim, devices):
    before, after = (value.shape[:dim], value.shape[dim + 1 :])
    return jnp.moveaxis(value.reshape(*before, devices, -1, *after), dim, 0)


def summed_on_arrival(value, axis, dim):
    pieces = cut_along(value, dim, lax.axis_size(axis))
    arrived = lax.all_to_all(pieces, axis, split_axis=0, concat_axis=0, tiled=True)
    return arrived.astype(jnp.float32).sum(axis=0)


def pair_combine(earlier, later):
    decay_early, state_early = earlier
    decay_late, state_late = later
    return (decay_early * decay_late, decay_late * state_early + state_late)


def fold_keys(carried, query_heads, query_pos, key_piece, value_piece, key_pos):
    total_keys = key_piece.shape[0]
    span = math.gcd(total_keys, 512)
    size_qk = query_heads.shape[-1]
    scale = size_qk ** (-0.5)

    def one_span(span_index, running):
        key_block = lax.dynamic_slice_in_dim(key_piece, span_index * span, span, 0)
        value_block = lax.dynamic_slice_in_dim(value_piece, span_index * span, span, 0)
        pos_block = lax.dynamic_slice_in_dim(key_pos, span_index * span, span, 0)

        def attend(state_now):
            peak_old, total_old, values_old = state_now
            key_maps = key_block.reshape(span, 2, size_qk)
            scores = (
                jnp.einsum(
                    "hqme,kme->hmqk", query_heads, key_maps, preferred_element_type=jnp.float32
                )
                * scale
            )
            visible = (pos_block[None, :] <= query_pos[:, None])[None, None]
            scores = jnp.where(visible, scores, far_below)
            peak_new = jnp.maximum(peak_old, jnp.max(scores, axis=-1))
            expos = jnp.where(visible, jnp.exp(scores - peak_new[..., None]), 0.0)
            fade = jnp.exp(peak_old - peak_new)
            total_new = total_old * fade + jnp.sum(expos, axis=-1)
            values_new = values_old * fade[..., None] + jnp.einsum(
                "hmqk,kv->hmqv",
                expos.astype(jnp.bfloat16),
                value_block,
                preferred_element_type=jnp.float32,
            )
            return (peak_new, total_new, values_new)

        def keep(state_now):
            return state_now

        return lax.cond(pos_block[0] <= query_pos[-1], attend, keep, running)

    return lax.fori_loop(0, total_keys // span, one_span, carried)


def empty_carry(head_count, row_count, value_size):
    return (
        jnp.full((head_count, 2, row_count), far_below, jnp.float32),
        jnp.zeros((head_count, 2, row_count), jnp.float32),
        jnp.zeros((head_count, 2, row_count, value_size), jnp.float32),
    )


def body(
    tokens,
    norm_gain,
    query_weight,
    w_key,
    w_value,
    w_input,
    w_gate,
    conv_kernel,
    w_recur,
    w_admit,
    decay_param,
    decay_scale,
    init_state,
    diff_lambda,
    head_gain,
    w_out_lru,
    w_out_attn,
):
    floats = tokens.astype(jnp.float32)
    normed = (
        floats * lax.rsqrt(jnp.mean(floats * floats, axis=1, keepdims=True) + input_eps) * norm_gain
    ).astype(jnp.bfloat16)
    weight_list = (query_weight, w_key, w_value, w_input, w_gate)

    def project_rows(piece):
        return jnp.concatenate(
            [
                jnp.dot(piece, weight, preferred_element_type=jnp.float32).astype(jnp.bfloat16)
                for weight in weight_list
            ],
            axis=1,
        )

    projected = project_rows(gather_directly(normed, ("fs", "tp"), 0))
    bounds = [0]
    for weight in weight_list:
        bounds.append(bounds[-1] + weight.shape[1])
    query = projected[:, bounds[0] : bounds[1]]
    keys_here = projected[:, bounds[1] : bounds[2]]
    values_here = projected[:, bounds[2] : bounds[3]]
    lru_in = projected[:, bounds[3] : bounds[4]]
    gate_proj = projected[:, bounds[4] : bounds[5]]
    row_count = projected.shape[0]
    channels = lru_in.shape[1]
    taps = conv_kernel.shape[0]
    earlier_rows = passed_along(lru_in[row_count - (taps - 1) :], SP, 1)
    padded = jnp.concatenate([earlier_rows, lru_in], axis=0).astype(jnp.float32)
    conv_sum = jnp.zeros((row_count, channels), jnp.float32)
    for offset in range(taps):
        conv_sum = conv_sum + conv_kernel[offset] * padded[offset : offset + row_count]
    conv_out = conv_sum.astype(jnp.bfloat16)
    grouped = conv_out.reshape(row_count, w_recur.shape[0], w_recur.shape[1])
    recur = jax.nn.sigmoid(
        jnp.einsum("tni,nij->tnj", grouped, w_recur, preferred_element_type=jnp.float32).reshape(
            row_count, channels
        )
    )
    admit = jax.nn.sigmoid(
        jnp.einsum("tni,nij->tnj", grouped, w_admit, preferred_element_type=jnp.float32).reshape(
            row_count, channels
        )
    )
    log_decay = -gate_scale * recur * jax.nn.softplus(-decay_param) * decay_scale
    decay = jnp.exp(log_decay)
    drive = jnp.sqrt(-jnp.expm1(2.0 * log_decay)) * admit * conv_out.astype(jnp.float32)
    decay_run, local_states = lax.associative_scan(pair_combine, (decay, drive), axis=0)
    identity = (jnp.ones((channels,), jnp.float32), jnp.zeros((channels,), jnp.float32))
    before_decay, before_state = prefix_by_axis(
        (decay_run[-1], local_states[-1]), SP, pair_combine, identity
    )
    entering = before_decay * init_state + before_state
    states = local_states + decay_run * entering[None, :]
    lru_out = (states * jax.nn.gelu(gate_proj.astype(jnp.float32))).astype(jnp.bfloat16)
    size_qk = query.shape[1] // 2
    value_size = values_here.shape[1]
    query_pos = lax.axis_index(SP) * row_count + jnp.arange(row_count)
    group_size = lax.axis_size("fs")
    member = lax.axis_index("fs")
    share_rows = row_count // group_size
    group_heads = gather_directly(query[None], "fs", 0)
    group_heads = group_heads.reshape(group_size, row_count, 2, size_qk)
    key_share = lax.dynamic_slice_in_dim(keys_here, member * share_rows, share_rows, 0)
    value_share = lax.dynamic_slice_in_dim(values_here, member * share_rows, share_rows, 0)
    key_piece, value_piece = sent_together((key_share, value_share), SP, 0, 1)
    collected_pointer = jnp.arange(key_piece.shape[0])
    key_pos = (
        collected_pointer // share_rows * row_count
        + member * share_rows
        + collected_pointer % share_rows
    )
    part_peak, part_total, part_values = fold_keys(
        empty_carry(group_size, row_count, value_size),
        group_heads,
        query_pos,
        key_piece,
        value_piece,
        key_pos,
    )
    part_peak, part_total, part_values = tuple(
        (
            part.astype(jnp.float32)
            for part in in_one_piece(
                (
                    part_peak.astype(jnp.bfloat16),
                    part_total.astype(jnp.bfloat16),
                    part_values.astype(jnp.bfloat16),
                ),
                "fs",
                0,
                0,
                3,
            )
        )
    )
    top_peak = jnp.max(part_peak, axis=0)
    fade = jnp.exp(part_peak - top_peak[None])
    total = jnp.sum(part_total * fade, axis=0)[None]
    heads_values = jnp.sum(part_values * fade[..., None], axis=0)[None]
    lam = diff_lambda[0]
    diff = (
        heads_values[0, 0] / total[0, 0][:, None] - lam * heads_values[0, 1] / total[0, 1][:, None]
    )
    scaled = diff * lax.rsqrt(jnp.mean(diff * diff, axis=-1, keepdims=True) + head_eps) * head_gain
    attn_out = scaled.astype(jnp.bfloat16)
    summed = summed_on_arrival(
        (
            jnp.dot(lru_out, w_out_lru, preferred_element_type=jnp.float32)
            + jnp.dot(attn_out, w_out_attn, preferred_element_type=jnp.float32)
        ).astype(jnp.bfloat16),
        ("fs", "tp"),
        0,
    )
    return summed.astype(jnp.bfloat16)


def solution(mesh):
    torus = Mesh(
        mesh.devices.reshape(8, 8, mesh.shape["fs"], mesh.shape["tp"]), ("sp_0", "sp_1", "fs", "tp")
    )
    return jax.shard_map(
        body,
        mesh=torus,
        in_specs=(
            P(SP_FS_TP, None),
            P(),
            P(None, ("fs", "tp")),
            P(None, "tp"),
            P(None, "tp"),
            P(None, ("fs", "tp")),
            P(None, ("fs", "tp")),
            P(None, ("fs", "tp")),
            P(("fs", "tp"), None, None),
            P(("fs", "tp"), None, None),
            P(("fs", "tp")),
            P(SP, ("fs", "tp")),
            P(("fs", "tp")),
            P(("fs", "tp")),
            P(),
            P(("fs", "tp"), None),
            P(("fs", "tp"), None),
        ),
        out_specs=P(SP_FS_TP, None),
        check_vma=False,
    )
```

profile of v0, /device:TPU:448, one launch (start us, length us, event | category | flops | bytes accessed | tf_op | source)
XLA Modules:
  0.0 231.8 jit_solution(10339489891016880196)
XLA Ops:
  9.8 4.3 %all-to-all-start = ((bf16[8,32,2048]{2,1,0:T(8,128)(2,1)}), bf16[8,32,2048]{2,1,0:T(8,128)(2,1)S(1)}, u32[]{:S(2)}, u32[]{:S(2)}) async-start(bf16[8,32,2048]{2,1,0:T(8,128)(2,1)} %broadcast_in_dim.64), calls=%async_computation | async-start | bytes 2097152 | tf_op jit(solution)/shard_map/all_to_all | solution.py:27
  17.6 12.5 %all-to-all-done = bf16[8,32,2048]{2,1,0:T(8,128)(2,1)S(1)} async-done(((bf16[8,32,2048]{2,1,0:T(8,128)(2,1)}), bf16[8,32,2048]{2,1,0:T(8,128)(2,1)S(1)}, u32[]{:S(2)}, u32[]{:S(2)}) %all-to-all-start) | async-done | bytes 1048608 | tf_op jit(solution)/shard_map/all_to_all | solution.py:27
  33.1 3.5 %collective-permute-start = (bf16[3,128]{1,0:T(4,128)(2,1)S(1)}, bf16[3,128]{1,0:T(4,128)(2,1)S(1)}, u32[]{:S(2)}, u32[]{:S(2)}) collective-permute-start(bf16[3,128]{1,0:T(4,128)(2,1)S(1)} %slice.550), channel_id=1, source_target_pairs={{0,8},{8,16},{16,24},{24,32},{32,40},{40,48},{48,56},{56,64},{64,7... | collective-permute-start | bytes 2312 | tf_op jit(solution)/shard_map/ppermute | solution.py:37
  37.9 3.4 %all-to-all-start.1 = ((bf16[4,1,256,128]{2,3,1,0:T(8,128)(2,1)}), bf16[4,1,256,128]{2,3,1,0:T(8,128)(2,1)S(1)}, u32[]{:S(2)}, u32[]{:S(2)}) async-start(bf16[4,1,256,128]{2,3,1,0:T(8,128)(2,1)} %broadcast_in_dim.69), calls=%async_computation.1 | async-start | bytes 524288 | tf_op jit(solution)/shard_map/all_to_all | solution.py:27
  44.3 16.0 %all-gather = f32[8,1,128]{2,1,0:T(1,128)S(1)} all-gather(f32[1,1,128]{2,1,0:T(1,128)S(1)} %add_bitcast_fusion.1), channel_id=1, replica_groups=mesh['sp_0'=8,'sp_1'=8,'fs'=4,'tp'=2] {'sp_1'}, dimensions={0}, use_global_device_ids=true | all-gather | bytes 4608 | tf_op jit(solution)/shard_map/all_gather | solution.py:51
  60.3 13.8 %all-gather.1 = f32[8,1,128]{2,1,0:T(1,128)} all-gather(f32[1,1,128]{2,1,0:T(1,128)S(1)} %fusion.92), channel_id=1, replica_groups=mesh['sp_0'=8,'sp_1'=8,'fs'=4,'tp'=2] {'sp_0'}, dimensions={0}, use_global_device_ids=true | all-gather | bytes 4608 | tf_op jit(solution)/shard_map/all_gather | solution.py:51
  74.2 13.9 %all-gather.2 = f32[8,1,128]{2,1,0:T(1,128)S(1)} all-gather(f32[1,1,128]{2,1,0:T(1,128)S(1)} %add_bitcast_fusion), channel_id=1, replica_groups=mesh['sp_0'=8,'sp_1'=8,'fs'=4,'tp'=2] {'sp_1'}, dimensions={0}, use_global_device_ids=true | all-gather | bytes 4608 | tf_op jit(solution)/shard_map/all_gather | solution.py:51
  88.1 16.6 %all-gather.3 = f32[8,1,128]{2,1,0:T(1,128)} all-gather(f32[1,1,128]{2,1,0:T(1,128)S(1)} %fusion.84), channel_id=1, replica_groups=mesh['sp_0'=8,'sp_1'=8,'fs'=4,'tp'=2] {'sp_0'}, dimensions={0}, use_global_device_ids=true | all-gather | bytes 4608 | tf_op jit(solution)/shard_map/all_gather | solution.py:51
  104.8 7.2 %all-gather.6.cloned.1.call-done = bf16[4096,256]{1,0:T(8,128)(2,1)} async-done(((bf16[64,256]{1,0:T(8,128)(2,1)}), bf16[4096,256]{1,0:T(8,128)(2,1)}) %all-gather.6.cloned.1.call-update) | async-done | bytes 2097168 | tf_op jit(solution)/shard_map/all_gather | solution.py:67
  112.0 2.7 %fusion.99 = (bf16[4096,128]{1,0:T(8,128)(2,1)}, bf16[4096,128]{1,0:T(8,128)(2,1)S(1)}) fusion(bf16[4096,256]{1,0:T(8,128)(2,1)} %all-gather.6.cloned.1.call-done), kind=kLoop, calls=%fused_computation.268 | loop fusion | bytes 4194304 | tf_op jit(solution)/shard_map/split | solution.py:67
  116.0 66.8 %while.17 = (s32[]{:T(128)}, f32[4,2,256]{2,0,1:T(4,128)S(1)}, f32[4,2,256]{2,0,1:T(4,128)S(1)}, f32[4,2,256,128]{3,2,1,0:T(8,128)S(1)}, s32[4096]{0:T(1024)}, /...) while((s32[]{:T(128)}, f32[4,2,256]{2,0,1:T(4,128)S(1)}, ...), condition=%wide.region_6.7_spmd, body=%wide.region_1.6_spmd.sunk | while | flops 412749824 | bytes 16006993 | solution.py:141
  119.0 5.4 %conditional.2 = ((f32[4,2,256]{2,0,1:T(4,128)S(1)}, f32[4,2,256]{2,0,1:T(4,128)S(1)}, f32[4,2,256,128]{3,2,1,0:T(8,128)S(1)})) conditional(s32[]{:T(128)} %bitcast.358, (f32[4,2,256]{2,0,1:T(4,128)S(1)}, f32[4,2,256]{2,0,1:T(4,128)S(1)}, f32[4,2,256,128]{3,2,1,0:T(8,128)S(1)}) %tuple.78, (s32[512]{0:T(512)S(1)}, s32[256]{0:T(256)S(1)}, ...), branch_computations={%region_2.2_spmd, %region_3.5_spmd} | conditional | flops 412749824 | bytes 16002596 | solution.py:139
  122.1 2.3 fusion.5
  127.4 5.3 %conditional.2 = ((f32[4,2,256]{2,0,1:T(4,128)S(1)}, f32[4,2,256]{2,0,1:T(4,128)S(1)}, f32[4,2,256,128]{3,2,1,0:T(8,128)S(1)})) conditional(s32[]{:T(128)} %bitcast.358, (f32[4,2,256]{2,0,1:T(4,128)S(1)}, f32[4,2,256]{2,0,1:T(4,128)S(1)}, f32[4,2,256,128]{3,2,1,0:T(8,128)S(1)}) %tuple.78, (s32[512]{0:T(512)S(1)}, s32[256]{0:T(256)S(1)}, ...), branch_computations={%region_2.2_spmd, %region_3.5_spmd} | conditional | flops 412749824 | bytes 16002596 | solution.py:139
  130.4 2.3 fusion.5
  135.7 5.4 %conditional.2 = ((f32[4,2,256]{2,0,1:T(4,128)S(1)}, f32[4,2,256]{2,0,1:T(4,128)S(1)}, f32[4,2,256,128]{3,2,1,0:T(8,128)S(1)})) conditional(s32[]{:T(128)} %bitcast.358, (f32[4,2,256]{2,0,1:T(4,128)S(1)}, f32[4,2,256]{2,0,1:T(4,128)S(1)}, f32[4,2,256,128]{3,2,1,0:T(8,128)S(1)}) %tuple.78, (s32[512]{0:T(512)S(1)}, s32[256]{0:T(256)S(1)}, ...), branch_computations={%region_2.2_spmd, %region_3.5_spmd} | conditional | flops 412749824 | bytes 16002596 | solution.py:139
  138.8 2.3 fusion.5
  144.1 5.4 %conditional.2 = ((f32[4,2,256]{2,0,1:T(4,128)S(1)}, f32[4,2,256]{2,0,1:T(4,128)S(1)}, f32[4,2,256,128]{3,2,1,0:T(8,128)S(1)})) conditional(s32[]{:T(128)} %bitcast.358, (f32[4,2,256]{2,0,1:T(4,128)S(1)}, f32[4,2,256]{2,0,1:T(4,128)S(1)}, f32[4,2,256,128]{3,2,1,0:T(8,128)S(1)}) %tuple.78, (s32[512]{0:T(512)S(1)}, s32[256]{0:T(256)S(1)}, ...), branch_computations={%region_2.2_spmd, %region_3.5_spmd} | conditional | flops 412749824 | bytes 16002596 | solution.py:139
  147.1 2.3 fusion.5
  152.4 5.3 %conditional.2 = ((f32[4,2,256]{2,0,1:T(4,128)S(1)}, f32[4,2,256]{2,0,1:T(4,128)S(1)}, f32[4,2,256,128]{3,2,1,0:T(8,128)S(1)})) conditional(s32[]{:T(128)} %bitcast.358, (f32[4,2,256]{2,0,1:T(4,128)S(1)}, f32[4,2,256]{2,0,1:T(4,128)S(1)}, f32[4,2,256,128]{3,2,1,0:T(8,128)S(1)}) %tuple.78, (s32[512]{0:T(512)S(1)}, s32[256]{0:T(256)S(1)}, ...), branch_computations={%region_2.2_spmd, %region_3.5_spmd} | conditional | flops 412749824 | bytes 16002596 | solution.py:139
  155.5 2.3 fusion.5
  160.8 5.4 %conditional.2 = ((f32[4,2,256]{2,0,1:T(4,128)S(1)}, f32[4,2,256]{2,0,1:T(4,128)S(1)}, f32[4,2,256,128]{3,2,1,0:T(8,128)S(1)})) conditional(s32[]{:T(128)} %bitcast.358, (f32[4,2,256]{2,0,1:T(4,128)S(1)}, f32[4,2,256]{2,0,1:T(4,128)S(1)}, f32[4,2,256,128]{3,2,1,0:T(8,128)S(1)}) %tuple.78, (s32[512]{0:T(512)S(1)}, s32[256]{0:T(256)S(1)}, ...), branch_computations={%region_2.2_spmd, %region_3.5_spmd} | conditional | flops 412749824 | bytes 16002596 | solution.py:139
  163.8 2.3 fusion.5
  169.1 5.4 %conditional.2 = ((f32[4,2,256]{2,0,1:T(4,128)S(1)}, f32[4,2,256]{2,0,1:T(4,128)S(1)}, f32[4,2,256,128]{3,2,1,0:T(8,128)S(1)})) conditional(s32[]{:T(128)} %bitcast.358, (f32[4,2,256]{2,0,1:T(4,128)S(1)}, f32[4,2,256]{2,0,1:T(4,128)S(1)}, f32[4,2,256,128]{3,2,1,0:T(8,128)S(1)}) %tuple.78, (s32[512]{0:T(512)S(1)}, s32[256]{0:T(256)S(1)}, ...), branch_computations={%region_2.2_spmd, %region_3.5_spmd} | conditional | flops 412749824 | bytes 16002596 | solution.py:139
  172.2 2.3 fusion.5
  177.5 5.3 %conditional.2 = ((f32[4,2,256]{2,0,1:T(4,128)S(1)}, f32[4,2,256]{2,0,1:T(4,128)S(1)}, f32[4,2,256,128]{3,2,1,0:T(8,128)S(1)})) conditional(s32[]{:T(128)} %bitcast.358, (f32[4,2,256]{2,0,1:T(4,128)S(1)}, f32[4,2,256]{2,0,1:T(4,128)S(1)}, f32[4,2,256,128]{3,2,1,0:T(8,128)S(1)}) %tuple.78, (s32[512]{0:T(512)S(1)}, s32[256]{0:T(256)S(1)}, ...), branch_computations={%region_2.2_spmd, %region_3.5_spmd} | conditional | flops 412749824 | bytes 16002596 | solution.py:139
  180.5 2.3 fusion.5
  185.0 4.2 %all-to-all-start.2 = ((bf16[4,2,256,130]{2,1,3,0:T(2,128)(2,1)}), bf16[4,2,256,130]{2,1,3,0:T(2,128)(2,1)S(1)}, u32[]{:S(2)}, u32[]{:S(2)}) async-start(bf16[4,2,256,130]{2,1,3,0:T(2,128)(2,1)} %pad_maximum_fusion), calls=%async_computation.2 | async-start | bytes 1064960 | tf_op jit(solution)/shard_map/all_to_all | solution.py:74
  190.1 3.2 %fusion.31 = f32[256,2048]{1,0:T(8,128)} fusion(bf16[128,2048]{1,0:T(8,128)(2,1)S(1)} %copy-done, bf16[256,2048]{1,0:T(8,128)(2,1)S(1)} %bitcast.364, bf16[2048,128]{1,0:T(8,128)(2,1)} %param.27, f32[256,128]{1,0:T(8,128)S(1)} %pad.128, f32[256,128]{1,0:T(8,128)S(1)} %pad.129, f32[256,128]{1,0:T(8,128)} %copy-done.5, f32[256,128]{1,0:T(8,128)S(1)} %pad.113, ...), kind=kOutput, calls=%fused_computation.46 | convolution fusion | flops 268959744 | bytes 4719104 | tf_op jit(solution)/shard_map/dot_general | solution.py:279
  193.3 4.1 %all-to-all-done.2 = bf16[4,2,256,130]{2,1,3,0:T(2,128)(2,1)S(1)} async-done(((bf16[4,2,256,130]{2,1,3,0:T(2,128)(2,1)}), bf16[4,2,256,130]{2,1,3,0:T(2,128)(2,1)S(1)}, u32[]{:S(2)}, u32[]{:S(2)}) %all-to-all-start.2) | async-done | bytes 532512 | tf_op jit(solution)/shard_map/all_to_all | solution.py:74
  198.6 2.0 copy.92
  205.8 18.4 %all_to_all.20 = bf16[8,32,2048]{2,1,0:T(8,128)(2,1)S(1)} all-to-all(bf16[8,32,2048]{2,1,0:T(8,128)(2,1)S(1)} %bitcast.366), channel_id=1, replica_groups=mesh['sp_0'=8,'sp_1'=8,'fs'=4,'tp'=2] {'fs','tp'}, dimensions={0} | all-to-all | bytes 2097152 | tf_op jit(solution)/shard_map/all_to_all | solution.py:92
  (294 shorter events, 62.8 us)
Async XLA Ops:
  6.5 183.6 %copy-start = (bf16[128,2048]{1,0:T(8,128)(2,1)S(1)}, bf16[128,2048]{1,0:T(8,128)(2,1)}, u32[]{:S(2)}) copy-start(bf16[128,2048]{1,0:T(8,128)(2,1)} %param.36) | copy-start | bytes 1572868
  6.5 25.0 %copy-start.2 = (bf16[2048,128]{1,0:T(8,128)(2,1)S(1)}, bf16[2048,128]{1,0:T(8,128)(2,1)}, u32[]{:S(2)}) copy-start(bf16[2048,128]{1,0:T(8,128)(2,1)} %param.25) | copy-start | bytes 1572868
  6.5 26.1 %copy-start.3 = (bf16[2048,128]{1,0:T(8,128)(2,1)S(1)}, bf16[2048,128]{1,0:T(8,128)(2,1)}, u32[]{:S(2)}) copy-start(bf16[2048,128]{1,0:T(8,128)(2,1)} %param.26) | copy-start | bytes 1572868
  8.7 27.9 %copy-start.4 = (bf16[2048,128]{1,0:T(8,128)(2,1)S(1)}, bf16[2048,128]{1,0:T(8,128)(2,1)}, u32[]{:S(2)}) copy-start(bf16[2048,128]{1,0:T(8,128)(2,1)} %param.23) | copy-start | bytes 1572868
  9.8 20.2 %all-to-all-start = ((bf16[8,32,2048]{2,1,0:T(8,128)(2,1)}), bf16[8,32,2048]{2,1,0:T(8,128)(2,1)S(1)}, u32[]{:S(2)}, u32[]{:S(2)}) async-start(bf16[8,32,2048]{2,1,0:T(8,128)(2,1)} %broadcast_in_dim.64), calls=%async_computation | async-start | bytes 2097152 | tf_op jit(solution)/shard_map/all_to_all | solution.py:27
  14.1 97.8 %all-gather.6.cloned.1.call-start = ((), (), s32[]{:S(2)}) async-start(), calls=%async_computation.4 | async-start | bytes 2129920 | tf_op jit(solution)/shard_map/all_gather | solution.py:67
  30.1 11.4 %copy-start.11 = (bf16[2,64,64]{2,1,0:T(8,128)(2,1)S(1)}, bf16[2,64,64]{2,1,0:T(8,128)(2,1)}, u32[]{:S(2)}) copy-start(bf16[2,64,64]{2,1,0:T(8,128)(2,1)} %param.29) | copy-start | bytes 49156
  31.6 10.3 %copy-start.12 = (bf16[2,64,64]{2,1,0:T(8,128)(2,1)S(1)}, bf16[2,64,64]{2,1,0:T(8,128)(2,1)}, u32[]{:S(2)}) copy-start(bf16[2,64,64]{2,1,0:T(8,128)(2,1)} %param.30) | copy-start | bytes 49156
  31.6 10.6 %copy-start.6 = (f32[256,128]{1,0:T(8,128)S(1)}, f32[256,128]{1,0:T(8,128)}, u32[]{:S(2)}) copy-start(f32[256,128]{1,0:T(8,128)} %param.32) | copy-start | bytes 393220
  33.1 8.2 %collective-permute-start = (bf16[3,128]{1,0:T(4,128)(2,1)S(1)}, bf16[3,128]{1,0:T(4,128)(2,1)S(1)}, u32[]{:S(2)}, u32[]{:S(2)}) collective-permute-start(bf16[3,128]{1,0:T(4,128)(2,1)S(1)} %slice.550), channel_id=1, source_target_pairs={{0,8},{8,16},{16,24},{24,32},{32,40},{40,48},{48,56},{56,64},{64,7... | collective-permute-start | bytes 2312 | tf_op jit(solution)/shard_map/ppermute | solution.py:37
  37.9 66.8 %all-to-all-start.1 = ((bf16[4,1,256,128]{2,3,1,0:T(8,128)(2,1)}), bf16[4,1,256,128]{2,3,1,0:T(8,128)(2,1)S(1)}, u32[]{:S(2)}, u32[]{:S(2)}) async-start(bf16[4,1,256,128]{2,3,1,0:T(8,128)(2,1)} %broadcast_in_dim.69), calls=%async_computation.1 | async-start | bytes 524288 | tf_op jit(solution)/shard_map/all_to_all | solution.py:27
  44.2 71.8 %copy-start.9 = (s32[256]{0:T(256)S(1)}, s32[256]{0:T(256)}, u32[]{:S(2)}) copy-start(s32[256]{0:T(256)} %iota_add_fusion) | copy-start | bytes 3076
  44.3 60.5 %copy-start.5 = (f32[256,128]{1,0:T(8,128)}, f32[256,128]{1,0:T(8,128)S(1)}, u32[]{:S(2)}) copy-start(f32[256,128]{1,0:T(8,128)S(1)} %pad.112) | copy-start | bytes 393220
  60.3 44.4 %copy-start.7 = (f32[8,1,128]{2,1,0:T(1,128)}, f32[8,1,128]{2,1,0:T(1,128)S(1)}, u32[]{:S(2)}) copy-start(f32[8,1,128]{2,1,0:T(1,128)S(1)} %all-gather) | copy-start | bytes 12292
  88.1 16.6 %copy-start.8 = (f32[8,1,128]{2,1,0:T(1,128)}, f32[8,1,128]{2,1,0:T(1,128)S(1)}, u32[]{:S(2)}) copy-start(f32[8,1,128]{2,1,0:T(1,128)S(1)} %all-gather.2) | copy-start | bytes 12292
  185.0 12.4 %all-to-all-start.2 = ((bf16[4,2,256,130]{2,1,3,0:T(2,128)(2,1)}), bf16[4,2,256,130]{2,1,3,0:T(2,128)(2,1)S(1)}, u32[]{:S(2)}, u32[]{:S(2)}) async-start(bf16[4,2,256,130]{2,1,3,0:T(2,128)(2,1)} %pad_maximum_fusion), calls=%async_computation.2 | async-start | bytes 1064960 | tf_op jit(solution)/shard_map/all_to_all | solution.py:74
  190.1 14.0 %copy-start.10 = (f32[128]{0:T(128)S(1)}, f32[128]{0:T(128)}, u32[]{:S(2)}) copy-start(f32[128]{0:T(128)} %param.35) | copy-start | bytes 1540
  193.3 10.8 %copy-start.1 = (f32[256,2048]{1,0:T(8,128)S(1)}, f32[256,2048]{1,0:T(8,128)}, u32[]{:S(2)}) copy-start(f32[256,2048]{1,0:T(8,128)} %fusion.31) | copy-start | bytes 6291460
Sparse Core Ops, SparseCore 0:
  32.8 79.1 all-gather.5
where the time goes:
time: 233 us; the launch traced here: 232 us
  blocking collectives  78.8 us (34%)
  local copies, waits for them, and re-layouts  34.8 us (15%)
  matrix products  32.8 us (14%)
  waiting for transfers between devices  23.8 us (10%)
  other arithmetic  21.3 us (9%)
  starting transfers between devices  15.5 us (7%)
  between operations  15.1 us (6%)
  loops' own time  9.79 us (4%)
    all_gather x4, blocking collectives, prefix_by_axis(): pieces = jax.tree.map(lambda part: lax.all_gather(part, axis), total)  60.4 us
    all_to_all x1, blocking collectives, summed_on_arrival(): lax.all_to_all(pieces, axis, split_axis=0, concat_axis=0, tiled=True)  18.4 us
    dot_general x8, matrix products, attend(): jnp.einsum('hmqk,kv->hmqv', expos.astype(jnp.bfloat16), value_block, pref...  18.3 us
    all_to_all x2, waiting for transfers between devices, from_everyone(): return lax.all_to_all(copies, axis, split_axis=0, concat_axis=0, tiled=True)  12.5 us
    another operation x1, loops' own time, fold_keys(): return lax.fori_loop(0, total_keys // span, one_span, carried)  9.24 us
    convert_element_type x8, other arithmetic, attend(): expos.astype(jnp.bfloat16)  8.79 us
    slice x16, local copies, waits for them, and re-layouts, one_span(): return lax.cond(pos_block[0] <= query_pos[-1], attend, keep, running)  8.7 us
    all_to_all x2, starting transfers between devices, from_everyone(): return lax.all_to_all(copies, axis, split_axis=0, concat_axis=0, tiled=True)  7.7 us
  transfers between devices with their start and end apart: 5, of which 3 were waited for; matrix products, arithmetic and copies ran while one was open for 5% of the time, Pallas kernels for 0%

commit v1 on v0

v1 whole, which is shorter than its diff:
```python
import functools

import jax
import jax.numpy as jnp
from jax import lax
from jax.experimental import pallas as pl
from jax.experimental.pallas import tpu as pltpu
from jax.sharding import Mesh
from jax.sharding import PartitionSpec as P


SP = ("sp_0", "sp_1")
SP_FS_TP = ("sp_0", "sp_1", "fs", "tp")


gate_scale = 8.0
input_eps = 1e-06
head_eps = 1e-05
far_below = -1e30
log2_e = 1.4426950408889634


def from_everyone(value, axis):
    copies = jnp.broadcast_to(value, (lax.axis_size(axis), *value.shape))
    return lax.all_to_all(copies, axis, split_axis=0, concat_axis=0, tiled=True)


def passed_along(value, axis, by):
    devices = lax.axis_size(axis)
    pairs = [(i, i + by) for i in range(devices) if 0 <= i + by < devices]
    return lax.ppermute(value, axis, pairs)


def pair_combine(earlier, later):
    decay_early, state_early = earlier
    decay_late, state_late = later
    return (decay_early * decay_late, decay_late * state_early + state_late)


def prefix_by_axis(pair, axes):
    start = (jnp.ones_like(pair[0]), jnp.zeros_like(pair[1]))
    before = start
    total = (pair[0], pair[1])
    for axis in reversed(axes):
        devices, here = (lax.axis_size(axis), lax.axis_index(axis))
        gather = lax.all_gather if axis == axes[-1] else from_everyone
        pieces = gather(jnp.stack(total), axis)
        inside, total = (start, start)
        for k in range(devices):
            passed = k < here
            total = pair_combine(total, (pieces[k, 0], pieces[k, 1]))
            inside = jax.tree.map(lambda new, old: jnp.where(passed, new, old), total, inside)
        before = pair_combine(inside, before)
    return before


def attention_kernel(
    place, group, kv, packed, query, peak, total, values, value_t, *, block_rows, part_rows
):
    heads, size, rows = group.shape
    chunk_keys = kv.shape[1]
    z, y, member = (place[0], place[1], place[2])
    scale = (size // 2) ** (-0.5) * log2_e
    line = lax.broadcasted_iota(jnp.int32, (size, rows), 0)
    for h in range(heads):
        whole = group[h]
        zero = jnp.zeros_like(whole)
        query[2 * h] = jnp.where(line < size // 2, whole, zero)
        query[2 * h + 1] = jnp.where(line < size // 2, zero, whole)
    peak[...] = jnp.full(peak.shape, far_below, jnp.float32)
    total[...] = jnp.zeros(total.shape, jnp.float32)
    values[...] = jnp.zeros(values.shape, jnp.float32)

    def visible_keys():
        row = lax.broadcasted_iota(jnp.int32, (chunk_keys, rows), 0)
        lane = lax.broadcasted_iota(jnp.int32, (chunk_keys, rows), 1)
        key_pos = (row // part_rows) * block_rows + member * part_rows + row % part_rows
        half, piece = (rows // 2, part_rows // 2)
        inside = (lane % half) // piece * part_rows + lane // half * piece + lane % piece
        return key_pos <= inside + y * block_rows

    def one_chunk(at, masked):
        both = kv[at]
        keys = both[:, :size]
        value_t[...] = both[:, size:].T
        visible = visible_keys() if masked else None

        def scores_of(i):
            found = jnp.dot(keys, query[i], preferred_element_type=jnp.float32) * scale
            return jnp.where(visible, found, far_below) if masked else found

        scores = scores_of(0)
        for i in range(2 * heads):
            following = scores_of(i + 1) if i + 1 < 2 * heads else None
            old = peak[i]
            now = jnp.maximum(old, jnp.max(scores, axis=0, keepdims=True))
            expos = jnp.exp2(scores - now)
            if masked:
                expos = jnp.where(visible, expos, 0.0)
            fade = jnp.exp2(old - now)
            peak[i] = now
            total[i] = total[i] * fade + jnp.sum(expos, axis=0, keepdims=True)
            values[i] = values[i] * fade + jnp.dot(
                value_t[...], expos.astype(jnp.bfloat16), preferred_element_type=jnp.float32
            )
            scores = following

    one_chunk(z, True)

    def earlier(at, _):
        one_chunk(at, False)
        return 0

    lax.fori_loop(0, z, earlier, 0)

    half = rows // 2
    line = lax.broadcasted_iota(jnp.int32, (16, rows), 0)
    for h in range(heads):
        tail = jnp.zeros((16, rows), jnp.float32)
        for m in range(2):
            amount = total[2 * h + m]
            some = amount > 0.0
            safe = jnp.where(some, amount, 1.0)
            shares = (values[2 * h + m] * jnp.where(some, 1.0 / safe, 0.0)).astype(jnp.bfloat16)
            level = jnp.where(some, peak[2 * h + m] + jnp.log2(safe), far_below)
            coarse = level.astype(jnp.bfloat16).astype(jnp.float32)
            tail = jnp.where(line == 2 * m, coarse, tail)
            tail = jnp.where(line == 2 * m + 1, level - coarse, tail)
            for t in range(2):
                packed[h, t, m * size : (m + 1) * size, :] = shares[:, t * half : (t + 1) * half]
        rounded = tail.astype(jnp.bfloat16)
        for t in range(2):
            packed[h, t, 2 * size : 2 * size + 16, :] = rounded[:, t * half : (t + 1) * half]


def vmem():
    return pl.BlockSpec(memory_space=pltpu.VMEM)


def smem():
    return pl.BlockSpec(memory_space=pltpu.SMEM)


def attention(place, group, kv, block_rows, part_rows):
    heads, size, rows = group.shape
    z_count, chunk_keys, _ = kv.shape
    keys = chunk_keys * z_count
    return pl.pallas_call(
        functools.partial(attention_kernel, block_rows=block_rows, part_rows=part_rows),
        out_shape=jax.ShapeDtypeStruct((heads, 2, 2 * size + 16, rows // 2), jnp.bfloat16),
        in_specs=[smem(), vmem(), vmem()],
        out_specs=vmem(),
        scratch_shapes=[
            pltpu.VMEM((2 * heads, size, rows), jnp.bfloat16),
            pltpu.VMEM((2 * heads, 1, rows), jnp.float32),
            pltpu.VMEM((2 * heads, 1, rows), jnp.float32),
            pltpu.VMEM((2 * heads, size, rows), jnp.float32),
            pltpu.VMEM((size, chunk_keys), jnp.bfloat16),
        ],
        cost_estimate=pl.CostEstimate(
            flops=4 * 2 * heads * rows * keys * size,
            bytes_accessed=4 << 20,
            transcendentals=2 * heads * rows * keys,
        ),
        name="attention",
    )(place, group, kv)


def finish_kernel(place, lams, parts, gain, lru_mine, lru_theirs, w_mine, w_theirs, out):
    count, _, lines, _ = parts.shape
    size = (lines - 16) // 2
    core = place[0]

    def head_output(owner):
        joined = []
        for m in range(2):
            tails = [parts[i, owner, 2 * size :, :].astype(jnp.float32) for i in range(count)]
            levels = [t[2 * m : 2 * m + 1] + t[2 * m + 1 : 2 * m + 2] for t in tails]
            top = functools.reduce(jnp.maximum, levels)
            shares = [jnp.exp2(level - top) for level in levels]
            inverse = 1.0 / functools.reduce(jnp.add, shares)
            weighted = [
                parts[i, owner, m * size : (m + 1) * size, :].astype(jnp.float32)
                * (shares[i] * inverse)
                for i in range(count)
            ]
            joined.append(functools.reduce(jnp.add, weighted))
        diff = joined[0] - lams[owner] * joined[1]
        level = lax.rsqrt(jnp.mean(diff * diff, axis=0, keepdims=True) + head_eps)
        return (diff * level * gain[...]).T.astype(jnp.bfloat16)

    mine = jnp.concatenate([lru_mine[...], head_output(core)], axis=1)
    theirs = jnp.concatenate([lru_theirs[...], head_output(1 - core)], axis=1)
    result = jnp.dot(mine, w_mine[...], preferred_element_type=jnp.float32)
    result = result + jnp.dot(theirs, w_theirs[...], preferred_element_type=jnp.float32)
    out[...] = result.astype(jnp.bfloat16)


def finish(place, lams, parts, gain, lru_mine, lru_theirs, w_mine, w_theirs):
    rows, wide = (lru_mine.shape[0], w_mine.shape[1])
    return pl.pallas_call(
        finish_kernel,
        out_shape=jax.ShapeDtypeStruct((rows, wide), jnp.bfloat16),
        in_specs=[smem(), smem()] + [vmem()] * 6,
        out_specs=vmem(),
        cost_estimate=pl.CostEstimate(
            flops=2 * rows * wide * 512, bytes_accessed=3 << 20, transcendentals=rows * 16
        ),
        name="finish",
    )(place, lams, parts, gain, lru_mine, lru_theirs, w_mine, w_theirs)


def body(
    tokens,
    norm_gain,
    query_weight,
    w_key,
    w_value,
    w_input,
    w_gate,
    conv_kernel,
    w_recur,
    w_admit,
    decay_param,
    decay_scale,
    init_state,
    diff_lambda,
    head_gain,
    w_out_lru,
    w_out_attn,
):
    member_rows, wide = tokens.shape
    fs_count = lax.axis_size("fs")
    tp_count = lax.axis_size("tp")
    row_count = member_rows * fs_count * tp_count
    share_rows = member_rows * tp_count
    member = lax.axis_index("fs")
    core = lax.axis_index("tp")
    z_count, z = (lax.axis_size("sp_0"), lax.axis_index("sp_0"))
    y_count, y = (lax.axis_size("sp_1"), lax.axis_index("sp_1"))

    floats = tokens.astype(jnp.float32)
    normed = (
        floats * lax.rsqrt(jnp.mean(floats * floats, axis=1, keepdims=True) + input_eps) * norm_gain
    ).astype(jnp.bfloat16)

    taps = conv_kernel.shape[0]
    margin = 8
    before_rows = passed_along(normed[member_rows - margin :], SP, 1)

    chip_rows = lax.all_gather(normed, "tp", axis=0, tiled=True)
    kv_here = jnp.concatenate(
        [
            jnp.dot(chip_rows, weight, preferred_element_type=jnp.float32).astype(jnp.bfloat16)
            for weight in (w_key, w_value)
        ],
        axis=1,
    )
    kv_here, normed, before_rows = lax.optimization_barrier((kv_here, normed, before_rows))
    everyone = from_everyone(kv_here, SP)
    everyone = everyone.reshape(z_count, y_count * share_rows, kv_here.shape[1])

    sent = jnp.concatenate([normed, before_rows], axis=0)
    sent_rows = sent.shape[0]
    mine = lax.all_gather(sent, "fs", axis=0, tiled=True)
    swap = [(0, 1), (1, 0)]
    theirs = lax.ppermute(mine, "tp", swap)

    def projected(weight):
        a, b = [
            jnp.dot(piece, weight, preferred_element_type=jnp.float32).astype(jnp.bfloat16)
            for piece in (mine, theirs)
        ]
        both = jnp.stack([jnp.where(core == 0, a, b), jnp.where(core == 0, b, a)], axis=0)
        return both.reshape(tp_count, fs_count, sent_rows, weight.shape[1])

    def in_order(both):
        return jnp.moveaxis(both[:, :, :member_rows], 0, 1).reshape(row_count, both.shape[3])

    query = projected(query_weight)[:, :, :member_rows].reshape(row_count, query_weight.shape[1])
    lru_all = projected(w_input)
    lru_in = in_order(lru_all)
    earlier_rows = lru_all[tp_count - 1, fs_count - 1, sent_rows - (taps - 1) :]
    gate_proj = in_order(projected(w_gate))

    group = lax.all_gather(query.T, "fs")

    w_mine = jnp.concatenate([w_out_lru, w_out_attn], axis=0)
    w_theirs = lax.ppermute(w_mine, "tp", swap)
    lams = lax.all_gather(diff_lambda, "tp", axis=0, tiled=True)

    channels = lru_in.shape[1]
    padded = jnp.concatenate([earlier_rows, lru_in], axis=0).astype(jnp.float32)
    conv_sum = jnp.zeros((row_count, channels), jnp.float32)
    for offset in range(taps):
        conv_sum = conv_sum + conv_kernel[offset] * padded[offset : offset + row_count]
    conv_out = conv_sum.astype(jnp.bfloat16)
    grouped = conv_out.reshape(row_count, w_recur.shape[0], w_recur.shape[1])
    recur = jax.nn.sigmoid(
        jnp.einsum("tni,nij->tnj", grouped, w_recur, preferred_element_type=jnp.float32).reshape(
            row_count, channels
        )
    )
    admit = jax.nn.sigmoid(
        jnp.einsum("tni,nij->tnj", grouped, w_admit, preferred_element_type=jnp.float32).reshape(
            row_count, channels
        )
    )
    log_decay = -gate_scale * recur * jax.nn.softplus(-decay_param) * decay_scale
    decay = jnp.exp(log_decay)
    drive = jnp.sqrt(-jnp.expm1(2.0 * log_decay)) * admit * conv_out.astype(jnp.float32)
    decay_run, local_states = lax.associative_scan(pair_combine, (decay, drive), axis=0)
    before_decay, before_state = prefix_by_axis(
        jnp.stack([decay_run[-1], local_states[-1]]), SP
    )
    entering = before_decay * init_state + before_state
    states = local_states + decay_run * entering[None, :]
    lru_out = (states * jax.nn.gelu(gate_proj.astype(jnp.float32))).astype(jnp.bfloat16)

    place = jnp.stack([z, y, member]).astype(jnp.int32)
    carried = attention(place, group, everyone, row_count, share_rows)
    lru_split = lru_out.reshape(fs_count, tp_count, member_rows, channels)
    lru_mine = lax.dynamic_index_in_dim(lru_split, core, 1, keepdims=False)
    lru_other = lax.dynamic_index_in_dim(lru_split, 1 - core, 1, keepdims=False)
    half_rows = fs_count * member_rows
    lru_theirs = lax.ppermute(lru_other.reshape(half_rows, channels), "tp", swap)

    lines = carried.shape[2]
    carried = carried.reshape(fs_count * tp_count, lines, half_rows)
    packed = lax.all_to_all(carried, ("fs", "tp"), split_axis=0, concat_axis=0, tiled=True)
    packed = packed.reshape(fs_count, tp_count, lines, half_rows)

    gain = jnp.broadcast_to(head_gain[:, None], (head_gain.shape[0], half_rows))
    partial = finish(
        core[None].astype(jnp.int32),
        lams,
        packed,
        gain,
        lru_mine.reshape(half_rows, channels),
        lru_theirs,
        w_mine,
        w_theirs,
    )
    partial = partial.reshape(fs_count, member_rows, wide)
    arrived = lax.all_to_all(partial, "fs", split_axis=0, concat_axis=0, tiled=True)
    return arrived.astype(jnp.float32).sum(axis=0).astype(jnp.bfloat16)


def solution(mesh):
    torus = Mesh(
        mesh.devices.reshape(8, 8, mesh.shape["fs"], mesh.shape["tp"]), ("sp_0", "sp_1", "fs", "tp")
    )

    return jax.shard_map(
        body,
        mesh=torus,
        in_specs=(
            P(SP_FS_TP, None),
            P(),
            P(None, ("fs", "tp")),
            P(None, "tp"),
            P(None, "tp"),
            P(None, ("fs", "tp")),
            P(None, ("fs", "tp")),
            P(None, ("fs", "tp")),
            P(("fs", "tp"), None, None),
            P(("fs", "tp"), None, None),
            P(("fs", "tp")),
            P(SP, ("fs", "tp")),
            P(("fs", "tp")),
            P(("fs", "tp")),
            P(),
            P(("fs", "tp"), None),
            P(("fs", "tp"), None),
        ),
        out_specs=P(SP_FS_TP, None),
        check_vma=False,
    )
```

time: 233 us -> 175 us (0.75)
  matrix products: 32.8 us -> 8.18 us
  Pallas kernels: 0 us -> 22.6 us
  waiting for transfers between devices: 23.8 us -> 1.87 us
  local copies, waits for them, and re-layouts: 34.8 us -> 17.4 us
  starting transfers between devices: 15.5 us -> 30.5 us
  between operations: 15.1 us -> 1.56 us
  loops' own time: 9.79 us -> 0 us
  other arithmetic: 21.3 us -> 12 us
    dot_general x22 -> x8, matrix products: 32.3 us -> 6.19 us  [the longest x6 5.76 us: projected(): jnp.dot(piece, weight, preferred_element_type=jnp.float32)]
    pallas_call x0 -> x2, Pallas kernels: none -> 22.6 us  [the longest x1 19.4 us: attention(): pl.pallas_call(functools.partial(attention_kernel, block_rows=block_rows,...]
    dynamic_slice x16 -> x1, local copies, waits for them, and re-layouts: 13.4 us -> 0.62 us  [body(): lru_other = lax.dynamic_index_in_dim(lru_split, 1 - core, 1, keepdims=False)]
    all_to_all x2, waiting for transfers between devices: 12.5 us -> 0.01 us  [from_everyone(): return lax.all_to_all(copies, axis, split_axis=0, concat_axis=0, tiled=True)]
    slice x19 -> x1, local copies, waits for them, and re-layouts: 9.88 us -> 0.01 us  [body(): before_rows = passed_along(normed[member_rows - margin:], SP, 1)]
    another operation x9 -> x0, loops' own time: 9.79 us -> none  [the longest x1 9.24 us: fold_keys(): return lax.fori_loop(0, total_keys // span, one_span, carried)]
    all_to_all x2, starting transfers between devices: 7.7 us -> 17 us  [from_everyone(): return lax.all_to_all(copies, axis, split_axis=0, concat_axis=0, tiled=True)]
    convert_element_type x8 -> x2, other arithmetic: 8.79 us -> 0.09 us  [the longest x1 0.07 us: body(): (states * jax.nn.gelu(gate_proj.astype(jnp.float32))).astype(jnp.bfloat16)]
  transfers between devices with their start and end apart: 5 -> 7, of which waited for: 3 -> 1; matrix products, arithmetic and copies ran while one was open for 5% -> 20% of each run, Pallas kernels for 0% -> 11%
where the time goes in v1:
time: 175 us; the launch traced here: 173 us
  blocking collectives  78.3 us (45%)
  starting transfers between devices  30.5 us (17%)
  Pallas kernels  22.6 us (13%)
  local copies, waits for them, and re-layouts  17.4 us (10%)
  other arithmetic  12 us (7%)
  matrix products  8.18 us (5%)
  waiting for transfers between devices  1.87 us (1%)
    all_gather x1, blocking collectives, prefix_by_axis(): pieces = gather(jnp.stack(total), axis)  34.6 us
    pallas_call x1, Pallas kernels, attention(): pl.pallas_call(functools.partial(attention_kernel, block_rows=block_rows,...  19.4 us
    all_to_all x2, starting transfers between devices, from_everyone(): return lax.all_to_all(copies, axis, split_axis=0, concat_axis=0, tiled=True)  17 us
    all_gather x1, blocking collectives, body(): mine = lax.all_gather(sent, 'fs', axis=0, tiled=True)  13.4 us
    all_to_all x1, blocking collectives, body(): lax.all_to_all(partial, 'fs', split_axis=0, concat_axis=0, tiled=True)  12.9 us
    all_gather x1, blocking collectives, body(): group = lax.all_gather(query.T, 'fs')  11.6 us
    dot_general x6, matrix products, projected(): jnp.dot(piece, weight, preferred_element_type=jnp.float32)  5.76 us
    pad x28, local copies, waits for them, and re-layouts, body(): lax.associative_scan(pair_combine, (decay, drive), axis=0)  5.33 us
  transfers between devices with their start and end apart: 7, of which 1 were waited for; matrix products, arithmetic and copies ran while one was open for 20% of the time, Pallas kernels for 11%

profile of v1, /device:TPU:448, one launch (start us, length us, event | category | flops | bytes accessed | tf_op | source)
XLA Modules:
  0.0 172.5 jit_solution(13915970422280048745)
XLA Ops:
  0.0 1.2 fusion.6
  1.2 1.0 fusion.8
  2.2 3.5 %collective-permute-start = (bf16[8,2048]{1,0:T(8,128)(2,1)S(1)}, bf16[8,2048]{1,0:T(8,128)(2,1)S(1)}, u32[]{:S(2)}, u32[]{:S(2)}) collective-permute-start(bf16[8,2048]{1,0:T(8,128)(2,1)S(1)} %slice.493), channel_id=1, source_target_pairs={{0,8},{8,16},{16,24},{24,32},{32,40},{40,48},{48,56},{56,64},{64,7... | collective-permute-start | bytes 98312 | tf_op jit(solution)/shard_map/ppermute | solution.py:31
  5.7 1.1 constant_dynamic-update-slice_fusion.1
  6.8 1.1 constant_dynamic-update-slice_fusion.w_mine
  7.9 1.9 %collective-permute-start.3 = (bf16[256,2048]{1,0:T(8,128)(2,1)S(1)}, bf16[256,2048]{1,0:T(8,128)(2,1)}, u32[]{:S(2)}, u32[]{:S(2)}) collective-permute-start(bf16[256,2048]{1,0:T(8,128)(2,1)S(1)} %constant_dynamic-update-slice_fusion.w_mine), channel_id=1, source_target_pairs={{0,1},{1,0},{2,3},{3,2},{4,5},{5,4},{6,7},{7,6},{8,9},{9,8},{10,11... | collective-permute-start | bytes 3145736 | tf_op jit(solution)/shard_map/ppermute | solution.py:289
  9.8 2.8 %all_gather.22 = bf16[64,2048]{1,0:T(8,128)(2,1)S(1)} all-gather(bf16[32,2048]{1,0:T(8,128)(2,1)S(1)} %fusion.8), channel_id=1, replica_groups=mesh['sp_0'=8,'sp_1'=8,'fs'=4,'tp'=2] {'tp'}, dimensions={0}, use_global_device_ids=true | all-gather | bytes 393216 | tf_op jit(solution)/shard_map/all_gather | solution.py:251
  14.4 13.4 %all_gather.23 = bf16[160,2048]{1,0:T(8,128)(2,1)S(1)} all-gather(bf16[40,2048]{1,0:T(8,128)(2,1)S(1)} %pad_maximum_fusion), channel_id=1, replica_groups=mesh['sp_0'=8,'sp_1'=8,'fs'=4,'tp'=2] {'fs'}, dimensions={0}, use_global_device_ids=true | all-gather | bytes 819200 | tf_op jit(solution)/shard_map/all_gather | solution.py:265
  27.9 1.9 %collective-permute-start.1 = (bf16[160,2048]{1,0:T(8,128)(2,1)S(1)}, bf16[160,2048]{1,0:T(8,128)(2,1)S(1)}, u32[]{:S(2)}, u32[]{:S(2)}) collective-permute-start(bf16[160,2048]{1,0:T(8,128)(2,1)S(1)} %all_gather.23), channel_id=1, source_target_pairs={{0,1},{1,0},{2,3},{3,2},{4,5},{5,4},{6,7},{7,6},{8,9},{9,8},{10,11... | collective-permute-start | bytes 1966088 | tf_op jit(solution)/shard_map/ppermute | solution.py:267
  29.8 1.6 broadcast_in_dim.11
  31.4 9.9 %all-to-all-start = ((bf16[64,64,256]{2,1,0:T(8,128)(2,1)}), bf16[64,64,256]{2,1,0:T(8,128)(2,1)}, u32[]{:S(2)}, u32[]{:S(2)}) async-start(bf16[64,64,256]{2,1,0:T(8,128)(2,1)} %broadcast_in_dim.11), calls=%async_computation | async-start | bytes 4194304 | tf_op jit(solution)/shard_map/all_to_all | solution.py:25
  41.6 2.0 %convolution_convert_fusion.1 = bf16[160,128]{1,0:T(8,128)(2,1)} fusion(bf16[160,2048]{1,0:T(8,128)(2,1)S(1)} %all_gather.23, bf16[2048,128]{1,0:T(8,128)(2,1)} %param.23), kind=kOutput, calls=%fused_computation.9 | convolution fusion | flops 83906560 | bytes 1220608 | tf_op jit(solution)/shard_map/dot_general | solution.py:271
  43.6 0.9 convolution_convert_fusion.5
  45.1 1.0 fusion.3
  46.2 1.0 fusion.5
  53.6 1.3 pad.129
  56.4 1.5 fusion.23
  58.8 1.5 pad_maximum_fusion.4
  60.3 2.2 %pad.112 = f32[256,128]{1,0:T(8,128)} pad(f32[128,128]{1,0:T(8,128)} %pad_maximum_fusion.4, f32[]{:T(128)} %constant.27.clone.1), padding=0_1_1x0_0_0 | pad | bytes 196612 | tf_op jit(solution)/shard_map/pad | solution.py:312
  63.8 34.6 %all-gather.2 = f32[8,2,128]{2,1,0:T(2,128)S(1)} all-gather(f32[1,2,128]{2,1,0:T(2,128)S(1)} %maximum_bitcast_fusion), channel_id=3, replica_groups=mesh['sp_0'=8,'sp_1'=8,'fs'=4,'tp'=2] {'sp_1'}, dimensions={0}, use_global_device_ids=true | all-gather | bytes 9216 | tf_op jit(solution)/shard_map/all_gather | solution.py:47
  98.5 1.1 broadcast_select_fusion.5
  99.6 1.1 broadcast_select_fusion.1
  100.7 11.6 %all-gather = bf16[512,256]{0,1:T(8,128)(2,1)S(1)} all-gather(bf16[128,256]{0,1:T(8,128)(2,1)S(1)} %bitcast.311), channel_id=2, replica_groups=mesh['sp_0'=8,'sp_1'=8,'fs'=4,'tp'=2] {'fs'}, dimensions={0}, use_global_device_ids=true | all-gather | bytes 327680 | tf_op jit(solution)/shard_map/all_gather | solution.py:286
  113.8 7.1 %all-to-all-start.2 = ((f32[8,2,128]{2,1,0:T(2,128)}), f32[8,2,128]{2,1,0:T(2,128)S(1)}, u32[]{:S(2)}, u32[]{:S(2)}) async-start(f32[8,2,128]{2,1,0:T(2,128)} %broadcast_in_dim.26), calls=%async_computation.2 | async-start | bytes 16384 | tf_op jit(solution)/shard_map/all_to_all | solution.py:25
  120.9 19.4 %attention.1 = bf16[4,2,272,128]{3,2,1,0:T(8,128)(2,1)} custom-call(s32[3]{0:T(128)} %pad_add_fusion.2.place, bf16[4,128,256]{2,1,0:T(8,128)(2,1)} %bitcast.314, bf16[8,512,256]{2,1,0:T(8,128)(2,1)} %bitcast.10.kv), custom_call_target="tpu_custom_call" | custom-call | flops 4294967296 | bytes 4194304 | tf_op jit(solution)/shard_map/attention/pallas_call | solution.py:148
  140.4 3.8 %all-to-all-start.1 = ((bf16[8,272,128]{2,1,0:T(8,128)(2,1)}), bf16[8,272,128]{2,1,0:T(8,128)(2,1)S(1)}, u32[]{:S(2)}, u32[]{:S(2)}) async-start(bf16[8,272,128]{2,1,0:T(8,128)(2,1)} %bitcast.310), calls=%async_computation.1 | async-start | bytes 1114112 | tf_op jit(solution)/shard_map/all_to_all | solution.py:330
  144.9 2.4 %collective-permute-start.2 = (bf16[128,128]{1,0:T(8,128)(2,1)S(1)}, bf16[128,128]{1,0:T(8,128)(2,1)S(1)}, u32[]{:S(2)}, u32[]{:S(2)}) collective-permute-start(bf16[128,128]{1,0:T(8,128)(2,1)S(1)} %bitcast.327), channel_id=1, source_target_pairs={{0,1},{1,0},{2,3},{3,2},{4,5},{5,4},{6,7},{7,6},{8,9},{9,8},{10,11... | collective-permute-start | bytes 98312 | tf_op jit(solution)/shard_map/ppermute | solution.py:326
  148.0 1.3 dynamic-slice
  150.0 3.0 %all-reduce.32.lams = f32[2]{0:T(128)} all-reduce(f32[2]{0:T(128)S(1)} %dynamic-update-slice), channel_id=1, replica_groups=mesh['sp_0'=8,'sp_1'=8,'fs'=4,'tp'=2] {'tp'}, use_global_device_ids=true, to_apply=%add.32 | all-reduce | flops 2 | bytes 16
  153.0 1.9 %all-to-all-done.1 = bf16[8,272,128]{2,1,0:T(8,128)(2,1)S(1)} async-done(((bf16[8,272,128]{2,1,0:T(8,128)(2,1)}), bf16[8,272,128]{2,1,0:T(8,128)(2,1)S(1)}, u32[]{:S(2)}, u32[]{:S(2)}) %all-to-all-start.1) | async-done | bytes 557088 | tf_op jit(solution)/shard_map/all_to_all | solution.py:330
  155.6 3.2 %finish.1 = bf16[128,2048]{1,0:T(8,128)(2,1)} custom-call(s32[1]{0:T(128)} %bitcast.place, f32[2]{0:T(128)} %all-reduce.32.lams, bf16[4,2,272,128]{3,2,1,0:T(8,128)(2,1)} %bitcast.308, f32[128,128]{1,0:T(8,128)} %broadcast_in_dim.12.gain, bf16[128,128]{1,0:T(8,128)(2,1)} %bitcast.322, bf16[128,128]{1,0:T(8,128)(2,1)} %copy-done.10, ...), custom_call_target="tpu_custom_call" | custom-call | flops 268435456 | bytes 3145728 | tf_op jit(solution)/shard_map/finish/pallas_call | solution.py:201
  158.9 12.9 %all_to_all.20 = bf16[4,32,2048]{2,1,0:T(8,128)(2,1)S(1)} all-to-all(bf16[4,32,2048]{2,1,0:T(8,128)(2,1)} %bitcast.309), channel_id=1, replica_groups=mesh['sp_0'=8,'sp_1'=8,'fs'=4,'tp'=2] {'fs'}, dimensions={0} | all-to-all | bytes 1048576 | tf_op jit(solution)/shard_map/all_to_all | solution.py:345
  (193 shorter events, 16.8 us)
Async XLA Ops:
  0.0 41.3 %copy-start = (bf16[2048,128]{1,0:T(8,128)(2,1)S(1)}, bf16[2048,128]{1,0:T(8,128)(2,1)}, u32[]{:S(2)}) copy-start(bf16[2048,128]{1,0:T(8,128)(2,1)} %param.22) | copy-start | bytes 1572868
  0.0 12.7 %copy-start.7 = (bf16[2048,128]{1,0:T(8,128)(2,1)S(1)}, bf16[2048,128]{1,0:T(8,128)(2,1)}, u32[]{:S(2)}) copy-start(bf16[2048,128]{1,0:T(8,128)(2,1)} %param.21) | copy-start | bytes 1572868
  0.0 12.9 %copy-start.8 = (bf16[2048,128]{1,0:T(8,128)(2,1)S(1)}, bf16[2048,128]{1,0:T(8,128)(2,1)}, u32[]{:S(2)}) copy-start(bf16[2048,128]{1,0:T(8,128)(2,1)} %param.20) | copy-start | bytes 1572868
  2.2 10.9 %copy-start.12 = (f32[4,128]{1,0:T(4,128)S(1)}, f32[4,128]{1,0:T(4,128)}, u32[]{:S(2)}) copy-start(f32[4,128]{1,0:T(4,128)} %param.24) | copy-start | bytes 6148
  2.2 10.9 %copy-start.15 = (f32[128]{0:T(128)S(1)}, f32[128]{0:T(128)}, u32[]{:S(2)}) copy-start(f32[128]{0:T(128)} %param.27) | copy-start | bytes 1540
  2.2 12.2 %collective-permute-start = (bf16[8,2048]{1,0:T(8,128)(2,1)S(1)}, bf16[8,2048]{1,0:T(8,128)(2,1)S(1)}, u32[]{:S(2)}, u32[]{:S(2)}) collective-permute-start(bf16[8,2048]{1,0:T(8,128)(2,1)S(1)} %slice.493), channel_id=1, source_target_pairs={{0,8},{8,16},{16,24},{24,32},{32,40},{40,48},{48,56},{56,64},{64,7... | collective-permute-start | bytes 98312 | tf_op jit(solution)/shard_map/ppermute | solution.py:31
  7.9 23.5 %copy-start.1 = (bf16[256,2048]{1,0:T(8,128)(2,1)}, bf16[256,2048]{1,0:T(8,128)(2,1)S(1)}, u32[]{:S(2)}) copy-start(bf16[256,2048]{1,0:T(8,128)(2,1)S(1)} %constant_dynamic-update-slice_fusion.w_mine) | copy-start | bytes 3145732
  7.9 145.1 %collective-permute-start.3 = (bf16[256,2048]{1,0:T(8,128)(2,1)S(1)}, bf16[256,2048]{1,0:T(8,128)(2,1)}, u32[]{:S(2)}, u32[]{:S(2)}) collective-permute-start(bf16[256,2048]{1,0:T(8,128)(2,1)S(1)} %constant_dynamic-update-slice_fusion.w_mine), channel_id=1, source_target_pairs={{0,1},{1,0},{2,3},{3,2},{4,5},{5,4},{6,7},{7,6},{8,9},{9,8},{10,11... | collective-permute-start | bytes 3145736 | tf_op jit(solution)/shard_map/ppermute | solution.py:289
  13.2 31.8 %copy-start.11 = (f32[128]{0:T(128)}, f32[128]{0:T(128)S(1)}, u32[]{:S(2)}) copy-start(f32[128]{0:T(128)S(1)} %get-tuple-element.52) | copy-start | bytes 1540
  27.9 16.7 %collective-permute-start.1 = (bf16[160,2048]{1,0:T(8,128)(2,1)S(1)}, bf16[160,2048]{1,0:T(8,128)(2,1)S(1)}, u32[]{:S(2)}, u32[]{:S(2)}) collective-permute-start(bf16[160,2048]{1,0:T(8,128)(2,1)S(1)} %all_gather.23), channel_id=1, source_target_pairs={{0,1},{1,0},{2,3},{3,2},{4,5},{5,4},{6,7},{7,6},{8,9},{9,8},{10,11... | collective-permute-start | bytes 1966088 | tf_op jit(solution)/shard_map/ppermute | solution.py:267
  31.4 81.8 %all-to-all-start = ((bf16[64,64,256]{2,1,0:T(8,128)(2,1)}), bf16[64,64,256]{2,1,0:T(8,128)(2,1)}, u32[]{:S(2)}, u32[]{:S(2)}) async-start(bf16[64,64,256]{2,1,0:T(8,128)(2,1)} %broadcast_in_dim.11), calls=%async_computation | async-start | bytes 4194304 | tf_op jit(solution)/shard_map/all_to_all | solution.py:25
  41.3 2.3 %copy-start.3 = (bf16[2048,128]{1,0:T(8,128)(2,1)S(1)}, bf16[2048,128]{1,0:T(8,128)(2,1)}, u32[]{:S(2)}) copy-start(bf16[2048,128]{1,0:T(8,128)(2,1)} %param.19) | copy-start | bytes 1572868
  44.5 2.8 %copy-start.9 = (f32[256,128]{1,0:T(8,128)S(1)}, f32[256,128]{1,0:T(8,128)}, u32[]{:S(2)}) copy-start(f32[256,128]{1,0:T(8,128)} %param.28) | copy-start | bytes 393220
  52.7 46.9 %copy-start.4 = (bf16[2048,128]{1,0:T(8,128)(2,1)S(1)}, bf16[2048,128]{1,0:T(8,128)(2,1)}, u32[]{:S(2)}) copy-start(bf16[2048,128]{1,0:T(8,128)(2,1)} %param.23) | copy-start | bytes 1572868
  113.8 26.6 %all-to-all-start.2 = ((f32[8,2,128]{2,1,0:T(2,128)}), f32[8,2,128]{2,1,0:T(2,128)S(1)}, u32[]{:S(2)}, u32[]{:S(2)}) async-start(f32[8,2,128]{2,1,0:T(2,128)} %broadcast_in_dim.26), calls=%async_computation.2 | async-start | bytes 16384 | tf_op jit(solution)/shard_map/all_to_all | solution.py:25
  120.9 23.2 %copy-start.14 = (f32[128]{0:T(128)S(1)}, f32[128]{0:T(128)}, u32[]{:S(2)}) copy-start(f32[128]{0:T(128)} %param.29) | copy-start | bytes 1540
  120.9 23.3 %copy-start.5 = (f32[256,128]{1,0:T(8,128)S(1)}, f32[256,128]{1,0:T(8,128)}, u32[]{:S(2)}) copy-start(f32[256,128]{1,0:T(8,128)} %pad.129) | copy-start | bytes 393220
  120.9 23.3 %copy-start.6 = (f32[256,128]{1,0:T(8,128)S(1)}, f32[256,128]{1,0:T(8,128)}, u32[]{:S(2)}) copy-start(f32[256,128]{1,0:T(8,128)} %pad.112) | copy-start | bytes 393220
  120.9 33.9 %copy-start.13 = (f32[128]{0:T(128)S(1)}, f32[128]{0:T(128)}, u32[]{:S(2)}) copy-start(f32[128]{0:T(128)} %param.31) | copy-start | bytes 1540
  140.4 14.5 %all-to-all-start.1 = ((bf16[8,272,128]{2,1,0:T(8,128)(2,1)}), bf16[8,272,128]{2,1,0:T(8,128)(2,1)S(1)}, u32[]{:S(2)}, u32[]{:S(2)}) async-start(bf16[8,272,128]{2,1,0:T(8,128)(2,1)} %bitcast.310), calls=%async_computation.1 | async-start | bytes 1114112 | tf_op jit(solution)/shard_map/all_to_all | solution.py:330
  144.9 8.0 %collective-permute-start.2 = (bf16[128,128]{1,0:T(8,128)(2,1)S(1)}, bf16[128,128]{1,0:T(8,128)(2,1)S(1)}, u32[]{:S(2)}, u32[]{:S(2)}) collective-permute-start(bf16[128,128]{1,0:T(8,128)(2,1)S(1)} %bitcast.327), channel_id=1, source_target_pairs={{0,1},{1,0},{2,3},{3,2},{4,5},{5,4},{6,7},{7,6},{8,9},{9,8},{10,11... | collective-permute-start | bytes 98312 | tf_op jit(solution)/shard_map/ppermute | solution.py:326
  153.0 2.7 %copy-start.10 = (bf16[128,128]{1,0:T(8,128)(2,1)}, bf16[128,128]{1,0:T(8,128)(2,1)S(1)}, u32[]{:S(2)}) copy-start(bf16[128,128]{1,0:T(8,128)(2,1)S(1)} %collective-permute-done.2.lru_theirs) | copy-start | bytes 98308
  154.8 0.8 copy-start.2

commit v2 on v1

--- a/solution.py
+++ b/solution.py
@@ -37,21 +37,151 @@
     return (decay_early * decay_late, decay_late * state_early + state_late)
 
 
-def prefix_by_axis(pair, axes):
-    start = (jnp.ones_like(pair[0]), jnp.zeros_like(pair[1]))
-    before = start
-    total = (pair[0], pair[1])
-    for axis in reversed(axes):
-        devices, here = (lax.axis_size(axis), lax.axis_index(axis))
-        gather = lax.all_gather if axis == axes[-1] else from_everyone
-        pieces = gather(jnp.stack(total), axis)
-        inside, total = (start, start)
-        for k in range(devices):
+def vmem():
+    return pl.BlockSpec(memory_space=pltpu.VMEM)
+
+
+def smem():
+    return pl.BlockSpec(memory_space=pltpu.SMEM)
+
+
+def one_minus_exp(x):
+    series = jnp.full_like(x, 1.0)
+    for k in range(7, 1, -1):
+        series = 1.0 - series * x * (1.0 / k)
+    return jnp.where(x < 0.35, x * series, 1.0 - jnp.exp(-x))
+
+
+def project_kernel(
+    place, mine, theirs, w_query, w_input, w_gate, taps, w_recur, w_admit, rate, scale,
+    query_t, decays, states, gates, ends, *, fs_count, member_rows,
+):
+    core = place[3]
+    sent_rows = mine.shape[0] // fs_count
+    first = jnp.where(core == 0, mine[...], theirs[...])
+    second = jnp.where(core == 0, theirs[...], mine[...])
+    rows = jnp.concatenate([first, second], axis=0)
+
+    def project(weight):
+        return jnp.dot(rows, weight[...], preferred_element_type=jnp.float32)
+
+    def piece(value, t, f):
+        at = (t * fs_count + f) * sent_rows
+        return value[at : at + member_rows]
+
+    def in_order(value):
+        pieces = [piece(value, t, f) for f in range(fs_count) for t in range(2)]
+        return jnp.concatenate(pieces, axis=0)
+
+    query = project(w_query)
+    query = jnp.concatenate([piece(query, t, f) for t in range(2) for f in range(fs_count)], axis=0)
+    query_t[...] = query.astype(jnp.bfloat16).T
+
+    gate = in_order(project(w_gate).astype(jnp.bfloat16)).astype(jnp.float32)
+    gates[...] = jax.nn.gelu(gate)
+
+    lru_all = project(w_input).astype(jnp.bfloat16).astype(jnp.float32)
+    margin = sent_rows - member_rows
+    before = lru_all[2 * fs_count * sent_rows - margin :]
+    padded = jnp.concatenate([before, in_order(lru_all)], axis=0)
+    count = taps.shape[0]
+    conv_sum = padded[margin:] * taps[count - 1 : count, :]
+    for back in range(1, count):
+        moved = pltpu.roll(padded, back, 0)[margin:]
+        conv_sum = conv_sum + moved * taps[count - 1 - back : count - back, :]
+    conv_out = conv_sum.astype(jnp.bfloat16)
+
+    def gate_of(weight):
+        zero = jnp.zeros(weight.shape[1:], weight.dtype)
+        whole = jnp.concatenate(
+            [
+                jnp.concatenate([weight[0], zero], axis=1),
+                jnp.concatenate([zero, weight[1]], axis=1),
+            ],
+            axis=0,
+        )
+        return jax.nn.sigmoid(jnp.dot(conv_out, whole, preferred_element_type=jnp.float32))
+
+    log_decay = -gate_of(w_recur) * rate[...] * scale[...]
+    decay = jnp.exp(log_decay)
+    drive = jnp.sqrt(one_minus_exp(-2.0 * log_decay)) * gate_of(w_admit) * conv_out.astype(jnp.float32)
+
+    row = lax.broadcasted_iota(jnp.int32, decay.shape, 0)
+    by = 1
+    while by < decay.shape[0]:
+        inside = row >= by
+        decay_before = jnp.where(inside, pltpu.roll(decay, by, 0), 1.0)
+        state_before = jnp.where(inside, pltpu.roll(drive, by, 0), 0.0)
+        drive = decay * state_before + drive
+        decay = decay * decay_before
+        by *= 2
+    decays[...] = decay
+    states[...] = drive
+    last = decay.shape[0] - 1
+    ends[0:1, :] = decay[last:]
+    ends[1:2, :] = drive[last:]
+
+
+def project(place, mine, theirs, weights, taps, w_recur, w_admit, rate, scale, fs_count, rows):
+    channels = scale.shape[1]
+    block = jax.ShapeDtypeStruct(scale.shape, jnp.float32)
+    return pl.pallas_call(
+        functools.partial(project_kernel, fs_count=fs_count, member_rows=rows),
+        out_shape=(
+            jax.ShapeDtypeStruct((channels, scale.shape[0]), jnp.bfloat16),
+            block,
+            block,
+            block,
+            jax.ShapeDtypeStruct((2, channels), jnp.float32),
+        ),
+        in_specs=[smem()] + [vmem()] * 10,
+        out_specs=(vmem(),) * 5,
+        cost_estimate=pl.CostEstimate(
+            flops=2 * scale.shape[0] * mine.shape[1] * 3 * channels,
+            bytes_accessed=4 << 20,
+            transcendentals=1 << 18,
+        ),
+        name="project",
+    )(place, mine, theirs, *weights, taps, w_recur, w_admit, rate, scale)
+
+
+def states_kernel(
+    place, near, far, start, decays, states, gates, mine, theirs, *, fs_count, member_rows
+):
+    z, y, core = (place[0], place[1], place[3])
+
+    def before(pieces, here):
+        decay, state = (jnp.ones_like(pieces[0, 0:1]), jnp.zeros_like(pieces[0, 1:2]))
+        for k in range(pieces.shape[0]):
             passed = k < here
-            total = pair_combine(total, (pieces[k, 0], pieces[k, 1]))
-            inside = jax.tree.map(lambda new, old: jnp.where(passed, new, old), total, inside)
-        before = pair_combine(inside, before)
-    return before
+            new_decay, new_state = pair_combine((decay, state), (pieces[k, 0:1], pieces[k, 1:2]))
+            decay = jnp.where(passed, new_decay, decay)
+            state = jnp.where(passed, new_state, state)
+        return decay, state
+
+    decay, state = pair_combine(before(far, z), before(near, y))
+    entering = decay * start[...] + state
+    out = ((states[...] + decays[...] * entering) * gates[...]).astype(jnp.bfloat16)
+    for f in range(fs_count):
+        at = 2 * f * member_rows
+        even = out[at : at + member_rows]
+        odd = out[at + member_rows : at + 2 * member_rows]
+        mine[f * member_rows : (f + 1) * member_rows] = jnp.where(core == 0, even, odd)
+        theirs[f * member_rows : (f + 1) * member_rows] = jnp.where(core == 0, odd, even)
+
+
+def final_states(place, near, far, start, decays, states, gates, fs_count, member_rows):
+    half = jax.ShapeDtypeStruct((fs_count * member_rows, decays.shape[1]), jnp.bfloat16)
+    return pl.pallas_call(
+        functools.partial(states_kernel, fs_count=fs_count, member_rows=member_rows),
+        out_shape=(half, half),
+        in_specs=[smem()] + [vmem()] * 6,
+        out_specs=(vmem(), vmem()),
+        cost_estimate=pl.CostEstimate(
+            flops=1 << 20, bytes_accessed=1 << 19, transcendentals=0
+        ),
+        name="final_states",
+    )(place, near, far, start, decays, states, gates)
 
 
 def attention_kernel(
@@ -131,14 +261,6 @@
         rounded = tail.astype(jnp.bfloat16)
         for t in range(2):
             packed[h, t, 2 * size : 2 * size + 16, :] = rounded[:, t * half : (t + 1) * half]
-
-
-def vmem():
-    return pl.BlockSpec(memory_space=pltpu.VMEM)
-
-
-def smem():
-    return pl.BlockSpec(memory_space=pltpu.SMEM)
 
 
 def attention(place, group, kv, block_rows, part_rows):
@@ -166,12 +288,12 @@
     )(place, group, kv)
 
 
-def finish_kernel(place, lams, parts, gain, lru_mine, lru_theirs, w_mine, w_theirs, out):
+def finish_kernel(place, lam, lam_theirs, parts, gain, lru_mine, lru_theirs, w_mine, w_theirs, out):
     count, _, lines, _ = parts.shape
     size = (lines - 16) // 2
-    core = place[0]
-
-    def head_output(owner):
+    core = place[3]
+
+    def head_output(owner, factor):
         joined = []
         for m in range(2):
             tails = [parts[i, owner, 2 * size :, :].astype(jnp.float32) for i in range(count)]
@@ -185,29 +307,29 @@
                 for i in range(count)
             ]
             joined.append(functools.reduce(jnp.add, weighted))
-        diff = joined[0] - lams[owner] * joined[1]
+        diff = joined[0] - factor * joined[1]
         level = lax.rsqrt(jnp.mean(diff * diff, axis=0, keepdims=True) + head_eps)
-        return (diff * level * gain[...]).T.astype(jnp.bfloat16)
-
-    mine = jnp.concatenate([lru_mine[...], head_output(core)], axis=1)
-    theirs = jnp.concatenate([lru_theirs[...], head_output(1 - core)], axis=1)
+        return ((diff * level).T * gain[...]).astype(jnp.bfloat16)
+
+    mine = jnp.concatenate([lru_mine[...], head_output(core, lam[0])], axis=1)
+    theirs = jnp.concatenate([lru_theirs[...], head_output(1 - core, lam_theirs[0])], axis=1)
     result = jnp.dot(mine, w_mine[...], preferred_element_type=jnp.float32)
     result = result + jnp.dot(theirs, w_theirs[...], preferred_element_type=jnp.float32)
     out[...] = result.astype(jnp.bfloat16)
 
 
-def finish(place, lams, parts, gain, lru_mine, lru_theirs, w_mine, w_theirs):
+def finish(place, lam, lam_theirs, parts, gain, lru_mine, lru_theirs, w_mine, w_theirs):
     rows, wide = (lru_mine.shape[0], w_mine.shape[1])
     return pl.pallas_call(
         finish_kernel,
         out_shape=jax.ShapeDtypeStruct((rows, wide), jnp.bfloat16),
-        in_specs=[smem(), smem()] + [vmem()] * 6,
+        in_specs=[smem()] * 3 + [vmem()] * 6,
         out_specs=vmem(),
         cost_estimate=pl.CostEstimate(
             flops=2 * rows * wide * 512, bytes_accessed=3 << 20, transcendentals=rows * 16
         ),
         name="finish",
-    )(place, lams, parts, gain, lru_mine, lru_theirs, w_mine, w_theirs)
+    )(place, lam, lam_theirs, parts, gain, lru_mine, lru_theirs, w_mine, w_theirs)
 
 
 def body(
@@ -244,7 +366,6 @@
         floats * lax.rsqrt(jnp.mean(floats * floats, axis=1, keepdims=True) + input_eps) * norm_gain
     ).astype(jnp.bfloat16)
 
-    taps = conv_kernel.shape[0]
     margin = 8
     before_rows = passed_along(normed[member_rows - margin :], SP, 1)
 
@@ -261,82 +382,56 @@
     everyone = everyone.reshape(z_count, y_count * share_rows, kv_here.shape[1])
 
     sent = jnp.concatenate([normed, before_rows], axis=0)
-    sent_rows = sent.shape[0]
     mine = lax.all_gather(sent, "fs", axis=0, tiled=True)
     swap = [(0, 1), (1, 0)]
     theirs = lax.ppermute(mine, "tp", swap)
 
-    def projected(weight):
-        a, b = [
-            jnp.dot(piece, weight, preferred_element_type=jnp.float32).astype(jnp.bfloat16)
-            for piece in (mine, theirs)
-        ]
-        both = jnp.stack([jnp.where(core == 0, a, b), jnp.where(core == 0, b, a)], axis=0)
-        return both.reshape(tp_count, fs_count, sent_rows, weight.shape[1])
-
-    def in_order(both):
-        return jnp.moveaxis(both[:, :, :member_rows], 0, 1).reshape(row_count, both.shape[3])
-
-    query = projected(query_weight)[:, :, :member_rows].reshape(row_count, query_weight.shape[1])
-    lru_all = projected(w_input)
-    lru_in = in_order(lru_all)
-    earlier_rows = lru_all[tp_count - 1, fs_count - 1, sent_rows - (taps - 1) :]
-    gate_proj = in_order(projected(w_gate))
-
-    group = lax.all_gather(query.T, "fs")
+    place = jnp.stack([z, y, member, core]).astype(jnp.int32)
+    rate = gate_scale * jax.nn.softplus(-decay_param)
+    query_t, decays, states, gates, ends = project(
+        place,
+        mine,
+        theirs,
+        (query_weight, w_input, w_gate),
+        conv_kernel,
+        w_recur,
+        w_admit,
+        rate[None],
+        decay_scale,
+        fs_count,
+        member_rows,
+    )
+
+    group = lax.all_gather(query_t, "fs")
+
+    near = lax.all_gather(ends, "sp_1")
+    row = (near[0, 0], near[0, 1])
+    for k in range(1, y_count):
+        row = pair_combine(row, (near[k, 0], near[k, 1]))
+    far = from_everyone(jnp.stack(row), "sp_0")
 
     w_mine = jnp.concatenate([w_out_lru, w_out_attn], axis=0)
     w_theirs = lax.ppermute(w_mine, "tp", swap)
-    lams = lax.all_gather(diff_lambda, "tp", axis=0, tiled=True)
-
-    channels = lru_in.shape[1]
-    padded = jnp.concatenate([earlier_rows, lru_in], axis=0).astype(jnp.float32)
-    conv_sum = jnp.zeros((row_count, channels), jnp.float32)
-    for offset in range(taps):
-        conv_sum = conv_sum + conv_kernel[offset] * padded[offset : offset + row_count]
-    conv_out = conv_sum.astype(jnp.bfloat16)
-    grouped = conv_out.reshape(row_count, w_recur.shape[0], w_recur.shape[1])
-    recur = jax.nn.sigmoid(
-        jnp.einsum("tni,nij->tnj", grouped, w_recur, preferred_element_type=jnp.float32).reshape(
-            row_count, channels
-        )
-    )
-    admit = jax.nn.sigmoid(
-        jnp.einsum("tni,nij->tnj", grouped, w_admit, preferred_element_type=jnp.float32).reshape(
-            row_count, channels
-        )
-    )
-    log_decay = -gate_scale * recur * jax.nn.softplus(-decay_param) * decay_scale
-    decay = jnp.exp(log_decay)
-    drive = jnp.sqrt(-jnp.expm1(2.0 * log_decay)) * admit * conv_out.astype(jnp.float32)
-    decay_run, local_states = lax.associative_scan(pair_combine, (decay, drive), axis=0)
-    before_decay, before_state = prefix_by_axis(
-        jnp.stack([decay_run[-1], local_states[-1]]), SP
-    )
-    entering = before_decay * init_state + before_state
-    states = local_states + decay_run * entering[None, :]
-    lru_out = (states * jax.nn.gelu(gate_proj.astype(jnp.float32))).astype(jnp.bfloat16)
-
-    place = jnp.stack([z, y, member]).astype(jnp.int32)
+    lam_theirs = lax.ppermute(diff_lambda, "tp", swap)
+
     carried = attention(place, group, everyone, row_count, share_rows)
-    lru_split = lru_out.reshape(fs_count, tp_count, member_rows, channels)
-    lru_mine = lax.dynamic_index_in_dim(lru_split, core, 1, keepdims=False)
-    lru_other = lax.dynamic_index_in_dim(lru_split, 1 - core, 1, keepdims=False)
-    half_rows = fs_count * member_rows
-    lru_theirs = lax.ppermute(lru_other.reshape(half_rows, channels), "tp", swap)
-
-    lines = carried.shape[2]
+    lines, half_rows = carried.shape[2:]
     carried = carried.reshape(fs_count * tp_count, lines, half_rows)
     packed = lax.all_to_all(carried, ("fs", "tp"), split_axis=0, concat_axis=0, tiled=True)
     packed = packed.reshape(fs_count, tp_count, lines, half_rows)
 
-    gain = jnp.broadcast_to(head_gain[:, None], (head_gain.shape[0], half_rows))
+    lru_mine, lru_other = final_states(
+        place, near, far, init_state[None], decays, states, gates, fs_count, member_rows
+    )
+    lru_theirs = lax.ppermute(lru_other, "tp", swap)
+
     partial = finish(
-        core[None].astype(jnp.int32),
-        lams,
+        place,
+        diff_lambda,
+        lam_theirs,
         packed,
-        gain,
-        lru_mine.reshape(half_rows, channels),
+        head_gain[None],
+        lru_mine,
         lru_theirs,
         w_mine,
         w_theirs,

time: 175 us -> 154 us (0.88)
  local copies, waits for them, and re-layouts: 17.4 us -> 3.13 us
  other arithmetic: 12 us -> 4.07 us
  matrix products: 8.18 us -> 1.48 us
  Pallas kernels: 22.6 us -> 29.3 us
  waiting for transfers between devices: 1.87 us -> 4.71 us
  starting transfers between devices: 30.5 us -> 32.6 us
    dot_general x8 -> x0, matrix products: 7.75 us -> none  [the longest x6 5.76 us: projected(): jnp.dot(piece, weight, preferred_element_type=jnp.float32)]
    pallas_call x0 -> x2, Pallas kernels: none -> 6.08 us  [the longest x1 4.27 us: project(): pl.pallas_call(functools.partial(project_kernel, fs_count=fs_count, membe...]
    pad x28 -> x0, local copies, waits for them, and re-layouts: 5.33 us -> none  [body(): lax.associative_scan(pair_combine, (decay, drive), axis=0)]
    slice x52 -> x0, local copies, waits for them, and re-layouts: 3.06 us -> none  [body(): lax.associative_scan(pair_combine, (decay, drive), axis=0)]
    unnamed x1 -> x0, blocking collectives: 2.96 us -> none
    add x16 -> x0, other arithmetic: 2.69 us -> none  [the longest x15 2.66 us: body(): lax.associative_scan(pair_combine, (decay, drive), axis=0)]
    add x15 -> x1, other arithmetic: 2.48 us -> 0.02 us  [pair_combine(): return (decay_early * decay_late, decay_late * state_early + state_late)]
    unnamed x36 -> x23, local copies, waits for them, and re-layouts: 3.18 us -> 0.91 us
  transfers between devices with their start and end apart: 7 -> 8, of which waited for: 1 -> 3; matrix products, arithmetic and copies ran while one was open for 20% -> 2% of each run, Pallas kernels for 11% -> 17%
where the time goes in v2:
time: 154 us; the launch traced here: 153 us
  blocking collectives  76.6 us (50%)
  starting transfers between devices  32.6 us (21%)
  Pallas kernels  29.3 us (19%)
  waiting for transfers between devices  4.71 us (3%)
  other arithmetic  4.07 us (3%)
  local copies, waits for them, and re-layouts  3.13 us (2%)
    all_gather x1, blocking collectives, body(): near = lax.all_gather(ends, 'sp_1')  33.9 us
    pallas_call x1, Pallas kernels, attention(): pl.pallas_call(functools.partial(attention_kernel, block_rows=block_rows,...  19.4 us
    all_to_all x2, starting transfers between devices, from_everyone(): return lax.all_to_all(copies, axis, split_axis=0, concat_axis=0, tiled=True)  16.9 us
    all_gather x1, blocking collectives, body(): group = lax.all_gather(query_t, 'fs')  14.2 us
    all_gather x1, blocking collectives, body(): mine = lax.all_gather(sent, 'fs', axis=0, tiled=True)  13.5 us
    all_to_all x1, blocking collectives, body(): lax.all_to_all(partial, 'fs', split_axis=0, concat_axis=0, tiled=True)  12.9 us
    pallas_call x1, Pallas kernels, project(): pl.pallas_call(functools.partial(project_kernel, fs_count=fs_count, membe...  4.27 us
    pallas_call x1, Pallas kernels, finish(): pl.pallas_call(finish_kernel, out_shape=jax.ShapeDtypeStruct((rows, wide)...  3.82 us
  transfers between devices with their start and end apart: 8, of which 3 were waited for; matrix products, arithmetic and copies ran while one was open for 2% of the time, Pallas kernels for 17%

profile of v2, /device:TPU:448, one launch (start us, length us, event | category | flops | bytes accessed | tf_op | source)
XLA Modules:
  0.0 152.7 jit_solution(4137283197680838338)
XLA Ops:
  0.0 1.1 fusion
  1.1 1.0 fusion.2
  2.1 3.5 %collective-permute-start.1 = (bf16[8,2048]{1,0:T(8,128)(2,1)S(1)}, bf16[8,2048]{1,0:T(8,128)(2,1)S(1)}, u32[]{:S(2)}, u32[]{:S(2)}) collective-permute-start(bf16[8,2048]{1,0:T(8,128)(2,1)S(1)} %slice.68), channel_id=1, source_target_pairs={{0,8},{8,16},{16,24},{24,32},{32,40},{40,48},{48,56},{56,64},{64,7... | collective-permute-start | bytes 98312 | tf_op jit(solution)/shard_map/ppermute | solution.py:31
  5.6 2.0 %all_gather.18 = bf16[64,2048]{1,0:T(8,128)(2,1)S(1)} all-gather(bf16[32,2048]{1,0:T(8,128)(2,1)S(1)} %fusion.2), channel_id=1, replica_groups=mesh['sp_0'=8,'sp_1'=8,'fs'=4,'tp'=2] {'tp'}, dimensions={0}, use_global_device_ids=true | all-gather | bytes 393216 | tf_op jit(solution)/shard_map/all_gather | solution.py:372
  7.6 0.2 convolution_convert_fusion
  7.9 1.3 convolution_convert_fusion.1
  9.1 0.9 collective-permute-done.1
  10.1 1.6 %broadcast_in_dim.18 = bf16[64,64,256]{2,1,0:T(8,128)(2,1)} broadcast(bf16[64,256]{1,0:T(8,128)(2,1)S(1)} %pad_maximum_fusion.1), dimensions={1,2} | broadcast | bytes 2129920 | tf_op jit(solution)/shard_map/broadcast_in_dim | solution.py:24
  11.6 10.0 %all-to-all-start = ((bf16[64,64,256]{2,1,0:T(8,128)(2,1)}), bf16[64,64,256]{2,1,0:T(8,128)(2,1)}, u32[]{:S(2)}, u32[]{:S(2)}) async-start(bf16[64,64,256]{2,1,0:T(8,128)(2,1)} %broadcast_in_dim.18), calls=%async_computation | async-start | bytes 4194304 | tf_op jit(solution)/shard_map/all_to_all | solution.py:25
  21.7 0.0 copy-start.6
  21.7 0.0 copy-start.10
  21.7 13.5 %all_gather.19.mine = bf16[160,2048]{1,0:T(8,128)(2,1)S(1)} all-gather(bf16[40,2048]{1,0:T(8,128)(2,1)S(1)} %pad_maximum_fusion), channel_id=1, replica_groups=mesh['sp_0'=8,'sp_1'=8,'fs'=4,'tp'=2] {'fs'}, dimensions={0}, use_global_device_ids=true | all-gather | bytes 819200 | tf_op jit(solution)/shard_map/all_gather | solution.py:385
  35.2 1.9 %collective-permute-start.2 = (bf16[160,2048]{1,0:T(8,128)(2,1)S(1)}, bf16[160,2048]{1,0:T(8,128)(2,1)}, u32[]{:S(2)}, u32[]{:S(2)}) collective-permute-start(bf16[160,2048]{1,0:T(8,128)(2,1)S(1)} %all_gather.19.mine), channel_id=1, source_target_pairs={{0,1},{1,0},{2,3},{3,2},{4,5},{5,4},{6,7},{7,6},{8,9},{9,8},{10,11... | collective-permute-start | bytes 1966088 | tf_op jit(solution)/shard_map/ppermute | solution.py:387
  37.3 2.4 %collective-permute-start.4 = (bf16[256,2048]{1,0:T(8,128)(2,1)S(1)}, bf16[256,2048]{1,0:T(8,128)(2,1)S(1)}, u32[]{:S(2)}, u32[]{:S(2)}) collective-permute-start(bf16[256,2048]{1,0:T(8,128)(2,1)S(1)} %constant_dynamic-update-slice_fusion.w_mine), channel_id=1, source_target_pairs={{0,1},{1,0},{2,3},{3,2},{4,5},{5,4},{6,7},{7,6},{8,9},{9,8},{10,11... | collective-permute-start | bytes 3145736 | tf_op jit(solution)/shard_map/ppermute | solution.py:414
  39.7 0.6 pad_add_fusion.place
  40.3 0.6 fusion.13.rate
  40.9 4.3 %project.1 = (bf16[128,256]{1,0:T(8,128)(2,1)}, f32[256,128]{1,0:T(8,128)}, f32[256,128]{1,0:T(8,128)}, f32[256,128]{1,0:T(8,128)}, f32[2,128]{1,0:T(2,128)}) custom-call(s32[4]{0:T(128)} %pad_add_fusion.place, bf16[160,2048]{1,0:T(8,128)(2,1)} %copy-done.1, bf16[160,2048]{1,0:T(8,128)(2,1)} %collective-permute-done.2.theirs, bf16[2048,128]{1,0:T(8,128)(2,1)} %w_query.1, ...), custom_call_target="tpu_custom_call" | custom-call | flops 402653184 | bytes 4194304 | tf_op jit(solution)/shard_map/project/pallas_call | solution.py:128
  45.1 33.9 %all-gather.2.near = f32[8,2,128]{2,1,0:T(2,128)S(1)} all-gather(f32[1,2,128]{2,1,0:T(2,128)} %bitcast.26), channel_id=3, replica_groups=mesh['sp_0'=8,'sp_1'=8,'fs'=4,'tp'=2] {'sp_1'}, dimensions={0}, use_global_device_ids=true | all-gather | bytes 9216 | tf_op jit(solution)/shard_map/all_gather | solution.py:407
  79.1 14.2 %all-gather = bf16[512,256]{1,0:T(8,128)(2,1)} all-gather(bf16[128,256]{1,0:T(8,128)(2,1)} %get-tuple-element.17), channel_id=2, replica_groups=mesh['sp_0'=8,'sp_1'=8,'fs'=4,'tp'=2] {'fs'}, dimensions={0}, use_global_device_ids=true | all-gather | bytes 327680 | tf_op jit(solution)/shard_map/all_gather | solution.py:405
  93.3 0.6 broadcast_in_dim.20
  93.9 6.9 %all-to-all-start.2 = ((f32[8,2,128]{2,1,0:T(2,128)}), f32[8,2,128]{2,1,0:T(2,128)S(1)}, u32[]{:S(2)}, u32[]{:S(2)}) async-start(f32[8,2,128]{2,1,0:T(2,128)} %broadcast_in_dim.20), calls=%async_computation.2 | async-start | bytes 16384 | tf_op jit(solution)/shard_map/all_to_all | solution.py:25
  100.8 19.4 %attention.1 = bf16[4,2,272,128]{3,2,1,0:T(8,128)(2,1)} custom-call(s32[4]{0:T(128)} %pad_add_fusion.place, bf16[4,128,256]{2,1,0:T(8,128)(2,1)} %bitcast.25, bf16[8,512,256]{2,1,0:T(8,128)(2,1)} %bitcast.6.kv), custom_call_target="tpu_custom_call" | custom-call | flops 4294967296 | bytes 4194304 | tf_op jit(solution)/shard_map/attention/pallas_call | solution.py:270
  120.2 3.5 %all-to-all-start.1 = ((bf16[8,272,128]{2,1,0:T(8,128)(2,1)}), bf16[8,272,128]{2,1,0:T(8,128)(2,1)S(1)}, u32[]{:S(2)}, u32[]{:S(2)}) async-start(bf16[8,272,128]{2,1,0:T(8,128)(2,1)} %bitcast.24), calls=%async_computation.1 | async-start | bytes 1114112 | tf_op jit(solution)/shard_map/all_to_all | solution.py:420
  123.8 1.8 %final_states.1 = (bf16[128,128]{1,0:T(8,128)(2,1)}, bf16[128,128]{1,0:T(8,128)(2,1)}) custom-call(s32[4]{0:T(128)} %pad_add_fusion.place, f32[8,2,128]{2,1,0:T(2,128)} %copy-done.7, f32[8,2,128]{2,1,0:T(2,128)} %copy-done.9, f32[1,128]{1,0:T(1,128)} %bitcast.27, f32[256,128]{1,0:T(8,128)} %get-tuple-element.20.decays, f32[256,128]{1,0:T(8,128)} %get-tuple-element.21.states, ...), custom_call_target="tpu_custom_call" | custom-call | flops 1048576 | bytes 524288 | tf_op jit(solution)/shard_map/final_states/pallas_call | solution.py:175
  125.6 2.3 %collective-permute-start.3 = (bf16[128,128]{1,0:T(8,128)(2,1)}, bf16[128,128]{1,0:T(8,128)(2,1)S(1)}, u32[]{:S(2)}, u32[]{:S(2)}) collective-permute-start(bf16[128,128]{1,0:T(8,128)(2,1)} %get-tuple-element.24), channel_id=1, source_target_pairs={{0,1},{1,0},{2,3},{3,2},{4,5},{5,4},{6,7},{7,6},{8,9},{9,8},{10,11... | collective-permute-start | bytes 98312 | tf_op jit(solution)/shard_map/ppermute | solution.py:426
  127.9 2.0 %collective-permute-start = (f32[1]{0:T(128)}, f32[1]{0:T(128)}, u32[]{:S(2)}, u32[]{:S(2)}) collective-permute-start(f32[1]{0:T(128)} %param.30), channel_id=1, source_target_pairs={{0,1},{1,0},{2,3},{3,2},{4,5},{5,4},{6,7},{7,6},{8,9},{9,8},{10,11... | collective-permute-start | bytes 20 | tf_op jit(solution)/shard_map/ppermute | solution.py:415
  130.6 0.6 collective-permute-done.lam_theirs
  131.2 3.1 %all-to-all-done.1 = bf16[8,272,128]{2,1,0:T(8,128)(2,1)S(1)} async-done(((bf16[8,272,128]{2,1,0:T(8,128)(2,1)}), bf16[8,272,128]{2,1,0:T(8,128)(2,1)S(1)}, u32[]{:S(2)}, u32[]{:S(2)}) %all-to-all-start.1) | async-done | bytes 557088 | tf_op jit(solution)/shard_map/all_to_all | solution.py:420
  134.4 0.8 copy-done.3
  135.2 3.8 %finish.1 = bf16[128,2048]{1,0:T(8,128)(2,1)} custom-call(s32[4]{0:T(128)} %pad_add_fusion.place, f32[1]{0:T(128)S(6)} %copy.19.lam, f32[1]{0:T(128)} %collective-permute-done.lam_theirs, bf16[4,2,272,128]{3,2,1,0:T(8,128)(2,1)} %bitcast.22, f32[1,128]{1,0:T(1,128)} %bitcast.28, bf16[128,128]{1,0:T(8,128)(2,1)} %get-tuple-element.23.lru_mine, ...), custom_call_target="tpu_custom_call" | custom-call | flops 268435456 | bytes 3145728 | tf_op jit(solution)/shard_map/finish/pallas_call | solution.py:323
  139.0 12.9 %all_to_all.20 = bf16[4,32,2048]{2,1,0:T(8,128)(2,1)S(1)} all-to-all(bf16[4,32,2048]{2,1,0:T(8,128)(2,1)} %bitcast.23), channel_id=1, replica_groups=mesh['sp_0'=8,'sp_1'=8,'fs'=4,'tp'=2] {'fs'}, dimensions={0} | all-to-all | bytes 1048576 | tf_op jit(solution)/shard_map/all_to_all | solution.py:440
  151.9 0.7 reduce_sum.22
  (33 shorter events, 0.2 us)
Async XLA Ops:
  0.0 7.6 %copy-start = (bf16[2048,128]{1,0:T(8,128)(2,1)S(1)}, bf16[2048,128]{1,0:T(8,128)(2,1)}, u32[]{:S(2)}) copy-start(bf16[2048,128]{1,0:T(8,128)(2,1)} %param.21) | copy-start | bytes 1572868
  2.1 7.9 %collective-permute-start.1 = (bf16[8,2048]{1,0:T(8,128)(2,1)S(1)}, bf16[8,2048]{1,0:T(8,128)(2,1)S(1)}, u32[]{:S(2)}, u32[]{:S(2)}) collective-permute-start(bf16[8,2048]{1,0:T(8,128)(2,1)S(1)} %slice.68), channel_id=1, source_target_pairs={{0,8},{8,16},{16,24},{24,32},{32,40},{40,48},{48,56},{56,64},{64,7... | collective-permute-start | bytes 98312 | tf_op jit(solution)/shard_map/ppermute | solution.py:31
  11.6 25.5 %copy-start.5 = (bf16[128,2048]{1,0:T(8,128)(2,1)S(1)}, bf16[128,2048]{1,0:T(8,128)(2,1)}, u32[]{:S(2)}) copy-start(bf16[128,2048]{1,0:T(8,128)(2,1)} %param.32) | copy-start | bytes 1572868
  11.6 81.7 %all-to-all-start = ((bf16[64,64,256]{2,1,0:T(8,128)(2,1)}), bf16[64,64,256]{2,1,0:T(8,128)(2,1)}, u32[]{:S(2)}, u32[]{:S(2)}) async-start(bf16[64,64,256]{2,1,0:T(8,128)(2,1)} %broadcast_in_dim.18), calls=%async_computation | async-start | bytes 4194304 | tf_op jit(solution)/shard_map/all_to_all | solution.py:25
  21.7 15.6 %copy-start.6 = (bf16[128,2048]{1,0:T(8,128)(2,1)S(1)}, bf16[128,2048]{1,0:T(8,128)(2,1)}, u32[]{:S(2)}) copy-start(bf16[128,2048]{1,0:T(8,128)(2,1)} %param.33) | copy-start | bytes 1572868
  21.7 18.6 %copy-start.10 = (f32[128]{0:T(128)S(1)}, f32[128]{0:T(128)}, u32[]{:S(2)}) copy-start(f32[128]{0:T(128)} %param.27) | copy-start | bytes 1540
  35.2 5.6 %copy-start.1 = (bf16[160,2048]{1,0:T(8,128)(2,1)}, bf16[160,2048]{1,0:T(8,128)(2,1)S(1)}, u32[]{:S(2)}) copy-start(bf16[160,2048]{1,0:T(8,128)(2,1)S(1)} %all_gather.19.mine) | copy-start | bytes 1966084
  35.2 5.6 %collective-permute-start.2 = (bf16[160,2048]{1,0:T(8,128)(2,1)S(1)}, bf16[160,2048]{1,0:T(8,128)(2,1)}, u32[]{:S(2)}, u32[]{:S(2)}) collective-permute-start(bf16[160,2048]{1,0:T(8,128)(2,1)S(1)} %all_gather.19.mine), channel_id=1, source_target_pairs={{0,1},{1,0},{2,3},{3,2},{4,5},{5,4},{6,7},{7,6},{8,9},{9,8},{10,11... | collective-permute-start | bytes 1966088 | tf_op jit(solution)/shard_map/ppermute | solution.py:387
  37.3 82.9 %copy-start.2 = (bf16[256,2048]{1,0:T(8,128)(2,1)}, bf16[256,2048]{1,0:T(8,128)(2,1)S(1)}, u32[]{:S(2)}) copy-start(bf16[256,2048]{1,0:T(8,128)(2,1)S(1)} %constant_dynamic-update-slice_fusion.w_mine) | copy-start | bytes 3145732
  37.3 94.0 %collective-permute-start.4 = (bf16[256,2048]{1,0:T(8,128)(2,1)S(1)}, bf16[256,2048]{1,0:T(8,128)(2,1)S(1)}, u32[]{:S(2)}, u32[]{:S(2)}) collective-permute-start(bf16[256,2048]{1,0:T(8,128)(2,1)S(1)} %constant_dynamic-update-slice_fusion.w_mine), channel_id=1, source_target_pairs={{0,1},{1,0},{2,3},{3,2},{4,5},{5,4},{6,7},{7,6},{8,9},{9,8},{10,11... | collective-permute-start | bytes 3145736 | tf_op jit(solution)/shard_map/ppermute | solution.py:414
  79.1 41.1 %copy-start.7 = (f32[8,2,128]{2,1,0:T(2,128)}, f32[8,2,128]{2,1,0:T(2,128)S(1)}, u32[]{:S(2)}) copy-start(f32[8,2,128]{2,1,0:T(2,128)S(1)} %all-gather.2.near) | copy-start | bytes 24580
  93.9 26.3 %all-to-all-start.2 = ((f32[8,2,128]{2,1,0:T(2,128)}), f32[8,2,128]{2,1,0:T(2,128)S(1)}, u32[]{:S(2)}, u32[]{:S(2)}) async-start(f32[8,2,128]{2,1,0:T(2,128)} %broadcast_in_dim.20), calls=%async_computation.2 | async-start | bytes 16384 | tf_op jit(solution)/shard_map/all_to_all | solution.py:25
  120.2 3.6 %copy-start.9 = (f32[8,2,128]{2,1,0:T(2,128)}, f32[8,2,128]{2,1,0:T(2,128)S(1)}, u32[]{:S(2)}) copy-start(f32[8,2,128]{2,1,0:T(2,128)S(1)} %all-to-all-done.2.far) | copy-start | bytes 24580
  120.2 14.1 %all-to-all-start.1 = ((bf16[8,272,128]{2,1,0:T(8,128)(2,1)}), bf16[8,272,128]{2,1,0:T(8,128)(2,1)S(1)}, u32[]{:S(2)}, u32[]{:S(2)}) async-start(bf16[8,272,128]{2,1,0:T(8,128)(2,1)} %bitcast.24), calls=%async_computation.1 | async-start | bytes 1114112 | tf_op jit(solution)/shard_map/all_to_all | solution.py:420
  125.6 5.6 %collective-permute-start.3 = (bf16[128,128]{1,0:T(8,128)(2,1)}, bf16[128,128]{1,0:T(8,128)(2,1)S(1)}, u32[]{:S(2)}, u32[]{:S(2)}) collective-permute-start(bf16[128,128]{1,0:T(8,128)(2,1)} %get-tuple-element.24), channel_id=1, source_target_pairs={{0,1},{1,0},{2,3},{3,2},{4,5},{5,4},{6,7},{7,6},{8,9},{9,8},{10,11... | collective-permute-start | bytes 98312 | tf_op jit(solution)/shard_map/ppermute | solution.py:426
  127.9 3.3 %collective-permute-start = (f32[1]{0:T(128)}, f32[1]{0:T(128)}, u32[]{:S(2)}, u32[]{:S(2)}) collective-permute-start(f32[1]{0:T(128)} %param.30), channel_id=1, source_target_pairs={{0,1},{1,0},{2,3},{3,2},{4,5},{5,4},{6,7},{7,6},{8,9},{9,8},{10,11... | collective-permute-start | bytes 20 | tf_op jit(solution)/shard_map/ppermute | solution.py:415
  131.2 3.2 %copy-start.8 = (bf16[128,128]{1,0:T(8,128)(2,1)}, bf16[128,128]{1,0:T(8,128)(2,1)S(1)}, u32[]{:S(2)}) copy-start(bf16[128,128]{1,0:T(8,128)(2,1)S(1)} %collective-permute-done.3.lru_theirs) | copy-start | bytes 98308
  131.2 3.2 %copy-start.4 = (bf16[256,2048]{1,0:T(8,128)(2,1)}, bf16[256,2048]{1,0:T(8,128)(2,1)S(1)}, u32[]{:S(2)}) copy-start(bf16[256,2048]{1,0:T(8,128)(2,1)S(1)} %collective-permute-done.4.w_theirs) | copy-start | bytes 3145732
  134.4 0.8 copy-start.3

commit v3 on v2

--- a/solution.py
+++ b/solution.py
@@ -184,12 +184,21 @@
     )(place, near, far, start, decays, states, gates)
 
 
-def attention_kernel(
-    place, group, kv, packed, query, peak, total, values, value_t, *, block_rows, part_rows
-):
+def attention_kernel(*refs, chunks, block_rows, part_rows, first, last):
+    place, flags, group = refs[:3]
+    kvs = refs[3 : 3 + chunks]
+    at = 3 + chunks
+    if not first:
+        before = refs[at : at + 3]
+        at += 3
+    if last:
+        packed = refs[at]
+        peak, total, values, query, value_t = refs[at + 1 :]
+    else:
+        peak, total, values, query, value_t = refs[at:]
     heads, size, rows = group.shape
-    chunk_keys = kv.shape[1]
-    z, y, member = (place[0], place[1], place[2])
+    chunk_keys = kvs[0].shape[0]
+    y, member = (place[1], place[2])
     scale = (size // 2) ** (-0.5) * log2_e
     line = lax.broadcasted_iota(jnp.int32, (size, rows), 0)
     for h in range(heads):
@@ -197,9 +206,14 @@
         zero = jnp.zeros_like(whole)
         query[2 * h] = jnp.where(line < size // 2, whole, zero)
         query[2 * h + 1] = jnp.where(line < size // 2, zero, whole)
-    peak[...] = jnp.full(peak.shape, far_below, jnp.float32)
-    total[...] = jnp.zeros(total.shape, jnp.float32)
-    values[...] = jnp.zeros(values.shape, jnp.float32)
+    if first:
+        peak[...] = jnp.full(peak.shape, far_below, jnp.float32)
+        total[...] = jnp.zeros(total.shape, jnp.float32)
+        values[...] = jnp.zeros(values.shape, jnp.float32)
+    else:
+        peak[...] = before[0][...]
+        total[...] = before[1][...]
+        values[...] = before[2][...]
 
     def visible_keys():
         row = lax.broadcasted_iota(jnp.int32, (chunk_keys, rows), 0)
@@ -209,10 +223,9 @@
         inside = (lane % half) // piece * part_rows + lane // half * piece + lane % piece
         return key_pos <= inside + y * block_rows
 
-    def one_chunk(at, masked):
-        both = kv[at]
-        keys = both[:, :size]
-        value_t[...] = both[:, size:].T
+    def one_chunk(kv, masked):
+        keys = kv[:, :size]
+        value_t[...] = kv[:, size:].T
         visible = visible_keys() if masked else None
 
         def scores_of(i):
@@ -235,14 +248,17 @@
             )
             scores = following
 
-    one_chunk(z, True)
-
-    def earlier(at, _):
-        one_chunk(at, False)
-        return 0
-
-    lax.fori_loop(0, z, earlier, 0)
-
+    for c in range(chunks):
+        if first and c == 0:
+            one_chunk(kvs[c], True)
+        else:
+
+            @pl.when(flags[c] > 0)
+            def _(c=c):
+                one_chunk(kvs[c], False)
+
+    if not last:
+        return
     half = rows // 2
     line = lax.broadcasted_iota(jnp.int32, (16, rows), 0)
     for h in range(heads):
@@ -263,29 +279,45 @@
             packed[h, t, 2 * size : 2 * size + 16, :] = rounded[:, t * half : (t + 1) * half]
 
 
-def attention(place, group, kv, block_rows, part_rows):
+def attention(place, flags, group, kvs, before, last, block_rows, part_rows):
     heads, size, rows = group.shape
-    z_count, chunk_keys, _ = kv.shape
-    keys = chunk_keys * z_count
+    chunk_keys = kvs[0].shape[0]
+    chunks = len(kvs)
+    first = before is None
+    small = jax.ShapeDtypeStruct((2 * heads, 1, rows), jnp.float32)
+    state = (small, small, jax.ShapeDtypeStruct((2 * heads, size, rows), jnp.float32))
+    scratch = [
+        pltpu.VMEM((2 * heads, size, rows), jnp.bfloat16),
+        pltpu.VMEM((size, chunk_keys), jnp.bfloat16),
+    ]
+    if last:
+        outs = jax.ShapeDtypeStruct((heads, 2, 2 * size + 16, rows // 2), jnp.bfloat16)
+        specs = vmem()
+        scratch = [pltpu.VMEM(s.shape, s.dtype) for s in state] + scratch
+    else:
+        outs = state
+        specs = (vmem(),) * 3
+    carried = () if first else tuple(before)
     return pl.pallas_call(
-        functools.partial(attention_kernel, block_rows=block_rows, part_rows=part_rows),
-        out_shape=jax.ShapeDtypeStruct((heads, 2, 2 * size + 16, rows // 2), jnp.bfloat16),
-        in_specs=[smem(), vmem(), vmem()],
-        out_specs=vmem(),
-        scratch_shapes=[
-            pltpu.VMEM((2 * heads, size, rows), jnp.bfloat16),
-            pltpu.VMEM((2 * heads, 1, rows), jnp.float32),
-            pltpu.VMEM((2 * heads, 1, rows), jnp.float32),
-            pltpu.VMEM((2 * heads, size, rows), jnp.float32),
-            pltpu.VMEM((size, chunk_keys), jnp.bfloat16),
-        ],
+        functools.partial(
+            attention_kernel,
+            chunks=chunks,
+            block_rows=block_rows,
+            part_rows=part_rows,
+            first=first,
+            last=last,
+        ),
+        out_shape=outs,
+        in_specs=[smem(), smem()] + [vmem()] * (1 + chunks + len(carried)),
+        out_specs=specs,
+        scratch_shapes=scratch,
         cost_estimate=pl.CostEstimate(
-            flops=4 * 2 * heads * rows * keys * size,
+            flops=4 * 2 * heads * rows * chunk_keys * chunks * size,
             bytes_accessed=4 << 20,
-            transcendentals=2 * heads * rows * keys,
+            transcendentals=2 * heads * rows * chunk_keys * chunks,
         ),
         name="attention",
-    )(place, group, kv)
+    )(place, flags, group, *kvs, *carried)
 
 
 def finish_kernel(place, lam, lam_theirs, parts, gain, lru_mine, lru_theirs, w_mine, w_theirs, out):
@@ -378,8 +410,20 @@
         axis=1,
     )
     kv_here, normed, before_rows = lax.optimization_barrier((kv_here, normed, before_rows))
-    everyone = from_everyone(kv_here, SP)
-    everyone = everyone.reshape(z_count, y_count * share_rows, kv_here.shape[1])
+    own = from_everyone(kv_here, "sp_1").reshape(y_count * share_rows, kv_here.shape[1])
+
+    steps = z_count // 2
+    up_pairs = [(i, i + 1) for i in range(z_count - 1)]
+    down_pairs = [
+        [(i, (i - 1) % z_count) for i in (2, 1, 0)],
+        [(i, (i - 1) % z_count) for i in (1, 0, z_count - 1)],
+        [(i, (i - 1) % z_count) for i in (0, z_count - 1, z_count - 2)],
+    ]
+    rising, falling = ([own], [own])
+    for step in range(1, steps + 1):
+        rising.append(lax.ppermute(rising[-1], "sp_0", up_pairs))
+        if step < steps:
+            falling.append(lax.ppermute(falling[-1], "sp_0", down_pairs[step - 1]))
 
     sent = jnp.concatenate([normed, before_rows], axis=0)
     mine = lax.all_gather(sent, "fs", axis=0, tiled=True)
@@ -404,7 +448,7 @@
 
     group = lax.all_gather(query_t, "fs")
 
-    near = lax.all_gather(ends, "sp_1")
+    near = from_everyone(ends, "sp_1")
     row = (near[0, 0], near[0, 1])
     for k in range(1, y_count):
         row = pair_combine(row, (near[k, 0], near[k, 1]))
@@ -414,7 +458,22 @@
     w_theirs = lax.ppermute(w_mine, "tp", swap)
     lam_theirs = lax.ppermute(diff_lambda, "tp", swap)
 
-    carried = attention(place, group, everyone, row_count, share_rows)
+    steps_of = jnp.arange(steps + 1)
+    ups = (z >= steps_of).astype(jnp.int32)
+    downs = (z + steps_of >= z_count).astype(jnp.int32)
+    flags = jnp.concatenate([ups, downs])
+
+    def pick(*at):
+        return jnp.stack([flags[i] for i in at])
+
+    n = steps + 1
+    kvs = (own, rising[1], falling[1])
+    carried = attention(place, pick(0, 1, n + 1), group, kvs, None, False, row_count, share_rows)
+    kvs = (rising[2], falling[2], rising[3], falling[3])
+    chosen = pick(2, n + 2, 3, n + 3)
+    carried = attention(place, chosen, group, kvs, carried, False, row_count, share_rows)
+    kvs = (rising[4],)
+    carried = attention(place, pick(4), group, kvs, carried, True, row_count, share_rows)
     lines, half_rows = carried.shape[2:]
     carried = carried.reshape(fs_count * tp_count, lines, half_rows)
     packed = lax.all_to_all(carried, ("fs", "tp"), split_axis=0, concat_axis=0, tiled=True)

time: 154 us -> 154 us (level)
  blocking collectives: 76.6 us -> 43.6 us
  starting transfers between devices: 32.6 us -> 49.5 us
  Pallas kernels: 29.3 us -> 34.8 us
  local copies, waits for them, and re-layouts: 3.13 us -> 7.14 us
  other arithmetic: 4.07 us -> 8 us
  waiting for transfers between devices: 4.71 us -> 7.53 us
    all_gather x1 -> x0, blocking collectives: 33.9 us -> none  [body(): near = lax.all_gather(ends, 'sp_1')]
    ppermute x0 -> x7, starting transfers between devices: none -> 15 us  [the longest x3 9.89 us: body(): falling.append(lax.ppermute(falling[-1], 'sp_0', down_pairs[step - 1]))]
    pallas_call x1 -> x3, Pallas kernels: 19.4 us -> 25 us  [attention(): pl.pallas_call(functools.partial(attention_kernel, chunks=chunks, block_r...]
    another operation x0 -> x2, other arithmetic: none -> 4.09 us  [pick(): return jnp.stack([flags[i] for i in at])]
    ppermute x0 -> x7, waiting for transfers between devices: none -> 3.73 us  [the longest x3 3.72 us: body(): falling.append(lax.ppermute(falling[-1], 'sp_0', down_pairs[step - 1]))]
    unnamed x23 -> x35, local copies, waits for them, and re-layouts: 0.91 us -> 3.93 us
    all_to_all x2 -> x3, starting transfers between devices: 16.9 us -> 19.1 us  [from_everyone(): return lax.all_to_all(copies, axis, split_axis=0, concat_axis=0, tiled=True)]
  transfers between devices with their start and end apart: 8 -> 16, of which waited for: 3 -> 3; matrix products, arithmetic and copies ran while one was open for 2% -> 7% of each run, Pallas kernels for 17% -> 20%
where the time goes in v3:
time: 154 us; the launch traced here: 152 us
  starting transfers between devices  49.5 us (32%)
  blocking collectives  43.6 us (28%)
  Pallas kernels  34.8 us (23%)
  other arithmetic  8 us (5%)
  waiting for transfers between devices  7.53 us (5%)
  local copies, waits for them, and re-layouts  7.14 us (5%)
    pallas_call x3, Pallas kernels, attention(): pl.pallas_call(functools.partial(attention_kernel, chunks=chunks, block_r...  25 us
    all_to_all x3, starting transfers between devices, from_everyone(): return lax.all_to_all(copies, axis, split_axis=0, concat_axis=0, tiled=True)  19.1 us
    all_gather x1, blocking collectives, body(): group = lax.all_gather(query_t, 'fs')  14.5 us
    all_gather x1, blocking collectives, body(): mine = lax.all_gather(sent, 'fs', axis=0, tiled=True)  13.4 us
    all_to_all x1, blocking collectives, body(): lax.all_to_all(partial, 'fs', split_axis=0, concat_axis=0, tiled=True)  12.9 us
    ppermute x3, starting transfers between devices, body(): falling.append(lax.ppermute(falling[-1], 'sp_0', down_pairs[step - 1]))  9.89 us
    ppermute x4, starting transfers between devices, body(): rising.append(lax.ppermute(rising[-1], 'sp_0', up_pairs))  5.15 us
    pallas_call x1, Pallas kernels, project(): pl.pallas_call(functools.partial(project_kernel, fs_count=fs_count, membe...  4.28 us
  transfers between devices with their start and end apart: 16, of which 3 were waited for; matrix products, arithmetic and copies ran while one was open for 7% of the time, Pallas kernels for 20%

profile of v3, /device:TPU:448, one launch (start us, length us, event | category | flops | bytes accessed | tf_op | source)
XLA Modules:
  0.0 152.0 jit_solution(16764799825252310611)
XLA Ops:
  0.0 1.1 fusion
  2.0 3.6 %collective-permute-start.1 = (bf16[8,2048]{1,0:T(8,128)(2,1)S(1)}, bf16[8,2048]{1,0:T(8,128)(2,1)S(1)}, u32[]{:S(2)}, u32[]{:S(2)}) collective-permute-start(bf16[8,2048]{1,0:T(8,128)(2,1)S(1)} %slice.98), channel_id=1, source_target_pairs={{0,8},{8,16},{16,24},{24,32},{32,40},{40,48},{48,56},{56,64},{64,7... | collective-permute-start | bytes 98312 | tf_op jit(solution)/shard_map/ppermute | solution.py:31
  5.6 1.1 constant_dynamic-update-slice_fusion.1
  6.8 2.1 %collective-permute-start.11 = (bf16[256,2048]{1,0:T(8,128)(2,1)S(1)}, bf16[256,2048]{1,0:T(8,128)(2,1)S(1)}, u32[]{:S(2)}, u32[]{:S(2)}) collective-permute-start(bf16[256,2048]{1,0:T(8,128)(2,1)S(1)} %constant_dynamic-update-slice_fusion.w_mine), channel_id=1, source_target_pairs={{0,1},{1,0},{2,3},{3,2},{4,5},{5,4},{6,7},{7,6},{8,9},{9,8},{10,11... | collective-permute-start | bytes 3145736 | tf_op jit(solution)/shard_map/ppermute | solution.py:458
  8.8 2.8 %all_gather.12 = bf16[64,2048]{1,0:T(8,128)(2,1)S(1)} all-gather(bf16[32,2048]{1,0:T(8,128)(2,1)S(1)} %fusion.2), channel_id=1, replica_groups=mesh['sp_0'=8,'sp_1'=8,'fs'=4,'tp'=2] {'tp'}, dimensions={0}, use_global_device_ids=true | all-gather | bytes 393216 | tf_op jit(solution)/shard_map/all_gather | solution.py:404
  13.5 6.2 %all-to-all-start = ((bf16[8,64,256]{2,1,0:T(8,128)(2,1)}), bf16[8,64,256]{2,1,0:T(8,128)(2,1)S(1)}, u32[]{:S(2)}, u32[]{:S(2)}) async-start(bf16[8,64,256]{2,1,0:T(8,128)(2,1)} %broadcast_in_dim.21), calls=%async_computation | async-start | bytes 524288 | tf_op jit(solution)/shard_map/all_to_all | solution.py:25
  19.7 13.4 %all_gather.13.mine = bf16[160,2048]{1,0:T(8,128)(2,1)S(1)} all-gather(bf16[40,2048]{1,0:T(8,128)(2,1)S(1)} %pad_maximum_fusion), channel_id=1, replica_groups=mesh['sp_0'=8,'sp_1'=8,'fs'=4,'tp'=2] {'fs'}, dimensions={0}, use_global_device_ids=true | all-gather | bytes 819200 | tf_op jit(solution)/shard_map/all_gather | solution.py:429
  33.1 1.9 %collective-permute-start.2 = (bf16[160,2048]{1,0:T(8,128)(2,1)S(1)}, bf16[160,2048]{1,0:T(8,128)(2,1)}, u32[]{:S(2)}, u32[]{:S(2)}) collective-permute-start(bf16[160,2048]{1,0:T(8,128)(2,1)S(1)} %all_gather.13.mine), channel_id=1, source_target_pairs={{0,1},{1,0},{2,3},{3,2},{4,5},{5,4},{6,7},{7,6},{8,9},{9,8},{10,11... | collective-permute-start | bytes 1966088 | tf_op jit(solution)/shard_map/ppermute | solution.py:431
  35.0 1.2 pad_add_fusion.2.refs_1_
  37.4 1.3 collective-permute-start.3
  38.7 1.3 collective-permute-start.7
  40.6 2.9 %pad_add_fusion.1.refs_1_ = s32[4]{0:T(128)} fusion(s32[1]{0:T(128)} %get-tuple-element.38, s32[1]{0:T(128)} %get-tuple-element.41, s32[1]{0:T(128)} %get-tuple-element.39, s32[1]{0:T(128)} %get-tuple-element.40), kind=kLoop, calls=%fused_computation.35 | loop fusion | flops 12 | bytes 32 | tf_op jit(solution)/shard_map/stack | solution.py:467
  43.6 4.3 %project.1 = (bf16[128,256]{1,0:T(8,128)(2,1)}, f32[256,128]{1,0:T(8,128)}, f32[256,128]{1,0:T(8,128)}, f32[256,128]{1,0:T(8,128)}, f32[2,128]{1,0:T(2,128)}) custom-call(s32[4]{0:T(128)} %pad_add_fusion.place.refs_0_, bf16[160,2048]{1,0:T(8,128)(2,1)} %copy-done.1, bf16[160,2048]{1,0:T(8,128)(2,1)} %collective-permute-done.2.theirs, ...), custom_call_target="tpu_custom_call" | custom-call | flops 402653184 | bytes 4194304 | tf_op jit(solution)/shard_map/project/pallas_call | solution.py:128
  49.1 7.2 %all-to-all-start.2 = ((f32[8,2,128]{2,1,0:T(2,128)}), f32[8,2,128]{2,1,0:T(2,128)S(1)}, u32[]{:S(2)}, u32[]{:S(2)}) async-start(f32[8,2,128]{2,1,0:T(2,128)} %broadcast_in_dim.23), calls=%async_computation.2 | async-start | bytes 16384 | tf_op jit(solution)/shard_map/all_to_all | solution.py:25
  56.3 1.3 collective-permute-start.4
  57.6 14.5 %all-gather = bf16[512,256]{1,0:T(8,128)(2,1)} all-gather(bf16[128,256]{1,0:T(8,128)(2,1)} %get-tuple-element.23), channel_id=2, replica_groups=mesh['sp_0'=8,'sp_1'=8,'fs'=4,'tp'=2] {'fs'}, dimensions={0}, use_global_device_ids=true | all-gather | bytes 327680 | tf_op jit(solution)/shard_map/all_gather | solution.py:449
  72.1 5.2 %collective-permute-start.8 = (bf16[512,256]{1,0:T(8,128)(2,1)}, bf16[512,256]{1,0:T(8,128)(2,1)S(1)}, u32[]{:S(2)}, u32[]{:S(2)}) collective-permute-start(bf16[512,256]{1,0:T(8,128)(2,1)} %collective-permute-done.7.refs_5_), channel_id=1, source_target_pairs={{64,0},{0,448},{448,384},{65,1},{1,449},{449,385},{66,2},{2,450},{... | collective-permute-start | bytes 786440 | tf_op jit(solution)/shard_map/ppermute | solution.py:426
  77.4 1.3 collective-permute-start.5
  78.7 3.7 %collective-permute-done.8.refs_4_ = bf16[512,256]{1,0:T(8,128)(2,1)S(1)} collective-permute-done((bf16[512,256]{1,0:T(8,128)(2,1)}, bf16[512,256]{1,0:T(8,128)(2,1)S(1)}, u32[]{:S(2)}, u32[]{:S(2)}) %collective-permute-start.8) | collective-permute-done | bytes 262176 | tf_op jit(solution)/shard_map/ppermute | solution.py:426
  82.4 3.4 %collective-permute-start.9 = (bf16[512,256]{1,0:T(8,128)(2,1)S(1)}, bf16[512,256]{1,0:T(8,128)(2,1)}, u32[]{:S(2)}, u32[]{:S(2)}) collective-permute-start(bf16[512,256]{1,0:T(8,128)(2,1)S(1)} %collective-permute-done.8.refs_4_), channel_id=1, source_target_pairs={{0,448},{448,384},{384,320},{1,449},{449,385},{385,321},{2,450},{4... | collective-permute-start | bytes 786440 | tf_op jit(solution)/shard_map/ppermute | solution.py:426
  86.4 5.7 %all-to-all-start.3 = ((f32[8,2,128]{2,1,0:T(2,128)}), f32[8,2,128]{2,1,0:T(2,128)S(1)}, u32[]{:S(2)}, u32[]{:S(2)}) async-start(f32[8,2,128]{2,1,0:T(2,128)} %broadcast_in_dim.24), calls=%async_computation.3 | async-start | bytes 16384 | tf_op jit(solution)/shard_map/all_to_all | solution.py:25
  92.1 1.3 collective-permute-start.6
  93.4 8.8 %attention.3 = (f32[8,1,256]{2,1,0:T(1,128)}, f32[8,1,256]{2,1,0:T(1,128)}, f32[8,128,256]{2,1,0:T(8,128)}) custom-call(s32[4]{0:T(128)} %pad_add_fusion.place.refs_0_, s32[3]{0:T(128)} %pad_add_fusion.2.refs_1_, bf16[4,128,256]{2,1,0:T(8,128)(2,1)} %bitcast.25, bf16[512,256]{1,0:T(8,128)(2,1)} %bitcast.30, bf16[512,256]{1,0:T(8,128)(2,1)} %collective-permute-done.3.refs_4_, ...), custom_call_target="tpu_custom_call" | custom-call | flops 1610612736 | bytes 4194304 | tf_op jit(solution)/shard_map/attention/pallas_call | solution.py:301
  102.2 11.1 %attention.4 = (f32[8,1,256]{2,1,0:T(1,128)}, f32[8,1,256]{2,1,0:T(1,128)}, f32[8,128,256]{2,1,0:T(8,128)}) custom-call(s32[4]{0:T(128)} %pad_add_fusion.place.refs_0_, s32[4]{0:T(128)} %pad_add_fusion.1.refs_1_, bf16[4,128,256]{2,1,0:T(8,128)(2,1)} %bitcast.26, bf16[512,256]{1,0:T(8,128)(2,1)} %copy-done.14, bf16[512,256]{1,0:T(8,128)(2,1)} %copy-done.15, ...), custom_call_target="tpu_custom_call" | custom-call | flops 2147483648 | bytes 4194304 | tf_op jit(solution)/shard_map/attention/pallas_call | solution.py:301
  113.9 5.1 %attention.5 = bf16[4,2,272,128]{3,2,1,0:T(8,128)(2,1)} custom-call(s32[4]{0:T(128)} %pad_add_fusion.place.refs_0_, s32[1]{0:T(128)} %get-tuple-element.42.refs_1_, bf16[4,128,256]{2,1,0:T(8,128)(2,1)} %bitcast.27, bf16[512,256]{1,0:T(8,128)(2,1)} %copy-done.9, f32[8,1,256]{2,1,0:T(1,128)} %get-tuple-element.28.refs_4_, ...), custom_call_target="tpu_custom_call" | custom-call | flops 536870912 | bytes 4194304 | tf_op jit(solution)/shard_map/attention/pallas_call | solution.py:301
  119.7 3.5 %all-to-all-start.1 = ((bf16[8,272,128]{2,1,0:T(8,128)(2,1)}), bf16[8,272,128]{2,1,0:T(8,128)(2,1)S(1)}, u32[]{:S(2)}, u32[]{:S(2)}) async-start(bf16[8,272,128]{2,1,0:T(8,128)(2,1)} %bitcast.22), calls=%async_computation.1 | async-start | bytes 1114112 | tf_op jit(solution)/shard_map/all_to_all | solution.py:479
  123.2 1.8 %final_states.1 = (bf16[128,128]{1,0:T(8,128)(2,1)}, bf16[128,128]{1,0:T(8,128)(2,1)}) custom-call(s32[4]{0:T(128)} %pad_add_fusion.place.refs_0_, f32[8,2,128]{2,1,0:T(2,128)} %copy-done.10, f32[8,2,128]{2,1,0:T(2,128)} %copy-done.12, f32[1,128]{1,0:T(1,128)} %bitcast.32, f32[256,128]{1,0:T(8,128)} %get-tuple-element.32.decays, ...), custom_call_target="tpu_custom_call" | custom-call | flops 1048576 | bytes 524288 | tf_op jit(solution)/shard_map/final_states/pallas_call | solution.py:175
  125.0 2.3 %collective-permute-start.10 = (bf16[128,128]{1,0:T(8,128)(2,1)}, bf16[128,128]{1,0:T(8,128)(2,1)S(1)}, u32[]{:S(2)}, u32[]{:S(2)}) collective-permute-start(bf16[128,128]{1,0:T(8,128)(2,1)} %get-tuple-element.36), channel_id=1, source_target_pairs={{0,1},{1,0},{2,3},{3,2},{4,5},{5,4},{6,7},{7,6},{8,9},{9,8},{10,11... | collective-permute-start | bytes 98312 | tf_op jit(solution)/shard_map/ppermute | solution.py:485
  127.3 2.0 %collective-permute-start = (f32[1]{0:T(128)}, f32[1]{0:T(128)}, u32[]{:S(2)}, u32[]{:S(2)}) collective-permute-start(f32[1]{0:T(128)} %param.30), channel_id=1, source_target_pairs={{0,1},{1,0},{2,3},{3,2},{4,5},{5,4},{6,7},{7,6},{8,9},{9,8},{10,11... | collective-permute-start | bytes 20 | tf_op jit(solution)/shard_map/ppermute | solution.py:459
  130.7 3.1 %all-to-all-done.1 = bf16[8,272,128]{2,1,0:T(8,128)(2,1)S(1)} async-done(((bf16[8,272,128]{2,1,0:T(8,128)(2,1)}), bf16[8,272,128]{2,1,0:T(8,128)(2,1)S(1)}, u32[]{:S(2)}, u32[]{:S(2)}) %all-to-all-start.1) | async-done | bytes 557088 | tf_op jit(solution)/shard_map/all_to_all | solution.py:479
  134.6 3.7 %finish.1 = bf16[128,2048]{1,0:T(8,128)(2,1)} custom-call(s32[4]{0:T(128)} %pad_add_fusion.place.refs_0_, f32[1]{0:T(128)S(6)} %copy.19.lam, f32[1]{0:T(128)} %collective-permute-done.lam_theirs, bf16[4,2,272,128]{3,2,1,0:T(8,128)(2,1)} %bitcast.23, f32[1,128]{1,0:T(1,128)} %bitcast.33, bf16[128,128]{1,0:T(8,128)(2,1)} %get-tuple-element.35.lru_mine, ...), custom_call_target="tpu_custom_call" | custom-call | flops 268435456 | bytes 3145728 | tf_op jit(solution)/shard_map/finish/pallas_call | solution.py:355
  138.4 12.9 %all_to_all.25 = bf16[4,32,2048]{2,1,0:T(8,128)(2,1)S(1)} all-to-all(bf16[4,32,2048]{2,1,0:T(8,128)(2,1)} %bitcast.24), channel_id=1, replica_groups=mesh['sp_0'=8,'sp_1'=8,'fs'=4,'tp'=2] {'fs'}, dimensions={0} | all-to-all | bytes 1048576 | tf_op jit(solution)/shard_map/all_to_all | solution.py:499
  (68 shorter events, 10.0 us)
Async XLA Ops:
  0.0 11.6 %copy-start = (bf16[2048,128]{1,0:T(8,128)(2,1)S(1)}, bf16[2048,128]{1,0:T(8,128)(2,1)}, u32[]{:S(2)}) copy-start(bf16[2048,128]{1,0:T(8,128)(2,1)} %param.21) | copy-start | bytes 1572868
  0.0 1.1 copy-start.7
  1.9 4.7 %copy-start.5 = (bf16[128,2048]{1,0:T(8,128)(2,1)S(1)}, bf16[128,2048]{1,0:T(8,128)(2,1)}, u32[]{:S(2)}) copy-start(bf16[128,2048]{1,0:T(8,128)(2,1)} %param.33) | copy-start | bytes 1572868
  2.0 10.8 %collective-permute-start.1 = (bf16[8,2048]{1,0:T(8,128)(2,1)S(1)}, bf16[8,2048]{1,0:T(8,128)(2,1)S(1)}, u32[]{:S(2)}, u32[]{:S(2)}) collective-permute-start(bf16[8,2048]{1,0:T(8,128)(2,1)S(1)} %slice.98), channel_id=1, source_target_pairs={{0,8},{8,16},{16,24},{24,32},{32,40},{40,48},{48,56},{56,64},{64,7... | collective-permute-start | bytes 98312 | tf_op jit(solution)/shard_map/ppermute | solution.py:31
  6.7 6.7 %copy-start.2 = (bf16[256,2048]{1,0:T(8,128)(2,1)}, bf16[256,2048]{1,0:T(8,128)(2,1)S(1)}, u32[]{:S(2)}) copy-start(bf16[256,2048]{1,0:T(8,128)(2,1)S(1)} %constant_dynamic-update-slice_fusion.w_mine) | copy-start | bytes 3145732
  6.7 5.1 %copy-start.6 = (bf16[2048,128]{1,0:T(8,128)(2,1)S(1)}, bf16[2048,128]{1,0:T(8,128)(2,1)}, u32[]{:S(2)}) copy-start(bf16[2048,128]{1,0:T(8,128)(2,1)} %param.20) | copy-start | bytes 1572868
  6.8 123.9 %collective-permute-start.11 = (bf16[256,2048]{1,0:T(8,128)(2,1)S(1)}, bf16[256,2048]{1,0:T(8,128)(2,1)S(1)}, u32[]{:S(2)}, u32[]{:S(2)}) collective-permute-start(bf16[256,2048]{1,0:T(8,128)(2,1)S(1)} %constant_dynamic-update-slice_fusion.w_mine), channel_id=1, source_target_pairs={{0,1},{1,0},{2,3},{3,2},{4,5},{5,4},{6,7},{7,6},{8,9},{9,8},{10,11... | collective-permute-start | bytes 3145736 | tf_op jit(solution)/shard_map/ppermute | solution.py:458
  13.5 23.9 %all-to-all-start = ((bf16[8,64,256]{2,1,0:T(8,128)(2,1)}), bf16[8,64,256]{2,1,0:T(8,128)(2,1)S(1)}, u32[]{:S(2)}, u32[]{:S(2)}) async-start(bf16[8,64,256]{2,1,0:T(8,128)(2,1)} %broadcast_in_dim.21), calls=%async_computation | async-start | bytes 524288 | tf_op jit(solution)/shard_map/all_to_all | solution.py:25
  33.1 10.5 %copy-start.1 = (bf16[160,2048]{1,0:T(8,128)(2,1)}, bf16[160,2048]{1,0:T(8,128)(2,1)S(1)}, u32[]{:S(2)}) copy-start(bf16[160,2048]{1,0:T(8,128)(2,1)S(1)} %all_gather.13.mine) | copy-start | bytes 1966084
  33.1 10.5 %collective-permute-start.2 = (bf16[160,2048]{1,0:T(8,128)(2,1)S(1)}, bf16[160,2048]{1,0:T(8,128)(2,1)}, u32[]{:S(2)}, u32[]{:S(2)}) collective-permute-start(bf16[160,2048]{1,0:T(8,128)(2,1)S(1)} %all_gather.13.mine), channel_id=1, source_target_pairs={{0,1},{1,0},{2,3},{3,2},{4,5},{5,4},{6,7},{7,6},{8,9},{9,8},{10,11... | collective-permute-start | bytes 1966088 | tf_op jit(solution)/shard_map/ppermute | solution.py:431
  36.2 0.7 copy-start.16
  37.4 10.4 %copy-start.8 = (bf16[8,64,256]{2,1,0:T(8,128)(2,1)}, bf16[8,64,256]{2,1,0:T(8,128)(2,1)S(1)}, u32[]{:S(2)}) copy-start(bf16[8,64,256]{2,1,0:T(8,128)(2,1)S(1)} %all-to-all-done) | copy-start | bytes 786436
  37.4 18.9 %collective-permute-start.3 = (bf16[512,256]{1,0:T(8,128)(2,1)S(1)}, bf16[512,256]{1,0:T(8,128)(2,1)}, u32[]{:S(2)}, u32[]{:S(2)}) collective-permute-start(bf16[512,256]{1,0:T(8,128)(2,1)S(1)} %bitcast.28), channel_id=1, source_target_pairs={{0,64},{64,128},{128,192},{192,256},{256,320},{320,384},{384,448},... | collective-permute-start | bytes 786440 | tf_op jit(solution)/shard_map/ppermute | solution.py:424
  38.7 33.4 %collective-permute-start.7 = (bf16[512,256]{1,0:T(8,128)(2,1)S(1)}, bf16[512,256]{1,0:T(8,128)(2,1)}, u32[]{:S(2)}, u32[]{:S(2)}) collective-permute-start(bf16[512,256]{1,0:T(8,128)(2,1)S(1)} %bitcast.29), channel_id=1, source_target_pairs={{128,64},{64,0},{0,448},{129,65},{65,1},{1,449},{130,66},{66,2},{2... | collective-permute-start | bytes 786440 | tf_op jit(solution)/shard_map/ppermute | solution.py:426
  47.8 0.7 copy-start.13
  49.1 28.2 %all-to-all-start.2 = ((f32[8,2,128]{2,1,0:T(2,128)}), f32[8,2,128]{2,1,0:T(2,128)S(1)}, u32[]{:S(2)}, u32[]{:S(2)}) async-start(f32[8,2,128]{2,1,0:T(2,128)} %broadcast_in_dim.23), calls=%async_computation.2 | async-start | bytes 16384 | tf_op jit(solution)/shard_map/all_to_all | solution.py:25
  56.3 21.0 %collective-permute-start.4 = (bf16[512,256]{1,0:T(8,128)(2,1)}, bf16[512,256]{1,0:T(8,128)(2,1)S(1)}, u32[]{:S(2)}, u32[]{:S(2)}) collective-permute-start(bf16[512,256]{1,0:T(8,128)(2,1)} %collective-permute-done.3.refs_4_), channel_id=1, source_target_pairs={{0,64},{64,128},{128,192},{192,256},{256,320},{320,384},{384,448},... | collective-permute-start | bytes 786440 | tf_op jit(solution)/shard_map/ppermute | solution.py:424
  72.1 10.3 %collective-permute-start.8 = (bf16[512,256]{1,0:T(8,128)(2,1)}, bf16[512,256]{1,0:T(8,128)(2,1)S(1)}, u32[]{:S(2)}, u32[]{:S(2)}) collective-permute-start(bf16[512,256]{1,0:T(8,128)(2,1)} %collective-permute-done.7.refs_5_), channel_id=1, source_target_pairs={{64,0},{0,448},{448,384},{65,1},{1,449},{449,385},{66,2},{2,450},{... | collective-permute-start | bytes 786440 | tf_op jit(solution)/shard_map/ppermute | solution.py:426
  77.3 9.1 %copy-start.10 = (f32[8,2,128]{2,1,0:T(2,128)}, f32[8,2,128]{2,1,0:T(2,128)S(1)}, u32[]{:S(2)}) copy-start(f32[8,2,128]{2,1,0:T(2,128)S(1)} %all-to-all-done.2.near) | copy-start | bytes 24580
  77.4 24.8 %copy-start.14 = (bf16[512,256]{1,0:T(8,128)(2,1)}, bf16[512,256]{1,0:T(8,128)(2,1)S(1)}, u32[]{:S(2)}) copy-start(bf16[512,256]{1,0:T(8,128)(2,1)S(1)} %collective-permute-done.4.refs_3_) | copy-start | bytes 786436
  77.4 14.7 %collective-permute-start.5 = (bf16[512,256]{1,0:T(8,128)(2,1)S(1)}, bf16[512,256]{1,0:T(8,128)(2,1)}, u32[]{:S(2)}, u32[]{:S(2)}) collective-permute-start(bf16[512,256]{1,0:T(8,128)(2,1)S(1)} %collective-permute-done.4.refs_3_), channel_id=1, source_target_pairs={{0,64},{64,128},{128,192},{192,256},{256,320},{320,384},{384,448},... | collective-permute-start | bytes 786440 | tf_op jit(solution)/shard_map/ppermute | solution.py:424
  82.4 19.7 %copy-start.15 = (bf16[512,256]{1,0:T(8,128)(2,1)}, bf16[512,256]{1,0:T(8,128)(2,1)S(1)}, u32[]{:S(2)}) copy-start(bf16[512,256]{1,0:T(8,128)(2,1)S(1)} %collective-permute-done.8.refs_4_) | copy-start | bytes 786436
  82.4 19.7 %collective-permute-start.9 = (bf16[512,256]{1,0:T(8,128)(2,1)S(1)}, bf16[512,256]{1,0:T(8,128)(2,1)}, u32[]{:S(2)}, u32[]{:S(2)}) collective-permute-start(bf16[512,256]{1,0:T(8,128)(2,1)S(1)} %collective-permute-done.8.refs_4_), channel_id=1, source_target_pairs={{0,448},{448,384},{384,320},{1,449},{449,385},{385,321},{2,450},{4... | collective-permute-start | bytes 786440 | tf_op jit(solution)/shard_map/ppermute | solution.py:426
  86.4 32.7 %all-to-all-start.3 = ((f32[8,2,128]{2,1,0:T(2,128)}), f32[8,2,128]{2,1,0:T(2,128)S(1)}, u32[]{:S(2)}, u32[]{:S(2)}) async-start(f32[8,2,128]{2,1,0:T(2,128)} %broadcast_in_dim.24), calls=%async_computation.3 | async-start | bytes 16384 | tf_op jit(solution)/shard_map/all_to_all | solution.py:25
  92.1 21.2 %collective-permute-start.6 = (bf16[512,256]{1,0:T(8,128)(2,1)}, bf16[512,256]{1,0:T(8,128)(2,1)S(1)}, u32[]{:S(2)}, u32[]{:S(2)}) collective-permute-start(bf16[512,256]{1,0:T(8,128)(2,1)} %collective-permute-done.5.refs_5_), channel_id=1, source_target_pairs={{0,64},{64,128},{128,192},{192,256},{256,320},{320,384},{384,448},... | collective-permute-start | bytes 786440 | tf_op jit(solution)/shard_map/ppermute | solution.py:424
  113.2 0.7 copy-start.9
  119.7 14.1 %all-to-all-start.1 = ((bf16[8,272,128]{2,1,0:T(8,128)(2,1)}), bf16[8,272,128]{2,1,0:T(8,128)(2,1)S(1)}, u32[]{:S(2)}, u32[]{:S(2)}) async-start(bf16[8,272,128]{2,1,0:T(8,128)(2,1)} %bitcast.22), calls=%async_computation.1 | async-start | bytes 1114112 | tf_op jit(solution)/shard_map/all_to_all | solution.py:479
  125.0 5.6 %collective-permute-start.10 = (bf16[128,128]{1,0:T(8,128)(2,1)}, bf16[128,128]{1,0:T(8,128)(2,1)S(1)}, u32[]{:S(2)}, u32[]{:S(2)}) collective-permute-start(bf16[128,128]{1,0:T(8,128)(2,1)} %get-tuple-element.36), channel_id=1, source_target_pairs={{0,1},{1,0},{2,3},{3,2},{4,5},{5,4},{6,7},{7,6},{8,9},{9,8},{10,11... | collective-permute-start | bytes 98312 | tf_op jit(solution)/shard_map/ppermute | solution.py:485
  127.3 3.3 %collective-permute-start = (f32[1]{0:T(128)}, f32[1]{0:T(128)}, u32[]{:S(2)}, u32[]{:S(2)}) collective-permute-start(f32[1]{0:T(128)} %param.30), channel_id=1, source_target_pairs={{0,1},{1,0},{2,3},{3,2},{4,5},{5,4},{6,7},{7,6},{8,9},{9,8},{10,11... | collective-permute-start | bytes 20 | tf_op jit(solution)/shard_map/ppermute | solution.py:459
  130.6 3.2 %copy-start.11 = (bf16[128,128]{1,0:T(8,128)(2,1)}, bf16[128,128]{1,0:T(8,128)(2,1)S(1)}, u32[]{:S(2)}) copy-start(bf16[128,128]{1,0:T(8,128)(2,1)S(1)} %collective-permute-done.10.lru_theirs) | copy-start | bytes 98308
  130.7 3.2 %copy-start.4 = (bf16[256,2048]{1,0:T(8,128)(2,1)}, bf16[256,2048]{1,0:T(8,128)(2,1)S(1)}, u32[]{:S(2)}) copy-start(bf16[256,2048]{1,0:T(8,128)(2,1)S(1)} %collective-permute-done.11.w_theirs) | copy-start | bytes 3145732
  133.8 0.8 copy-start.3
  (1 other events, 0.6 us)

commit v4 on v2

--- a/solution.py
+++ b/solution.py
@@ -29,12 +29,6 @@
     devices = lax.axis_size(axis)
     pairs = [(i, i + by) for i in range(devices) if 0 <= i + by < devices]
     return lax.ppermute(value, axis, pairs)
-
-
-def pair_combine(earlier, later):
-    decay_early, state_early = earlier
-    decay_late, state_late = later
-    return (decay_early * decay_late, decay_late * state_early + state_late)
 
 
 def vmem():
@@ -146,21 +140,24 @@
 
 
 def states_kernel(
-    place, near, far, start, decays, states, gates, mine, theirs, *, fs_count, member_rows
+    place, pieces, start, decays, states, gates, mine, theirs, *, y_count, fs_count, member_rows
 ):
-    z, y, core = (place[0], place[1], place[3])
-
-    def before(pieces, here):
-        decay, state = (jnp.ones_like(pieces[0, 0:1]), jnp.zeros_like(pieces[0, 1:2]))
-        for k in range(pieces.shape[0]):
-            passed = k < here
-            new_decay, new_state = pair_combine((decay, state), (pieces[k, 0:1], pieces[k, 1:2]))
-            decay = jnp.where(passed, new_decay, decay)
-            state = jnp.where(passed, new_state, state)
-        return decay, state
-
-    decay, state = pair_combine(before(far, z), before(near, y))
-    entering = decay * start[...] + state
+    here, core = (place[0] * y_count + place[1], place[3])
+
+    count = pieces.shape[0]
+    decay, state = (pieces[:, 0, :], pieces[:, 1, :])
+    row = lax.broadcasted_iota(jnp.int32, decay.shape, 0)
+    decay = jnp.where(row < here, decay, 1.0)
+    state = jnp.where(row < here, state, 0.0)
+    by = 1
+    while by < count:
+        inside = row >= by
+        decay_before = jnp.where(inside, pltpu.roll(decay, by, 0), 1.0)
+        state_before = jnp.where(inside, pltpu.roll(state, by, 0), 0.0)
+        state = decay * state_before + state
+        decay = decay * decay_before
+        by *= 2
+    entering = decay[count - 1 :] * start[...] + state[count - 1 :]
     out = ((states[...] + decays[...] * entering) * gates[...]).astype(jnp.bfloat16)
     for f in range(fs_count):
         at = 2 * f * member_rows
@@ -170,18 +167,20 @@
         theirs[f * member_rows : (f + 1) * member_rows] = jnp.where(core == 0, odd, even)
 
 
-def final_states(place, near, far, start, decays, states, gates, fs_count, member_rows):
+def final_states(place, pieces, start, decays, states, gates, y_count, fs_count, member_rows):
     half = jax.ShapeDtypeStruct((fs_count * member_rows, decays.shape[1]), jnp.bfloat16)
     return pl.pallas_call(
-        functools.partial(states_kernel, fs_count=fs_count, member_rows=member_rows),
+        functools.partial(
+            states_kernel, y_count=y_count, fs_count=fs_count, member_rows=member_rows
+        ),
         out_shape=(half, half),
-        in_specs=[smem()] + [vmem()] * 6,
+        in_specs=[smem()] + [vmem()] * 5,
         out_specs=(vmem(), vmem()),
         cost_estimate=pl.CostEstimate(
             flops=1 << 20, bytes_accessed=1 << 19, transcendentals=0
         ),
         name="final_states",
-    )(place, near, far, start, decays, states, gates)
+    )(place, pieces, start, decays, states, gates)
 
 
 def attention_kernel(
@@ -404,11 +403,7 @@
 
     group = lax.all_gather(query_t, "fs")
 
-    near = lax.all_gather(ends, "sp_1")
-    row = (near[0, 0], near[0, 1])
-    for k in range(1, y_count):
-        row = pair_combine(row, (near[k, 0], near[k, 1]))
-    far = from_everyone(jnp.stack(row), "sp_0")
+    everywhere = from_everyone(ends, SP)
 
     w_mine = jnp.concatenate([w_out_lru, w_out_attn], axis=0)
     w_theirs = lax.ppermute(w_mine, "tp", swap)
@@ -421,7 +416,7 @@
     packed = packed.reshape(fs_count, tp_count, lines, half_rows)
 
     lru_mine, lru_other = final_states(
-        place, near, far, init_state[None], decays, states, gates, fs_count, member_rows
+        place, everywhere, init_state[None], decays, states, gates, y_count, fs_count, member_rows
     )
     lru_theirs = lax.ppermute(lru_other, "tp", swap)
 

time: 154 us -> 137 us (0.89)
  blocking collectives: 76.6 us -> 42.9 us
  waiting for transfers between devices: 4.71 us -> 17.6 us
  starting transfers between devices: 32.6 us -> 36.5 us
    all_gather x1 -> x0, blocking collectives: 33.9 us -> none  [body(): near = lax.all_gather(ends, 'sp_1')]
    all_to_all x2, waiting for transfers between devices: 0.01 us -> 12.9 us  [from_everyone(): return lax.all_to_all(copies, axis, split_axis=0, concat_axis=0, tiled=True)]
    all_to_all x2, starting transfers between devices: 16.9 us -> 20.1 us  [from_everyone(): return lax.all_to_all(copies, axis, split_axis=0, concat_axis=0, tiled=True)]
  transfers between devices with their start and end apart: 8 -> 8, of which waited for: 3 -> 4; matrix products, arithmetic and copies ran while one was open for 2% -> 3% of each run, Pallas kernels for 17% -> 19%
where the time goes in v4:
time: 137 us; the launch traced here: 136 us
  blocking collectives  42.9 us (31%)
  starting transfers between devices  36.5 us (27%)
  Pallas kernels  29.3 us (21%)
  waiting for transfers between devices  17.6 us (13%)
  other arithmetic  4.03 us (3%)
  local copies, waits for them, and re-layouts  3.82 us (3%)
  matrix products  1.48 us (1%)
    all_to_all x2, starting transfers between devices, from_everyone(): return lax.all_to_all(copies, axis, split_axis=0, concat_axis=0, tiled=True)  20.1 us
    pallas_call x1, Pallas kernels, attention(): pl.pallas_call(functools.partial(attention_kernel, block_rows=block_rows,...  19.4 us
    all_gather x1, blocking collectives, body(): group = lax.all_gather(query_t, 'fs')  14.5 us
    all_gather x1, blocking collectives, body(): mine = lax.all_gather(sent, 'fs', axis=0, tiled=True)  13.5 us
    all_to_all x1, blocking collectives, body(): lax.all_to_all(partial, 'fs', split_axis=0, concat_axis=0, tiled=True)  12.9 us
    all_to_all x2, waiting for transfers between devices, from_everyone(): return lax.all_to_all(copies, axis, split_axis=0, concat_axis=0, tiled=True)  12.9 us
    all_to_all x1, starting transfers between devices, body(): lax.all_to_all(carried, ('fs', 'tp'), split_axis=0, concat_axis=0, tiled=...  4.27 us
    pallas_call x1, Pallas kernels, project(): pl.pallas_call(functools.partial(project_kernel, fs_count=fs_count, membe...  4.26 us
  transfers between devices with their start and end apart: 8, of which 4 were waited for; matrix products, arithmetic and copies ran while one was open for 3% of the time, Pallas kernels for 19%

profile of v4, /device:TPU:448, one launch (start us, length us, event | category | flops | bytes accessed | tf_op | source)
XLA Modules:
  0.0 136.5 jit_solution(4819345780133358012)
XLA Ops:
  0.0 1.1 fusion
  1.1 1.0 fusion.2
  2.1 3.5 %collective-permute-start.1 = (bf16[8,2048]{1,0:T(8,128)(2,1)S(1)}, bf16[8,2048]{1,0:T(8,128)(2,1)S(1)}, u32[]{:S(2)}, u32[]{:S(2)}) collective-permute-start(bf16[8,2048]{1,0:T(8,128)(2,1)S(1)} %slice.4), channel_id=1, source_target_pairs={{0,8},{8,16},{16,24},{24,32},{32,40},{40,48},{48,56},{56,64},{64,7... | collective-permute-start | bytes 98312 | tf_op jit(solution)/shard_map/ppermute | solution.py:31
  5.6 2.0 %all_gather.12 = bf16[64,2048]{1,0:T(8,128)(2,1)S(1)} all-gather(bf16[32,2048]{1,0:T(8,128)(2,1)S(1)} %fusion.2), channel_id=1, replica_groups=mesh['sp_0'=8,'sp_1'=8,'fs'=4,'tp'=2] {'tp'}, dimensions={0}, use_global_device_ids=true | all-gather | bytes 393216 | tf_op jit(solution)/shard_map/all_gather | solution.py:371
  7.6 0.2 convolution_convert_fusion
  7.9 1.3 convolution_convert_fusion.1
  9.1 0.9 collective-permute-done.1
  10.1 1.6 %broadcast_in_dim.18 = bf16[64,64,256]{2,1,0:T(8,128)(2,1)} broadcast(bf16[64,256]{1,0:T(8,128)(2,1)S(1)} %pad_maximum_fusion.1), dimensions={1,2} | broadcast | bytes 2129920 | tf_op jit(solution)/shard_map/broadcast_in_dim | solution.py:24
  11.6 10.0 %all-to-all-start = ((bf16[64,64,256]{2,1,0:T(8,128)(2,1)}), bf16[64,64,256]{2,1,0:T(8,128)(2,1)}, u32[]{:S(2)}, u32[]{:S(2)}) async-start(bf16[64,64,256]{2,1,0:T(8,128)(2,1)} %broadcast_in_dim.18), calls=%async_computation | async-start | bytes 4194304 | tf_op jit(solution)/shard_map/all_to_all | solution.py:25
  21.7 0.0 copy-start.6
  21.7 0.0 copy-start.9
  21.7 13.5 %all_gather.13.mine = bf16[160,2048]{1,0:T(8,128)(2,1)S(1)} all-gather(bf16[40,2048]{1,0:T(8,128)(2,1)S(1)} %pad_maximum_fusion), channel_id=1, replica_groups=mesh['sp_0'=8,'sp_1'=8,'fs'=4,'tp'=2] {'fs'}, dimensions={0}, use_global_device_ids=true | all-gather | bytes 819200 | tf_op jit(solution)/shard_map/all_gather | solution.py:384
  35.2 1.9 %collective-permute-start.2 = (bf16[160,2048]{1,0:T(8,128)(2,1)S(1)}, bf16[160,2048]{1,0:T(8,128)(2,1)}, u32[]{:S(2)}, u32[]{:S(2)}) collective-permute-start(bf16[160,2048]{1,0:T(8,128)(2,1)S(1)} %all_gather.13.mine), channel_id=1, source_target_pairs={{0,1},{1,0},{2,3},{3,2},{4,5},{5,4},{6,7},{7,6},{8,9},{9,8},{10,11... | collective-permute-start | bytes 1966088 | tf_op jit(solution)/shard_map/ppermute | solution.py:386
  37.3 2.4 %collective-permute-start.4 = (bf16[256,2048]{1,0:T(8,128)(2,1)S(1)}, bf16[256,2048]{1,0:T(8,128)(2,1)S(1)}, u32[]{:S(2)}, u32[]{:S(2)}) collective-permute-start(bf16[256,2048]{1,0:T(8,128)(2,1)S(1)} %constant_dynamic-update-slice_fusion.w_mine), channel_id=1, source_target_pairs={{0,1},{1,0},{2,3},{3,2},{4,5},{5,4},{6,7},{7,6},{8,9},{9,8},{10,11... | collective-permute-start | bytes 3145736 | tf_op jit(solution)/shard_map/ppermute | solution.py:409
  39.7 0.5 fusion.4.rate
  40.2 0.7 pad_add_fusion.place
  40.9 4.3 %project.1 = (bf16[128,256]{1,0:T(8,128)(2,1)}, f32[256,128]{1,0:T(8,128)}, f32[256,128]{1,0:T(8,128)}, f32[256,128]{1,0:T(8,128)}, f32[2,128]{1,0:T(2,128)}) custom-call(s32[4]{0:T(128)} %pad_add_fusion.place, bf16[160,2048]{1,0:T(8,128)(2,1)} %copy-done.1, bf16[160,2048]{1,0:T(8,128)(2,1)} %collective-permute-done.2.theirs, bf16[2048,128]{1,0:T(8,128)(2,1)} %w_query.1, ...), custom_call_target="tpu_custom_call" | custom-call | flops 402653184 | bytes 4194304 | tf_op jit(solution)/shard_map/project/pallas_call | solution.py:122
  45.1 14.5 %all-gather = bf16[512,256]{1,0:T(8,128)(2,1)} all-gather(bf16[128,256]{1,0:T(8,128)(2,1)} %get-tuple-element.17), channel_id=2, replica_groups=mesh['sp_0'=8,'sp_1'=8,'fs'=4,'tp'=2] {'fs'}, dimensions={0}, use_global_device_ids=true | all-gather | bytes 327680 | tf_op jit(solution)/shard_map/all_gather | solution.py:404
  59.7 12.9 %all-to-all-done = bf16[64,64,256]{2,1,0:T(8,128)(2,1)} async-done(((bf16[64,64,256]{2,1,0:T(8,128)(2,1)}), bf16[64,64,256]{2,1,0:T(8,128)(2,1)}, u32[]{:S(2)}, u32[]{:S(2)}) %all-to-all-start) | async-done | bytes 2097184 | tf_op jit(solution)/shard_map/all_to_all | solution.py:25
  72.5 1.3 broadcast_in_dim.20
  73.8 10.0 %all-to-all-start.2 = ((f32[64,2,128]{2,1,0:T(2,128)}), f32[64,2,128]{2,1,0:T(2,128)S(1)}, u32[]{:S(2)}, u32[]{:S(2)}) async-start(f32[64,2,128]{2,1,0:T(2,128)} %broadcast_in_dim.20), calls=%async_computation.2 | async-start | bytes 131072 | tf_op jit(solution)/shard_map/all_to_all | solution.py:25
  83.9 19.4 %attention.1 = bf16[4,2,272,128]{3,2,1,0:T(8,128)(2,1)} custom-call(s32[4]{0:T(128)} %pad_add_fusion.place, bf16[4,128,256]{2,1,0:T(8,128)(2,1)} %bitcast.20, bf16[8,512,256]{2,1,0:T(8,128)(2,1)} %bitcast.6.kv), custom_call_target="tpu_custom_call" | custom-call | flops 4294967296 | bytes 4194304 | tf_op jit(solution)/shard_map/attention/pallas_call | solution.py:269
  103.3 4.3 %all-to-all-start.1 = ((bf16[8,272,128]{2,1,0:T(8,128)(2,1)}), bf16[8,272,128]{2,1,0:T(8,128)(2,1)S(1)}, u32[]{:S(2)}, u32[]{:S(2)}) async-start(bf16[8,272,128]{2,1,0:T(8,128)(2,1)} %bitcast.19), calls=%async_computation.1 | async-start | bytes 1114112 | tf_op jit(solution)/shard_map/all_to_all | solution.py:415
  107.5 1.8 %final_states.1 = (bf16[128,128]{1,0:T(8,128)(2,1)}, bf16[128,128]{1,0:T(8,128)(2,1)}) custom-call(s32[4]{0:T(128)} %pad_add_fusion.place, f32[64,2,128]{2,1,0:T(2,128)} %copy-done.7, f32[1,128]{1,0:T(1,128)} %bitcast.21, f32[256,128]{1,0:T(8,128)} %get-tuple-element.20.decays, f32[256,128]{1,0:T(8,128)} %get-tuple-element.21.states, ...), custom_call_target="tpu_custom_call" | custom-call | flops 1048576 | bytes 524288 | tf_op jit(solution)/shard_map/final_states/pallas_call | solution.py:172
  109.4 2.4 %collective-permute-start.3 = (bf16[128,128]{1,0:T(8,128)(2,1)}, bf16[128,128]{1,0:T(8,128)(2,1)S(1)}, u32[]{:S(2)}, u32[]{:S(2)}) collective-permute-start(bf16[128,128]{1,0:T(8,128)(2,1)} %get-tuple-element.24), channel_id=1, source_target_pairs={{0,1},{1,0},{2,3},{3,2},{4,5},{5,4},{6,7},{7,6},{8,9},{9,8},{10,11... | collective-permute-start | bytes 98312 | tf_op jit(solution)/shard_map/ppermute | solution.py:421
  111.8 1.9 %collective-permute-start = (f32[1]{0:T(128)}, f32[1]{0:T(128)}, u32[]{:S(2)}, u32[]{:S(2)}) collective-permute-start(f32[1]{0:T(128)} %param.30), channel_id=1, source_target_pairs={{0,1},{1,0},{2,3},{3,2},{4,5},{5,4},{6,7},{7,6},{8,9},{9,8},{10,11... | collective-permute-start | bytes 20 | tf_op jit(solution)/shard_map/ppermute | solution.py:410
  114.3 0.7 collective-permute-done.lam_theirs
  115.1 3.1 %all-to-all-done.1 = bf16[8,272,128]{2,1,0:T(8,128)(2,1)S(1)} async-done(((bf16[8,272,128]{2,1,0:T(8,128)(2,1)}), bf16[8,272,128]{2,1,0:T(8,128)(2,1)S(1)}, u32[]{:S(2)}, u32[]{:S(2)}) %all-to-all-start.1) | async-done | bytes 557088 | tf_op jit(solution)/shard_map/all_to_all | solution.py:415
  118.2 0.8 copy-done.3
  119.0 3.8 %finish.1 = bf16[128,2048]{1,0:T(8,128)(2,1)} custom-call(s32[4]{0:T(128)} %pad_add_fusion.place, f32[1]{0:T(128)S(6)} %copy.19.lam, f32[1]{0:T(128)} %collective-permute-done.lam_theirs, bf16[4,2,272,128]{3,2,1,0:T(8,128)(2,1)} %bitcast.17, f32[1,128]{1,0:T(1,128)} %bitcast.22, bf16[128,128]{1,0:T(8,128)(2,1)} %get-tuple-element.23.lru_mine, ...), custom_call_target="tpu_custom_call" | custom-call | flops 268435456 | bytes 3145728 | tf_op jit(solution)/shard_map/finish/pallas_call | solution.py:322
  122.8 12.9 %all_to_all.20 = bf16[4,32,2048]{2,1,0:T(8,128)(2,1)S(1)} all-to-all(bf16[4,32,2048]{2,1,0:T(8,128)(2,1)} %bitcast.18), channel_id=1, replica_groups=mesh['sp_0'=8,'sp_1'=8,'fs'=4,'tp'=2] {'fs'}, dimensions={0} | all-to-all | bytes 1048576 | tf_op jit(solution)/shard_map/all_to_all | solution.py:435
  135.7 0.7 reduce_sum.22
  (27 shorter events, 0.2 us)
Async XLA Ops:
  0.0 7.6 %copy-start = (bf16[2048,128]{1,0:T(8,128)(2,1)S(1)}, bf16[2048,128]{1,0:T(8,128)(2,1)}, u32[]{:S(2)}) copy-start(bf16[2048,128]{1,0:T(8,128)(2,1)} %param.21) | copy-start | bytes 1572868
  2.1 7.9 %collective-permute-start.1 = (bf16[8,2048]{1,0:T(8,128)(2,1)S(1)}, bf16[8,2048]{1,0:T(8,128)(2,1)S(1)}, u32[]{:S(2)}, u32[]{:S(2)}) collective-permute-start(bf16[8,2048]{1,0:T(8,128)(2,1)S(1)} %slice.4), channel_id=1, source_target_pairs={{0,8},{8,16},{16,24},{24,32},{32,40},{40,48},{48,56},{56,64},{64,7... | collective-permute-start | bytes 98312 | tf_op jit(solution)/shard_map/ppermute | solution.py:31
  11.6 25.5 %copy-start.5 = (bf16[128,2048]{1,0:T(8,128)(2,1)S(1)}, bf16[128,2048]{1,0:T(8,128)(2,1)}, u32[]{:S(2)}) copy-start(bf16[128,2048]{1,0:T(8,128)(2,1)} %param.32) | copy-start | bytes 1572868
  11.6 60.9 %all-to-all-start = ((bf16[64,64,256]{2,1,0:T(8,128)(2,1)}), bf16[64,64,256]{2,1,0:T(8,128)(2,1)}, u32[]{:S(2)}, u32[]{:S(2)}) async-start(bf16[64,64,256]{2,1,0:T(8,128)(2,1)} %broadcast_in_dim.18), calls=%async_computation | async-start | bytes 4194304 | tf_op jit(solution)/shard_map/all_to_all | solution.py:25
  21.7 15.6 %copy-start.6 = (bf16[128,2048]{1,0:T(8,128)(2,1)S(1)}, bf16[128,2048]{1,0:T(8,128)(2,1)}, u32[]{:S(2)}) copy-start(bf16[128,2048]{1,0:T(8,128)(2,1)} %param.33) | copy-start | bytes 1572868
  21.7 18.0 %copy-start.9 = (f32[128]{0:T(128)S(1)}, f32[128]{0:T(128)}, u32[]{:S(2)}) copy-start(f32[128]{0:T(128)} %param.27) | copy-start | bytes 1540
  35.2 5.6 %copy-start.1 = (bf16[160,2048]{1,0:T(8,128)(2,1)}, bf16[160,2048]{1,0:T(8,128)(2,1)S(1)}, u32[]{:S(2)}) copy-start(bf16[160,2048]{1,0:T(8,128)(2,1)S(1)} %all_gather.13.mine) | copy-start | bytes 1966084
  35.2 5.6 %collective-permute-start.2 = (bf16[160,2048]{1,0:T(8,128)(2,1)S(1)}, bf16[160,2048]{1,0:T(8,128)(2,1)}, u32[]{:S(2)}, u32[]{:S(2)}) collective-permute-start(bf16[160,2048]{1,0:T(8,128)(2,1)S(1)} %all_gather.13.mine), channel_id=1, source_target_pairs={{0,1},{1,0},{2,3},{3,2},{4,5},{5,4},{6,7},{7,6},{8,9},{9,8},{10,11... | collective-permute-start | bytes 1966088 | tf_op jit(solution)/shard_map/ppermute | solution.py:386
  37.3 66.0 %copy-start.2 = (bf16[256,2048]{1,0:T(8,128)(2,1)}, bf16[256,2048]{1,0:T(8,128)(2,1)S(1)}, u32[]{:S(2)}) copy-start(bf16[256,2048]{1,0:T(8,128)(2,1)S(1)} %constant_dynamic-update-slice_fusion.w_mine) | copy-start | bytes 3145732
  37.3 77.8 %collective-permute-start.4 = (bf16[256,2048]{1,0:T(8,128)(2,1)S(1)}, bf16[256,2048]{1,0:T(8,128)(2,1)S(1)}, u32[]{:S(2)}, u32[]{:S(2)}) collective-permute-start(bf16[256,2048]{1,0:T(8,128)(2,1)S(1)} %constant_dynamic-update-slice_fusion.w_mine), channel_id=1, source_target_pairs={{0,1},{1,0},{2,3},{3,2},{4,5},{5,4},{6,7},{7,6},{8,9},{9,8},{10,11... | collective-permute-start | bytes 3145736 | tf_op jit(solution)/shard_map/ppermute | solution.py:409
  73.8 29.4 %all-to-all-start.2 = ((f32[64,2,128]{2,1,0:T(2,128)}), f32[64,2,128]{2,1,0:T(2,128)S(1)}, u32[]{:S(2)}, u32[]{:S(2)}) async-start(f32[64,2,128]{2,1,0:T(2,128)} %broadcast_in_dim.20), calls=%async_computation.2 | async-start | bytes 131072 | tf_op jit(solution)/shard_map/all_to_all | solution.py:25
  103.3 4.3 %copy-start.7 = (f32[64,2,128]{2,1,0:T(2,128)}, f32[64,2,128]{2,1,0:T(2,128)S(1)}, u32[]{:S(2)}) copy-start(f32[64,2,128]{2,1,0:T(2,128)S(1)} %all-to-all-done.2.pieces) | copy-start | bytes 196612
  103.3 14.9 %all-to-all-start.1 = ((bf16[8,272,128]{2,1,0:T(8,128)(2,1)}), bf16[8,272,128]{2,1,0:T(8,128)(2,1)S(1)}, u32[]{:S(2)}, u32[]{:S(2)}) async-start(bf16[8,272,128]{2,1,0:T(8,128)(2,1)} %bitcast.19), calls=%async_computation.1 | async-start | bytes 1114112 | tf_op jit(solution)/shard_map/all_to_all | solution.py:415
  109.4 5.7 %collective-permute-start.3 = (bf16[128,128]{1,0:T(8,128)(2,1)}, bf16[128,128]{1,0:T(8,128)(2,1)S(1)}, u32[]{:S(2)}, u32[]{:S(2)}) collective-permute-start(bf16[128,128]{1,0:T(8,128)(2,1)} %get-tuple-element.24), channel_id=1, source_target_pairs={{0,1},{1,0},{2,3},{3,2},{4,5},{5,4},{6,7},{7,6},{8,9},{9,8},{10,11... | collective-permute-start | bytes 98312 | tf_op jit(solution)/shard_map/ppermute | solution.py:421
  111.8 3.3 %collective-permute-start = (f32[1]{0:T(128)}, f32[1]{0:T(128)}, u32[]{:S(2)}, u32[]{:S(2)}) collective-permute-start(f32[1]{0:T(128)} %param.30), channel_id=1, source_target_pairs={{0,1},{1,0},{2,3},{3,2},{4,5},{5,4},{6,7},{7,6},{8,9},{9,8},{10,11... | collective-permute-start | bytes 20 | tf_op jit(solution)/shard_map/ppermute | solution.py:410
  115.1 3.1 %copy-start.8 = (bf16[128,128]{1,0:T(8,128)(2,1)}, bf16[128,128]{1,0:T(8,128)(2,1)S(1)}, u32[]{:S(2)}) copy-start(bf16[128,128]{1,0:T(8,128)(2,1)S(1)} %collective-permute-done.3.lru_theirs) | copy-start | bytes 98308
  115.1 3.1 %copy-start.4 = (bf16[256,2048]{1,0:T(8,128)(2,1)}, bf16[256,2048]{1,0:T(8,128)(2,1)S(1)}, u32[]{:S(2)}) copy-start(bf16[256,2048]{1,0:T(8,128)(2,1)S(1)} %collective-permute-done.4.w_theirs) | copy-start | bytes 3145732
  118.2 0.8 copy-start.3

commit v5 on v2

--- a/solution.py
+++ b/solution.py
@@ -185,15 +185,18 @@
 
 
 def attention_kernel(
-    place, group, kv, packed, query, peak, total, values, value_t, *, block_rows, part_rows
+    place, *refs, block_rows, part_rows
 ):
-    heads, size, rows = group.shape
+    group = refs[:-7]
+    kv, packed, query, peak, total, values, value_t = refs[-7:]
+    heads = len(group)
+    size, rows = group[0].shape
     chunk_keys = kv.shape[1]
     z, y, member = (place[0], place[1], place[2])
     scale = (size // 2) ** (-0.5) * log2_e
     line = lax.broadcasted_iota(jnp.int32, (size, rows), 0)
     for h in range(heads):
-        whole = group[h]
+        whole = group[h][...]
         zero = jnp.zeros_like(whole)
         query[2 * h] = jnp.where(line < size // 2, whole, zero)
         query[2 * h + 1] = jnp.where(line < size // 2, zero, whole)
@@ -257,20 +260,21 @@
             tail = jnp.where(line == 2 * m, coarse, tail)
             tail = jnp.where(line == 2 * m + 1, level - coarse, tail)
             for t in range(2):
-                packed[h, t, m * size : (m + 1) * size, :] = shares[:, t * half : (t + 1) * half]
+                packed[member ^ h, t, m * size : (m + 1) * size, :] = shares[:, t * half : (t + 1) * half]
         rounded = tail.astype(jnp.bfloat16)
         for t in range(2):
-            packed[h, t, 2 * size : 2 * size + 16, :] = rounded[:, t * half : (t + 1) * half]
+            packed[member ^ h, t, 2 * size : 2 * size + 16, :] = rounded[:, t * half : (t + 1) * half]
 
 
 def attention(place, group, kv, block_rows, part_rows):
-    heads, size, rows = group.shape
+    heads = len(group)
+    size, rows = group[0].shape
     z_count, chunk_keys, _ = kv.shape
     keys = chunk_keys * z_count
     return pl.pallas_call(
         functools.partial(attention_kernel, block_rows=block_rows, part_rows=part_rows),
         out_shape=jax.ShapeDtypeStruct((heads, 2, 2 * size + 16, rows // 2), jnp.bfloat16),
-        in_specs=[smem(), vmem(), vmem()],
+        in_specs=[smem()] + [vmem()] * (heads + 1),
         out_specs=vmem(),
         scratch_shapes=[
             pltpu.VMEM((2 * heads, size, rows), jnp.bfloat16),
@@ -285,7 +289,7 @@
             transcendentals=2 * heads * rows * keys,
         ),
         name="attention",
-    )(place, group, kv)
+    )(place, *group, kv)
 
 
 def finish_kernel(place, lam, lam_theirs, parts, gain, lru_mine, lru_theirs, w_mine, w_theirs, out):
@@ -358,7 +362,7 @@
     share_rows = member_rows * tp_count
     member = lax.axis_index("fs")
     core = lax.axis_index("tp")
-    z_count, z = (lax.axis_size("sp_0"), lax.axis_index("sp_0"))
+    z = lax.axis_index("sp_0")
     y_count, y = (lax.axis_size("sp_1"), lax.axis_index("sp_1"))
 
     floats = tokens.astype(jnp.float32)
@@ -378,8 +382,8 @@
         axis=1,
     )
     kv_here, normed, before_rows = lax.optimization_barrier((kv_here, normed, before_rows))
-    everyone = from_everyone(kv_here, SP)
-    everyone = everyone.reshape(z_count, y_count * share_rows, kv_here.shape[1])
+    chunk = from_everyone(kv_here, "sp_1").reshape(y_count * share_rows, kv_here.shape[1])
+    everyone = from_everyone(chunk, "sp_0")
 
     sent = jnp.concatenate([normed, before_rows], axis=0)
     mine = lax.all_gather(sent, "fs", axis=0, tiled=True)
@@ -402,7 +406,9 @@
         member_rows,
     )
 
-    group = lax.all_gather(query_t, "fs")
+    group = [query_t]
+    for by in range(1, fs_count):
+        group.append(lax.ppermute(query_t, "fs", [(i, i ^ by) for i in range(fs_count)]))
 
     near = lax.all_gather(ends, "sp_1")
     row = (near[0, 0], near[0, 1])

time: 154 us -> 144 us (0.935)
  blocking collectives: 76.6 us -> 60.4 us
  starting transfers between devices: 32.6 us -> 37.3 us
    all_gather x1, blocking collectives: 33.9 us -> 14 us  [body(): near = lax.all_gather(ends, 'sp_1')]
    all_to_all x0 -> x1, blocking collectives: none -> 17.3 us  [from_everyone(): return lax.all_to_all(copies, axis, split_axis=0, concat_axis=0, tiled=True)]
    all_gather x1 -> x0, blocking collectives: 14.2 us -> none  [body(): group = lax.all_gather(query_t, 'fs')]
    ppermute x0 -> x3, starting transfers between devices: none -> 10.4 us  [body(): lax.ppermute(query_t, 'fs', [(i, i ^ by) for i in range(fs_count)])]
    all_to_all x2, starting transfers between devices: 16.9 us -> 11.1 us  [from_everyone(): return lax.all_to_all(copies, axis, split_axis=0, concat_axis=0, tiled=True)]
  transfers between devices with their start and end apart: 8 -> 11, of which waited for: 3 -> 3; matrix products, arithmetic and copies ran while one was open for 2% -> 2% of each run, Pallas kernels for 17% -> 18%
where the time goes in v5:
time: 144 us; the launch traced here: 143 us
  blocking collectives  60.4 us (42%)
  starting transfers between devices  37.3 us (26%)
  Pallas kernels  29.3 us (20%)
  waiting for transfers between devices  4.82 us (3%)
  local copies, waits for them, and re-layouts  4.25 us (3%)
  other arithmetic  4.01 us (3%)
  matrix products  1.48 us (1%)
    pallas_call x1, Pallas kernels, attention(): pl.pallas_call(functools.partial(attention_kernel, block_rows=block_rows,...  19.4 us
    all_to_all x1, blocking collectives, from_everyone(): return lax.all_to_all(copies, axis, split_axis=0, concat_axis=0, tiled=True)  17.3 us
    all_gather x1, blocking collectives, body(): mine = lax.all_gather(sent, 'fs', axis=0, tiled=True)  14.3 us
    all_gather x1, blocking collectives, body(): near = lax.all_gather(ends, 'sp_1')  14 us
    all_to_all x1, blocking collectives, body(): lax.all_to_all(partial, 'fs', split_axis=0, concat_axis=0, tiled=True)  12.9 us
    all_to_all x2, starting transfers between devices, from_everyone(): return lax.all_to_all(copies, axis, split_axis=0, concat_axis=0, tiled=True)  11.1 us
    ppermute x3, starting transfers between devices, body(): lax.ppermute(query_t, 'fs', [(i, i ^ by) for i in range(fs_count)])  10.4 us
    pallas_call x1, Pallas kernels, project(): pl.pallas_call(functools.partial(project_kernel, fs_count=fs_count, membe...  4.27 us
  transfers between devices with their start and end apart: 11, of which 3 were waited for; matrix products, arithmetic and copies ran while one was open for 2% of the time, Pallas kernels for 18%

profile of v5, /device:TPU:448, one launch (start us, length us, event | category | flops | bytes accessed | tf_op | source)
XLA Modules:
  0.0 142.5 jit_solution(16410146296233657790)
XLA Ops:
  0.0 1.1 fusion
  1.1 1.0 fusion.2
  2.1 3.5 %collective-permute-start.1 = (bf16[8,2048]{1,0:T(8,128)(2,1)S(1)}, bf16[8,2048]{1,0:T(8,128)(2,1)S(1)}, u32[]{:S(2)}, u32[]{:S(2)}) collective-permute-start(bf16[8,2048]{1,0:T(8,128)(2,1)S(1)} %slice.68), channel_id=1, source_target_pairs={{0,8},{8,16},{16,24},{24,32},{32,40},{40,48},{48,56},{56,64},{64,7... | collective-permute-start | bytes 98312 | tf_op jit(solution)/shard_map/ppermute | solution.py:31
  5.6 2.0 %all_gather.12 = bf16[64,2048]{1,0:T(8,128)(2,1)S(1)} all-gather(bf16[32,2048]{1,0:T(8,128)(2,1)S(1)} %fusion.2), channel_id=1, replica_groups=mesh['sp_0'=8,'sp_1'=8,'fs'=4,'tp'=2] {'tp'}, dimensions={0}, use_global_device_ids=true | all-gather | bytes 393216 | tf_op jit(solution)/shard_map/all_gather | solution.py:376
  7.9 1.3 convolution_convert_fusion.1
  9.1 0.9 collective-permute-done.1
  10.1 17.3 %all_to_all.25 = bf16[8,64,256]{2,1,0:T(8,128)(2,1)S(1)} all-to-all(bf16[8,64,256]{2,1,0:T(8,128)(2,1)S(1)} %broadcast_in_dim.21), channel_id=1, replica_groups=mesh['sp_0'=8,'sp_1'=8,'fs'=4,'tp'=2] {'sp_1'}, dimensions={0} | all-to-all | bytes 524288 | tf_op jit(solution)/shard_map/all_to_all | solution.py:25
  27.4 1.4 %broadcast_in_dim.22 = bf16[8,512,256]{2,1,0:T(8,128)(2,1)} broadcast(bf16[512,256]{1,0:T(8,128)(2,1)S(1)} %bitcast.23), dimensions={1,2} | broadcast | bytes 2359296 | tf_op jit(solution)/shard_map/broadcast_in_dim | solution.py:24
  28.8 4.6 %all-to-all-start.1 = ((bf16[8,512,256]{2,1,0:T(8,128)(2,1)}), bf16[8,512,256]{2,1,0:T(8,128)(2,1)}, u32[]{:S(2)}, u32[]{:S(2)}) async-start(bf16[8,512,256]{2,1,0:T(8,128)(2,1)} %broadcast_in_dim.22), calls=%async_computation.1 | async-start | bytes 4194304 | tf_op jit(solution)/shard_map/all_to_all | solution.py:25
  33.5 14.3 %all_gather.13.mine = bf16[160,2048]{1,0:T(8,128)(2,1)S(1)} all-gather(bf16[40,2048]{1,0:T(8,128)(2,1)S(1)} %pad_maximum_fusion), channel_id=1, replica_groups=mesh['sp_0'=8,'sp_1'=8,'fs'=4,'tp'=2] {'fs'}, dimensions={0}, use_global_device_ids=true | all-gather | bytes 819200 | tf_op jit(solution)/shard_map/all_gather | solution.py:389
  47.8 1.9 %collective-permute-start.2 = (bf16[160,2048]{1,0:T(8,128)(2,1)S(1)}, bf16[160,2048]{1,0:T(8,128)(2,1)}, u32[]{:S(2)}, u32[]{:S(2)}) collective-permute-start(bf16[160,2048]{1,0:T(8,128)(2,1)S(1)} %all_gather.13.mine), channel_id=1, source_target_pairs={{0,1},{1,0},{2,3},{3,2},{4,5},{5,4},{6,7},{7,6},{8,9},{9,8},{10,11... | collective-permute-start | bytes 1966088 | tf_op jit(solution)/shard_map/ppermute | solution.py:391
  49.8 2.4 %collective-permute-start.7 = (bf16[256,2048]{1,0:T(8,128)(2,1)S(1)}, bf16[256,2048]{1,0:T(8,128)(2,1)S(1)}, u32[]{:S(2)}, u32[]{:S(2)}) collective-permute-start(bf16[256,2048]{1,0:T(8,128)(2,1)S(1)} %constant_dynamic-update-slice_fusion.w_mine), channel_id=1, source_target_pairs={{0,1},{1,0},{2,3},{3,2},{4,5},{5,4},{6,7},{7,6},{8,9},{9,8},{10,11... | collective-permute-start | bytes 3145736 | tf_op jit(solution)/shard_map/ppermute | solution.py:420
  52.2 0.6 pad_add_fusion.place
  53.3 4.3 %project.1 = (bf16[128,256]{1,0:T(8,128)(2,1)}, f32[256,128]{1,0:T(8,128)}, f32[256,128]{1,0:T(8,128)}, f32[256,128]{1,0:T(8,128)}, f32[2,128]{1,0:T(2,128)}) custom-call(s32[4]{0:T(128)} %pad_add_fusion.place, bf16[160,2048]{1,0:T(8,128)(2,1)} %copy-done.1, bf16[160,2048]{1,0:T(8,128)(2,1)} %collective-permute-done.2.theirs, bf16[2048,128]{1,0:T(8,128)(2,1)} %w_query.1, ...), custom_call_target="tpu_custom_call" | custom-call | flops 402653184 | bytes 4194304 | tf_op jit(solution)/shard_map/project/pallas_call | solution.py:128
  57.6 14.0 %all-gather.1.near = f32[8,2,128]{2,1,0:T(2,128)S(1)} all-gather(f32[1,2,128]{2,1,0:T(2,128)} %bitcast.25), channel_id=2, replica_groups=mesh['sp_0'=8,'sp_1'=8,'fs'=4,'tp'=2] {'sp_1'}, dimensions={0}, use_global_device_ids=true | all-gather | bytes 9216 | tf_op jit(solution)/shard_map/all_gather | solution.py:413
  71.6 2.3 %collective-permute-start.3 = (bf16[128,256]{1,0:T(8,128)(2,1)}, bf16[128,256]{1,0:T(8,128)(2,1)S(1)}, u32[]{:S(2)}, u32[]{:S(2)}) collective-permute-start(bf16[128,256]{1,0:T(8,128)(2,1)} %get-tuple-element.17.refs_0_), channel_id=1, source_target_pairs={{0,2},{2,0},{4,6},{6,4},{1,3},{3,1},{5,7},{7,5},{8,10},{10,8},{12,... | collective-permute-start | bytes 196616 | tf_op jit(solution)/shard_map/ppermute | solution.py:411
  73.9 4.6 %collective-permute-start.4 = (bf16[128,256]{1,0:T(8,128)(2,1)}, bf16[128,256]{1,0:T(8,128)(2,1)S(1)}, u32[]{:S(2)}, u32[]{:S(2)}) collective-permute-start(bf16[128,256]{1,0:T(8,128)(2,1)} %get-tuple-element.17.refs_0_), channel_id=1, source_target_pairs={{0,4},{2,6},{4,0},{6,2},{1,5},{3,7},{5,1},{7,3},{8,12},{10,14},{12... | collective-permute-start | bytes 196616 | tf_op jit(solution)/shard_map/ppermute | solution.py:411
  78.5 3.5 %collective-permute-start.5 = (bf16[128,256]{1,0:T(8,128)(2,1)}, bf16[128,256]{1,0:T(8,128)(2,1)S(1)}, u32[]{:S(2)}, u32[]{:S(2)}) collective-permute-start(bf16[128,256]{1,0:T(8,128)(2,1)} %get-tuple-element.17.refs_0_), channel_id=1, source_target_pairs={{0,6},{2,4},{4,2},{6,0},{1,7},{3,5},{5,3},{7,1},{8,14},{10,12},{12... | collective-permute-start | bytes 196616 | tf_op jit(solution)/shard_map/ppermute | solution.py:411
  82.1 0.6 broadcast_in_dim.24
  82.7 6.4 %all-to-all-start.3 = ((f32[8,2,128]{2,1,0:T(2,128)}), f32[8,2,128]{2,1,0:T(2,128)S(1)}, u32[]{:S(2)}, u32[]{:S(2)}) async-start(f32[8,2,128]{2,1,0:T(2,128)} %broadcast_in_dim.24), calls=%async_computation.3 | async-start | bytes 16384 | tf_op jit(solution)/shard_map/all_to_all | solution.py:25
  89.8 0.6 copy-done.12
  90.4 19.4 %attention.1 = bf16[4,2,272,128]{3,2,1,0:T(8,128)(2,1)} custom-call(s32[4]{0:T(128)} %pad_add_fusion.place, bf16[128,256]{1,0:T(8,128)(2,1)} %get-tuple-element.17.refs_0_, bf16[128,256]{1,0:T(8,128)(2,1)} %copy-done.10, bf16[128,256]{1,0:T(8,128)(2,1)} %copy-done.11, bf16[128,256]{1,0:T(8,128)(2,1)} %copy-done.12, bf16[8,512,256]{2,1,0:T(8,128)(2,1)} %all-to-all-done.1.refs_4_), custom_call_target="tpu_custom_call" | custom-call | flops 4294967296 | bytes 4194304 | tf_op jit(solution)/shard_map/attention/pallas_call | solution.py:274
  109.8 3.7 %all-to-all-start.2 = ((bf16[8,272,128]{2,1,0:T(8,128)(2,1)}), bf16[8,272,128]{2,1,0:T(8,128)(2,1)S(1)}, u32[]{:S(2)}, u32[]{:S(2)}) async-start(bf16[8,272,128]{2,1,0:T(8,128)(2,1)} %bitcast.24), calls=%async_computation.2 | async-start | bytes 1114112 | tf_op jit(solution)/shard_map/all_to_all | solution.py:426
  113.6 1.8 %final_states.1 = (bf16[128,128]{1,0:T(8,128)(2,1)}, bf16[128,128]{1,0:T(8,128)(2,1)}) custom-call(s32[4]{0:T(128)} %pad_add_fusion.place, f32[8,2,128]{2,1,0:T(2,128)} %copy-done.7, f32[8,2,128]{2,1,0:T(2,128)} %copy-done.9, f32[1,128]{1,0:T(1,128)} %bitcast.26, f32[256,128]{1,0:T(8,128)} %get-tuple-element.20.decays, f32[256,128]{1,0:T(8,128)} %get-tuple-element.21.states, ...), custom_call_target="tpu_custom_call" | custom-call | flops 1048576 | bytes 524288 | tf_op jit(solution)/shard_map/final_states/pallas_call | solution.py:175
  115.3 2.4 %collective-permute-start.6 = (bf16[128,128]{1,0:T(8,128)(2,1)}, bf16[128,128]{1,0:T(8,128)(2,1)S(1)}, u32[]{:S(2)}, u32[]{:S(2)}) collective-permute-start(bf16[128,128]{1,0:T(8,128)(2,1)} %get-tuple-element.24), channel_id=1, source_target_pairs={{0,1},{1,0},{2,3},{3,2},{4,5},{5,4},{6,7},{7,6},{8,9},{9,8},{10,11... | collective-permute-start | bytes 98312 | tf_op jit(solution)/shard_map/ppermute | solution.py:432
  117.7 1.9 %collective-permute-start = (f32[1]{0:T(128)}, f32[1]{0:T(128)}, u32[]{:S(2)}, u32[]{:S(2)}) collective-permute-start(f32[1]{0:T(128)} %param.30), channel_id=1, source_target_pairs={{0,1},{1,0},{2,3},{3,2},{4,5},{5,4},{6,7},{7,6},{8,9},{9,8},{10,11... | collective-permute-start | bytes 20 | tf_op jit(solution)/shard_map/ppermute | solution.py:421
  120.3 0.6 collective-permute-done.lam_theirs
  120.9 3.3 %all-to-all-done.2 = bf16[8,272,128]{2,1,0:T(8,128)(2,1)S(1)} async-done(((bf16[8,272,128]{2,1,0:T(8,128)(2,1)}), bf16[8,272,128]{2,1,0:T(8,128)(2,1)S(1)}, u32[]{:S(2)}, u32[]{:S(2)}) %all-to-all-start.2) | async-done | bytes 557088 | tf_op jit(solution)/shard_map/all_to_all | solution.py:426
  124.2 0.8 copy-done.3
  125.0 3.8 %finish.1 = bf16[128,2048]{1,0:T(8,128)(2,1)} custom-call(s32[4]{0:T(128)} %pad_add_fusion.place, f32[1]{0:T(128)S(6)} %copy.19.lam, f32[1]{0:T(128)} %collective-permute-done.lam_theirs, bf16[4,2,272,128]{3,2,1,0:T(8,128)(2,1)} %bitcast.21, f32[1,128]{1,0:T(1,128)} %bitcast.27, bf16[128,128]{1,0:T(8,128)(2,1)} %get-tuple-element.23.lru_mine, ...), custom_call_target="tpu_custom_call" | custom-call | flops 268435456 | bytes 3145728 | tf_op jit(solution)/shard_map/finish/pallas_call | solution.py:327
  128.9 12.9 %all_to_all.26 = bf16[4,32,2048]{2,1,0:T(8,128)(2,1)S(1)} all-to-all(bf16[4,32,2048]{2,1,0:T(8,128)(2,1)} %bitcast.22), channel_id=1, replica_groups=mesh['sp_0'=8,'sp_1'=8,'fs'=4,'tp'=2] {'fs'}, dimensions={0} | all-to-all | bytes 1048576 | tf_op jit(solution)/shard_map/all_to_all | solution.py:446
  141.8 0.7 reduce_sum.22
  (46 shorter events, 1.6 us)
Async XLA Ops:
  0.0 7.6 %copy-start = (bf16[2048,128]{1,0:T(8,128)(2,1)S(1)}, bf16[2048,128]{1,0:T(8,128)(2,1)}, u32[]{:S(2)}) copy-start(bf16[2048,128]{1,0:T(8,128)(2,1)} %param.21) | copy-start | bytes 1572868
  2.1 7.9 %collective-permute-start.1 = (bf16[8,2048]{1,0:T(8,128)(2,1)S(1)}, bf16[8,2048]{1,0:T(8,128)(2,1)S(1)}, u32[]{:S(2)}, u32[]{:S(2)}) collective-permute-start(bf16[8,2048]{1,0:T(8,128)(2,1)S(1)} %slice.68), channel_id=1, source_target_pairs={{0,8},{8,16},{16,24},{24,32},{32,40},{40,48},{48,56},{56,64},{64,7... | collective-permute-start | bytes 98312 | tf_op jit(solution)/shard_map/ppermute | solution.py:31
  28.8 20.9 %copy-start.5 = (bf16[128,2048]{1,0:T(8,128)(2,1)S(1)}, bf16[128,2048]{1,0:T(8,128)(2,1)}, u32[]{:S(2)}) copy-start(bf16[128,2048]{1,0:T(8,128)(2,1)} %param.32) | copy-start | bytes 1572868
  28.8 53.3 %all-to-all-start.1 = ((bf16[8,512,256]{2,1,0:T(8,128)(2,1)}), bf16[8,512,256]{2,1,0:T(8,128)(2,1)}, u32[]{:S(2)}, u32[]{:S(2)}) async-start(bf16[8,512,256]{2,1,0:T(8,128)(2,1)} %broadcast_in_dim.22), calls=%async_computation.1 | async-start | bytes 4194304 | tf_op jit(solution)/shard_map/all_to_all | solution.py:25
  33.4 16.3 %copy-start.6 = (bf16[128,2048]{1,0:T(8,128)(2,1)S(1)}, bf16[128,2048]{1,0:T(8,128)(2,1)}, u32[]{:S(2)}) copy-start(bf16[128,2048]{1,0:T(8,128)(2,1)} %param.33) | copy-start | bytes 1572868
  33.5 19.4 %copy-start.13 = (f32[128]{0:T(128)S(1)}, f32[128]{0:T(128)}, u32[]{:S(2)}) copy-start(f32[128]{0:T(128)} %param.27) | copy-start | bytes 1540
  47.8 5.6 %copy-start.1 = (bf16[160,2048]{1,0:T(8,128)(2,1)}, bf16[160,2048]{1,0:T(8,128)(2,1)S(1)}, u32[]{:S(2)}) copy-start(bf16[160,2048]{1,0:T(8,128)(2,1)S(1)} %all_gather.13.mine) | copy-start | bytes 1966084
  47.8 5.6 %collective-permute-start.2 = (bf16[160,2048]{1,0:T(8,128)(2,1)S(1)}, bf16[160,2048]{1,0:T(8,128)(2,1)}, u32[]{:S(2)}, u32[]{:S(2)}) collective-permute-start(bf16[160,2048]{1,0:T(8,128)(2,1)S(1)} %all_gather.13.mine), channel_id=1, source_target_pairs={{0,1},{1,0},{2,3},{3,2},{4,5},{5,4},{6,7},{7,6},{8,9},{9,8},{10,11... | collective-permute-start | bytes 1966088 | tf_op jit(solution)/shard_map/ppermute | solution.py:391
  49.8 60.0 %copy-start.2 = (bf16[256,2048]{1,0:T(8,128)(2,1)}, bf16[256,2048]{1,0:T(8,128)(2,1)S(1)}, u32[]{:S(2)}) copy-start(bf16[256,2048]{1,0:T(8,128)(2,1)S(1)} %constant_dynamic-update-slice_fusion.w_mine) | copy-start | bytes 3145732
  49.8 71.1 %collective-permute-start.7 = (bf16[256,2048]{1,0:T(8,128)(2,1)S(1)}, bf16[256,2048]{1,0:T(8,128)(2,1)S(1)}, u32[]{:S(2)}, u32[]{:S(2)}) collective-permute-start(bf16[256,2048]{1,0:T(8,128)(2,1)S(1)} %constant_dynamic-update-slice_fusion.w_mine), channel_id=1, source_target_pairs={{0,1},{1,0},{2,3},{3,2},{4,5},{5,4},{6,7},{7,6},{8,9},{9,8},{10,11... | collective-permute-start | bytes 3145736 | tf_op jit(solution)/shard_map/ppermute | solution.py:420
  71.6 38.3 %copy-start.7 = (f32[8,2,128]{2,1,0:T(2,128)}, f32[8,2,128]{2,1,0:T(2,128)S(1)}, u32[]{:S(2)}) copy-start(f32[8,2,128]{2,1,0:T(2,128)S(1)} %all-gather.1.near) | copy-start | bytes 24580
  71.6 17.5 %collective-permute-start.3 = (bf16[128,256]{1,0:T(8,128)(2,1)}, bf16[128,256]{1,0:T(8,128)(2,1)S(1)}, u32[]{:S(2)}, u32[]{:S(2)}) collective-permute-start(bf16[128,256]{1,0:T(8,128)(2,1)} %get-tuple-element.17.refs_0_), channel_id=1, source_target_pairs={{0,2},{2,0},{4,6},{6,4},{1,3},{3,1},{5,7},{7,5},{8,10},{10,8},{12,... | collective-permute-start | bytes 196616 | tf_op jit(solution)/shard_map/ppermute | solution.py:411
  73.9 15.2 %collective-permute-start.4 = (bf16[128,256]{1,0:T(8,128)(2,1)}, bf16[128,256]{1,0:T(8,128)(2,1)S(1)}, u32[]{:S(2)}, u32[]{:S(2)}) collective-permute-start(bf16[128,256]{1,0:T(8,128)(2,1)} %get-tuple-element.17.refs_0_), channel_id=1, source_target_pairs={{0,4},{2,6},{4,0},{6,2},{1,5},{3,7},{5,1},{7,3},{8,12},{10,14},{12... | collective-permute-start | bytes 196616 | tf_op jit(solution)/shard_map/ppermute | solution.py:411
  78.5 10.6 %collective-permute-start.5 = (bf16[128,256]{1,0:T(8,128)(2,1)}, bf16[128,256]{1,0:T(8,128)(2,1)S(1)}, u32[]{:S(2)}, u32[]{:S(2)}) collective-permute-start(bf16[128,256]{1,0:T(8,128)(2,1)} %get-tuple-element.17.refs_0_), channel_id=1, source_target_pairs={{0,6},{2,4},{4,2},{6,0},{1,7},{3,5},{5,3},{7,1},{8,14},{10,12},{12... | collective-permute-start | bytes 196616 | tf_op jit(solution)/shard_map/ppermute | solution.py:411
  82.7 27.2 %all-to-all-start.3 = ((f32[8,2,128]{2,1,0:T(2,128)}), f32[8,2,128]{2,1,0:T(2,128)S(1)}, u32[]{:S(2)}, u32[]{:S(2)}) async-start(f32[8,2,128]{2,1,0:T(2,128)} %broadcast_in_dim.24), calls=%async_computation.3 | async-start | bytes 16384 | tf_op jit(solution)/shard_map/all_to_all | solution.py:25
  89.1 0.6 copy-start.10
  89.1 0.6 copy-start.11
  89.8 0.6 copy-start.12
  109.8 3.7 %copy-start.9 = (f32[8,2,128]{2,1,0:T(2,128)}, f32[8,2,128]{2,1,0:T(2,128)S(1)}, u32[]{:S(2)}) copy-start(f32[8,2,128]{2,1,0:T(2,128)S(1)} %all-to-all-done.3.far) | copy-start | bytes 24580
  109.8 14.4 %all-to-all-start.2 = ((bf16[8,272,128]{2,1,0:T(8,128)(2,1)}), bf16[8,272,128]{2,1,0:T(8,128)(2,1)S(1)}, u32[]{:S(2)}, u32[]{:S(2)}) async-start(bf16[8,272,128]{2,1,0:T(8,128)(2,1)} %bitcast.24), calls=%async_computation.2 | async-start | bytes 1114112 | tf_op jit(solution)/shard_map/all_to_all | solution.py:426
  115.3 5.6 %collective-permute-start.6 = (bf16[128,128]{1,0:T(8,128)(2,1)}, bf16[128,128]{1,0:T(8,128)(2,1)S(1)}, u32[]{:S(2)}, u32[]{:S(2)}) collective-permute-start(bf16[128,128]{1,0:T(8,128)(2,1)} %get-tuple-element.24), channel_id=1, source_target_pairs={{0,1},{1,0},{2,3},{3,2},{4,5},{5,4},{6,7},{7,6},{8,9},{9,8},{10,11... | collective-permute-start | bytes 98312 | tf_op jit(solution)/shard_map/ppermute | solution.py:432
  117.7 3.2 %collective-permute-start = (f32[1]{0:T(128)}, f32[1]{0:T(128)}, u32[]{:S(2)}, u32[]{:S(2)}) collective-permute-start(f32[1]{0:T(128)} %param.30), channel_id=1, source_target_pairs={{0,1},{1,0},{2,3},{3,2},{4,5},{5,4},{6,7},{7,6},{8,9},{9,8},{10,11... | collective-permute-start | bytes 20 | tf_op jit(solution)/shard_map/ppermute | solution.py:421
  120.9 3.3 %copy-start.8 = (bf16[128,128]{1,0:T(8,128)(2,1)}, bf16[128,128]{1,0:T(8,128)(2,1)S(1)}, u32[]{:S(2)}) copy-start(bf16[128,128]{1,0:T(8,128)(2,1)S(1)} %collective-permute-done.6.lru_theirs) | copy-start | bytes 98308
  120.9 3.3 %copy-start.4 = (bf16[256,2048]{1,0:T(8,128)(2,1)}, bf16[256,2048]{1,0:T(8,128)(2,1)S(1)}, u32[]{:S(2)}) copy-start(bf16[256,2048]{1,0:T(8,128)(2,1)S(1)} %collective-permute-done.7.w_theirs) | copy-start | bytes 3145732
  124.2 0.8 copy-start.3

commit v6 on v4

--- a/solution.py
+++ b/solution.py
@@ -35,8 +35,31 @@
     return pl.BlockSpec(memory_space=pltpu.VMEM)
 
 
+def anywhere():
+    return pl.BlockSpec(memory_space=pl.ANY)
+
+
 def smem():
     return pl.BlockSpec(memory_space=pltpu.SMEM)
+
+
+def norm_kernel(tokens, gain, out):
+    floats = tokens[...].astype(jnp.float32)
+    level = lax.rsqrt(jnp.mean(floats * floats, axis=1, keepdims=True) + input_eps)
+    out[...] = (floats * level * gain[...]).astype(jnp.bfloat16)
+
+
+def normalized(tokens, gain):
+    return pl.pallas_call(
+        norm_kernel,
+        out_shape=jax.ShapeDtypeStruct(tokens.shape, jnp.bfloat16),
+        in_specs=[vmem(), vmem()],
+        out_specs=vmem(),
+        cost_estimate=pl.CostEstimate(
+            flops=4 * tokens.size, bytes_accessed=1 << 18, transcendentals=0
+        ),
+        name="normalized",
+    )(tokens, gain)
 
 
 def one_minus_exp(x):
@@ -69,7 +92,8 @@
 
     query = project(w_query)
     query = jnp.concatenate([piece(query, t, f) for t in range(2) for f in range(fs_count)], axis=0)
-    query_t[...] = query.astype(jnp.bfloat16).T
+    score_scale = (query.shape[1] // 2) ** (-0.5) * log2_e
+    query_t[...] = (query * score_scale).astype(jnp.bfloat16).T
 
     gate = in_order(project(w_gate).astype(jnp.bfloat16)).astype(jnp.float32)
     gates[...] = jax.nn.gelu(gate)
@@ -184,12 +208,23 @@
 
 
 def attention_kernel(
-    place, group, kv, packed, query, peak, total, values, value_t, *, block_rows, part_rows
+    place, group, kv_far, packed, query, peak, values, value_t, kv, arrivals,
+    *, block_rows, part_rows,
 ):
     heads, size, rows = group.shape
     chunk_keys = kv.shape[1]
     z, y, member = (place[0], place[1], place[2])
-    scale = (size // 2) ** (-0.5) * log2_e
+
+    def arrival(at):
+        return pltpu.make_async_copy(kv_far.at[at], kv.at[at], arrivals.at[at])
+
+    arrival(z).start()
+
+    def begin(at, _):
+        arrival(at).start()
+        return 0
+
+    lax.fori_loop(0, z, begin, 0)
     line = lax.broadcasted_iota(jnp.int32, (size, rows), 0)
     for h in range(heads):
         whole = group[h]
@@ -197,7 +232,7 @@
         query[2 * h] = jnp.where(line < size // 2, whole, zero)
         query[2 * h + 1] = jnp.where(line < size // 2, zero, whole)
     peak[...] = jnp.full(peak.shape, far_below, jnp.float32)
-    total[...] = jnp.zeros(total.shape, jnp.float32)
+    value_t[size:, :] = jnp.ones((16, chunk_keys), jnp.bfloat16)
     values[...] = jnp.zeros(values.shape, jnp.float32)
 
     def visible_keys():
@@ -209,13 +244,14 @@
         return key_pos <= inside + y * block_rows
 
     def one_chunk(at, masked):
+        arrival(at).wait()
         both = kv[at]
         keys = both[:, :size]
-        value_t[...] = both[:, size:].T
+        value_t[:size, :] = both[:, size:].T
         visible = visible_keys() if masked else None
 
         def scores_of(i):
-            found = jnp.dot(keys, query[i], preferred_element_type=jnp.float32) * scale
+            found = jnp.dot(keys, query[i], preferred_element_type=jnp.float32)
             return jnp.where(visible, found, far_below) if masked else found
 
         scores = scores_of(0)
@@ -228,7 +264,6 @@
                 expos = jnp.where(visible, expos, 0.0)
             fade = jnp.exp2(old - now)
             peak[i] = now
-            total[i] = total[i] * fade + jnp.sum(expos, axis=0, keepdims=True)
             values[i] = values[i] * fade + jnp.dot(
                 value_t[...], expos.astype(jnp.bfloat16), preferred_element_type=jnp.float32
             )
@@ -247,10 +282,10 @@
     for h in range(heads):
         tail = jnp.zeros((16, rows), jnp.float32)
         for m in range(2):
-            amount = total[2 * h + m]
+            amount = values[2 * h + m, size : size + 1, :]
             some = amount > 0.0
             safe = jnp.where(some, amount, 1.0)
-            shares = (values[2 * h + m] * jnp.where(some, 1.0 / safe, 0.0)).astype(jnp.bfloat16)
+            shares = (values[2 * h + m, :size, :] * jnp.where(some, 1.0 / safe, 0.0)).astype(jnp.bfloat16)
             level = jnp.where(some, peak[2 * h + m] + jnp.log2(safe), far_below)
             coarse = level.astype(jnp.bfloat16).astype(jnp.float32)
             tail = jnp.where(line == 2 * m, coarse, tail)
@@ -269,14 +304,15 @@
     return pl.pallas_call(
         functools.partial(attention_kernel, block_rows=block_rows, part_rows=part_rows),
         out_shape=jax.ShapeDtypeStruct((heads, 2, 2 * size + 16, rows // 2), jnp.bfloat16),
-        in_specs=[smem(), vmem(), vmem()],
+        in_specs=[smem(), vmem(), anywhere()],
         out_specs=vmem(),
         scratch_shapes=[
             pltpu.VMEM((2 * heads, size, rows), jnp.bfloat16),
             pltpu.VMEM((2 * heads, 1, rows), jnp.float32),
-            pltpu.VMEM((2 * heads, 1, rows), jnp.float32),
-            pltpu.VMEM((2 * heads, size, rows), jnp.float32),
-            pltpu.VMEM((size, chunk_keys), jnp.bfloat16),
+            pltpu.VMEM((2 * heads, size + 16, rows), jnp.float32),
+            pltpu.VMEM((size + 16, chunk_keys), jnp.bfloat16),
+            pltpu.VMEM(kv.shape, kv.dtype),
+            pltpu.SemaphoreType.DMA((z_count,)),
         ],
         cost_estimate=pl.CostEstimate(
             flops=4 * 2 * heads * rows * keys * size,
@@ -287,7 +323,17 @@
     )(place, group, kv)
 
 
-def finish_kernel(place, lam, lam_theirs, parts, gain, lru_mine, lru_theirs, w_mine, w_theirs, out):
+def finish_kernel(
+    place, lam, lam_theirs, parts, gain, lru_mine, lru_theirs, w_mine_far, w_theirs_far, *refs,
+):
+    outs = refs[:-4]
+    w_mine, w_theirs, whole, arrivals = refs[-4:]
+    copies = [
+        pltpu.make_async_copy(w_mine_far, w_mine, arrivals.at[0]),
+        pltpu.make_async_copy(w_theirs_far, w_theirs, arrivals.at[1]),
+    ]
+    for copy in copies:
+        copy.start()
     count, _, lines, _ = parts.shape
     size = (lines - 16) // 2
     core = place[3]
@@ -312,18 +358,28 @@
 
     mine = jnp.concatenate([lru_mine[...], head_output(core, lam[0])], axis=1)
     theirs = jnp.concatenate([lru_theirs[...], head_output(1 - core, lam_theirs[0])], axis=1)
+    for copy in copies:
+        copy.wait()
     result = jnp.dot(mine, w_mine[...], preferred_element_type=jnp.float32)
     result = result + jnp.dot(theirs, w_theirs[...], preferred_element_type=jnp.float32)
-    out[...] = result.astype(jnp.bfloat16)
-
-
-def finish(place, lam, lam_theirs, parts, gain, lru_mine, lru_theirs, w_mine, w_theirs):
+    whole[...] = result.astype(jnp.bfloat16).reshape(whole.shape)
+    for by, out in enumerate(outs):
+        out[...] = whole[place[2] ^ by]
+
+
+def finish(place, lam, lam_theirs, parts, gain, lru_mine, lru_theirs, w_mine, w_theirs, slots):
     rows, wide = (lru_mine.shape[0], w_mine.shape[1])
     return pl.pallas_call(
         finish_kernel,
-        out_shape=jax.ShapeDtypeStruct((rows, wide), jnp.bfloat16),
-        in_specs=[smem()] * 3 + [vmem()] * 6,
-        out_specs=vmem(),
+        out_shape=(jax.ShapeDtypeStruct((rows // slots, wide), jnp.bfloat16),) * slots,
+        in_specs=[smem()] * 3 + [vmem()] * 4 + [anywhere()] * 2,
+        out_specs=(vmem(),) * slots,
+        scratch_shapes=[
+            pltpu.VMEM(w_mine.shape, w_mine.dtype),
+            pltpu.VMEM(w_theirs.shape, w_theirs.dtype),
+            pltpu.VMEM((slots, rows // slots, wide), jnp.bfloat16),
+            pltpu.SemaphoreType.DMA((2,)),
+        ],
         cost_estimate=pl.CostEstimate(
             flops=2 * rows * wide * 512, bytes_accessed=3 << 20, transcendentals=rows * 16
         ),
@@ -350,7 +406,7 @@
     w_out_lru,
     w_out_attn,
 ):
-    member_rows, wide = tokens.shape
+    member_rows, _ = tokens.shape
     fs_count = lax.axis_size("fs")
     tp_count = lax.axis_size("tp")
     row_count = member_rows * fs_count * tp_count
@@ -360,10 +416,7 @@
     z_count, z = (lax.axis_size("sp_0"), lax.axis_index("sp_0"))
     y_count, y = (lax.axis_size("sp_1"), lax.axis_index("sp_1"))
 
-    floats = tokens.astype(jnp.float32)
-    normed = (
-        floats * lax.rsqrt(jnp.mean(floats * floats, axis=1, keepdims=True) + input_eps) * norm_gain
-    ).astype(jnp.bfloat16)
+    normed = normalized(tokens, norm_gain[None])
 
     margin = 8
     before_rows = passed_along(normed[member_rows - margin :], SP, 1)
@@ -376,7 +429,7 @@
         ],
         axis=1,
     )
-    kv_here, normed, before_rows = lax.optimization_barrier((kv_here, normed, before_rows))
+    kv_here, normed = lax.optimization_barrier((kv_here, normed))
     everyone = from_everyone(kv_here, SP)
     everyone = everyone.reshape(z_count, y_count * share_rows, kv_here.shape[1])
 
@@ -430,10 +483,13 @@
         lru_theirs,
         w_mine,
         w_theirs,
+        fs_count,
     )
-    partial = partial.reshape(fs_count, member_rows, wide)
-    arrived = lax.all_to_all(partial, "fs", split_axis=0, concat_axis=0, tiled=True)
-    return arrived.astype(jnp.float32).sum(axis=0).astype(jnp.bfloat16)
+    mixed = partial[0].astype(jnp.float32)
+    for by in (2, 1, 3):
+        pairs = [(i, i ^ by) for i in range(fs_count)]
+        mixed = mixed + lax.ppermute(partial[by], "fs", pairs).astype(jnp.float32)
+    return mixed.astype(jnp.bfloat16)
 
 
 def solution(mesh):

time: 137 us -> 170 us (1.24)
  waiting for transfers between devices: 17.6 us -> 54.4 us
  blocking collectives: 42.9 us -> 29.6 us
  starting transfers between devices: 36.5 us -> 46 us
    ppermute x1, waiting for transfers between devices: 0.92 us -> 46.3 us  [passed_along(): return lax.ppermute(value, axis, pairs)]
    all_to_all x1 -> x0, blocking collectives: 12.9 us -> none  [body(): lax.all_to_all(partial, 'fs', split_axis=0, concat_axis=0, tiled=True)]
    all_to_all x2, waiting for transfers between devices: 12.9 us -> 0.01 us  [from_everyone(): return lax.all_to_all(copies, axis, split_axis=0, concat_axis=0, tiled=True)]
    ppermute x0 -> x3, starting transfers between devices: none -> 9.82 us  [body(): mixed = mixed + lax.ppermute(partial[by], 'fs', pairs).astype(jnp.float32)]
    ppermute x0 -> x3, waiting for transfers between devices: none -> 4.28 us  [body(): mixed = mixed + lax.ppermute(partial[by], 'fs', pairs).astype(jnp.float32)]
    pallas_call x1 -> x2, Pallas kernels: 3.82 us -> 6.39 us  [the longest x1 4.65 us: finish(): pl.pallas_call(finish_kernel, out_shape=(jax.ShapeDtypeStruct((rows // sl...]
    pallas_call x1, Pallas kernels: 19.4 us -> 17.4 us  [attention(): pl.pallas_call(functools.partial(attention_kernel, block_rows=block_rows,...]
    reduce_sum x2 -> x0, other arithmetic: 1.83 us -> none  [the longest x1 1.09 us: body(): jnp.mean(floats * floats, axis=1, keepdims=True) + input_eps]
  transfers between devices with their start and end apart: 8 -> 11, of which waited for: 4 -> 5; matrix products, arithmetic and copies ran while one was open for 3% -> 2% of each run, Pallas kernels for 19% -> 14%
where the time goes in v6:
time: 170 us; the launch traced here: 169 us
  waiting for transfers between devices  54.4 us (32%)
  starting transfers between devices  46 us (27%)
  Pallas kernels  29.9 us (18%)
  blocking collectives  29.6 us (17%)
  local copies, waits for them, and re-layouts  3.8 us (2%)
  other arithmetic  2.8 us (2%)
    ppermute x1, waiting for transfers between devices, passed_along(): return lax.ppermute(value, axis, pairs)  46.3 us
    all_to_all x2, starting transfers between devices, from_everyone(): return lax.all_to_all(copies, axis, split_axis=0, concat_axis=0, tiled=True)  20.5 us
    pallas_call x1, Pallas kernels, attention(): pl.pallas_call(functools.partial(attention_kernel, block_rows=block_rows,...  17.4 us
    all_gather x1, blocking collectives, body(): mine = lax.all_gather(sent, 'fs', axis=0, tiled=True)  14.2 us
    all_gather x1, blocking collectives, body(): group = lax.all_gather(query_t, 'fs')  13.2 us
    ppermute x3, starting transfers between devices, body(): mixed = mixed + lax.ppermute(partial[by], 'fs', pairs).astype(jnp.float32)  9.82 us
    pallas_call x1, Pallas kernels, finish(): pl.pallas_call(finish_kernel, out_shape=(jax.ShapeDtypeStruct((rows // sl...  4.65 us
    ppermute x3, waiting for transfers between devices, body(): mixed = mixed + lax.ppermute(partial[by], 'fs', pairs).astype(jnp.float32)  4.28 us
  transfers between devices with their start and end apart: 11, of which 5 were waited for; matrix products, arithmetic and copies ran while one was open for 2% of the time, Pallas kernels for 14%

profile of v6, /device:TPU:448, one launch (start us, length us, event | category | flops | bytes accessed | tf_op | source)
XLA Modules:
  0.0 168.9 jit_solution(6525532895629963004)
XLA Ops:
  0.0 1.7 %normalized.1 = bf16[32,2048]{1,0:T(8,128)(2,1)} custom-call(bf16[32,2048]{1,0:T(8,128)(2,1)} %tokens.1, f32[1,2048]{1,0:T(1,128)} %bitcast.20), custom_call_target="tpu_custom_call" | custom-call | flops 262144 | bytes 262144 | tf_op jit(solution)/shard_map/normalized/pallas_call | solution.py:53
  1.7 2.2 %all_gather.12 = bf16[64,2048]{1,0:T(8,128)(2,1)S(1)} all-gather(bf16[32,2048]{1,0:T(8,128)(2,1)} %normalized.1), channel_id=1, replica_groups=mesh['sp_0'=8,'sp_1'=8,'fs'=4,'tp'=2] {'tp'}, dimensions={0}, use_global_device_ids=true | all-gather | bytes 393216 | tf_op jit(solution)/shard_map/all_gather | solution.py:424
  3.9 0.2 convolution_convert_fusion
  4.2 1.3 convolution_convert_fusion.1
  5.5 1.5 broadcast_in_dim.20
  7.0 10.9 %all-to-all-start = ((bf16[64,64,256]{2,1,0:T(8,128)(2,1)}), bf16[64,64,256]{2,1,0:T(8,128)(2,1)}, u32[]{:S(2)}, u32[]{:S(2)}) async-start(bf16[64,64,256]{2,1,0:T(8,128)(2,1)} %broadcast_in_dim.20), calls=%async_computation | async-start | bytes 4194304 | tf_op jit(solution)/shard_map/all_to_all | solution.py:25
  18.0 3.5 %collective-permute-start.1 = (bf16[8,2048]{1,0:T(8,128)(2,1)S(1)}, bf16[8,2048]{1,0:T(8,128)(2,1)S(1)}, u32[]{:S(2)}, u32[]{:S(2)}) collective-permute-start(bf16[8,2048]{1,0:T(8,128)(2,1)S(1)} %slice.4), channel_id=1, source_target_pairs={{0,8},{8,16},{16,24},{24,32},{32,40},{40,48},{48,56},{56,64},{64,7... | collective-permute-start | bytes 98312 | tf_op jit(solution)/shard_map/ppermute | solution.py:31
  21.5 46.3 %collective-permute-done.1 = bf16[8,2048]{1,0:T(8,128)(2,1)S(1)} collective-permute-done((bf16[8,2048]{1,0:T(8,128)(2,1)S(1)}, bf16[8,2048]{1,0:T(8,128)(2,1)S(1)}, u32[]{:S(2)}, u32[]{:S(2)}) %collective-permute-start.1) | collective-permute-done | bytes 32800 | tf_op jit(solution)/shard_map/ppermute | solution.py:31
  67.8 14.2 %all_gather.13.mine = bf16[160,2048]{1,0:T(8,128)(2,1)S(1)} all-gather(bf16[40,2048]{1,0:T(8,128)(2,1)S(1)} %pad_maximum_fusion), channel_id=1, replica_groups=mesh['sp_0'=8,'sp_1'=8,'fs'=4,'tp'=2] {'fs'}, dimensions={0}, use_global_device_ids=true | all-gather | bytes 819200 | tf_op jit(solution)/shard_map/all_gather | solution.py:437
  82.0 1.9 %collective-permute-start.2 = (bf16[160,2048]{1,0:T(8,128)(2,1)S(1)}, bf16[160,2048]{1,0:T(8,128)(2,1)}, u32[]{:S(2)}, u32[]{:S(2)}) collective-permute-start(bf16[160,2048]{1,0:T(8,128)(2,1)S(1)} %all_gather.13.mine), channel_id=1, source_target_pairs={{0,1},{1,0},{2,3},{3,2},{4,5},{5,4},{6,7},{7,6},{8,9},{9,8},{10,11... | collective-permute-start | bytes 1966088 | tf_op jit(solution)/shard_map/ppermute | solution.py:439
  84.1 2.4 %collective-permute-start.4 = (bf16[256,2048]{1,0:T(8,128)(2,1)S(1)}, bf16[256,2048]{1,0:T(8,128)(2,1)S(1)}, u32[]{:S(2)}, u32[]{:S(2)}) collective-permute-start(bf16[256,2048]{1,0:T(8,128)(2,1)S(1)} %constant_dynamic-update-slice_fusion.w_mine_far), channel_id=1, source_target_pairs={{0,1},{1,0},{2,3},{3,2},{4,5},{5,4},{6,7},{7,6},{8,9},{9,8},{10,11... | collective-permute-start | bytes 3145736 | tf_op jit(solution)/shard_map/ppermute | solution.py:462
  86.5 0.6 fusion.1.rate
  87.1 0.6 pad_add_fusion.place
  87.7 4.2 %project.1 = (bf16[128,256]{1,0:T(8,128)(2,1)}, f32[256,128]{1,0:T(8,128)}, f32[256,128]{1,0:T(8,128)}, f32[256,128]{1,0:T(8,128)}, f32[2,128]{1,0:T(2,128)}) custom-call(s32[4]{0:T(128)} %pad_add_fusion.place, bf16[160,2048]{1,0:T(8,128)(2,1)} %copy-done.1, bf16[160,2048]{1,0:T(8,128)(2,1)} %collective-permute-done.2.theirs, bf16[2048,128]{1,0:T(8,128)(2,1)} %w_query.1, ...), custom_call_target="tpu_custom_call" | custom-call | flops 402653184 | bytes 4194304 | tf_op jit(solution)/shard_map/project/pallas_call | solution.py:146
  91.9 13.2 %all-gather = bf16[512,256]{1,0:T(8,128)(2,1)} all-gather(bf16[128,256]{1,0:T(8,128)(2,1)} %get-tuple-element.19), channel_id=2, replica_groups=mesh['sp_0'=8,'sp_1'=8,'fs'=4,'tp'=2] {'fs'}, dimensions={0}, use_global_device_ids=true | all-gather | bytes 327680 | tf_op jit(solution)/shard_map/all_gather | solution.py:457
  105.1 1.3 broadcast_in_dim.22
  106.4 9.6 %all-to-all-start.2 = ((f32[64,2,128]{2,1,0:T(2,128)}), f32[64,2,128]{2,1,0:T(2,128)S(1)}, u32[]{:S(2)}, u32[]{:S(2)}) async-start(f32[64,2,128]{2,1,0:T(2,128)} %broadcast_in_dim.22), calls=%async_computation.2 | async-start | bytes 131072 | tf_op jit(solution)/shard_map/all_to_all | solution.py:25
  116.0 17.4 %attention.1 = bf16[4,2,272,128]{3,2,1,0:T(8,128)(2,1)} custom-call(s32[4]{0:T(128)} %pad_add_fusion.place, bf16[4,128,256]{2,1,0:T(8,128)(2,1)} %bitcast.19, bf16[8,512,256]{2,1,0:T(8,128)(2,1)} %bitcast.7.kv_far), custom_call_target="tpu_custom_call" | custom-call | flops 4294967296 | bytes 4194304 | tf_op jit(solution)/shard_map/attention/pallas_call | solution.py:304
  133.5 3.5 %all-to-all-start.1 = ((bf16[8,272,128]{2,1,0:T(8,128)(2,1)}), bf16[8,272,128]{2,1,0:T(8,128)(2,1)S(1)}, u32[]{:S(2)}, u32[]{:S(2)}) async-start(bf16[8,272,128]{2,1,0:T(8,128)(2,1)} %bitcast.18), calls=%async_computation.1 | async-start | bytes 1114112 | tf_op jit(solution)/shard_map/all_to_all | solution.py:468
  137.1 1.8 %final_states.1 = (bf16[128,128]{1,0:T(8,128)(2,1)}, bf16[128,128]{1,0:T(8,128)(2,1)}) custom-call(s32[4]{0:T(128)} %pad_add_fusion.place, f32[64,2,128]{2,1,0:T(2,128)} %copy-done.8, f32[1,128]{1,0:T(1,128)} %bitcast.21, f32[256,128]{1,0:T(8,128)} %get-tuple-element.22.decays, f32[256,128]{1,0:T(8,128)} %get-tuple-element.23.states, ...), custom_call_target="tpu_custom_call" | custom-call | flops 1048576 | bytes 524288 | tf_op jit(solution)/shard_map/final_states/pallas_call | solution.py:196
  138.9 2.3 %collective-permute-start.3 = (bf16[128,128]{1,0:T(8,128)(2,1)}, bf16[128,128]{1,0:T(8,128)(2,1)S(1)}, u32[]{:S(2)}, u32[]{:S(2)}) collective-permute-start(bf16[128,128]{1,0:T(8,128)(2,1)} %get-tuple-element.26), channel_id=1, source_target_pairs={{0,1},{1,0},{2,3},{3,2},{4,5},{5,4},{6,7},{7,6},{8,9},{9,8},{10,11... | collective-permute-start | bytes 98312 | tf_op jit(solution)/shard_map/ppermute | solution.py:474
  141.2 2.0 %collective-permute-start = (f32[1]{0:T(128)}, f32[1]{0:T(128)}, u32[]{:S(2)}, u32[]{:S(2)}) collective-permute-start(f32[1]{0:T(128)} %param.30), channel_id=1, source_target_pairs={{0,1},{1,0},{2,3},{3,2},{4,5},{5,4},{6,7},{7,6},{8,9},{9,8},{10,11... | collective-permute-start | bytes 20 | tf_op jit(solution)/shard_map/ppermute | solution.py:463
  143.8 0.6 collective-permute-done.lam_theirs
  144.5 3.1 %all-to-all-done.1 = bf16[8,272,128]{2,1,0:T(8,128)(2,1)S(1)} async-done(((bf16[8,272,128]{2,1,0:T(8,128)(2,1)}), bf16[8,272,128]{2,1,0:T(8,128)(2,1)S(1)}, u32[]{:S(2)}, u32[]{:S(2)}) %all-to-all-start.1) | async-done | bytes 557088 | tf_op jit(solution)/shard_map/all_to_all | solution.py:468
  147.7 0.8 copy-done.3
  148.5 4.6 %finish.1 = (bf16[32,2048]{1,0:T(8,128)(2,1)}, bf16[32,2048]{1,0:T(8,128)(2,1)}, bf16[32,2048]{1,0:T(8,128)(2,1)}, bf16[32,2048]{1,0:T(8,128)(2,1)}) custom-call(s32[4]{0:T(128)} %pad_add_fusion.place, f32[1]{0:T(128)S(6)} %copy.19.lam, f32[1]{0:T(128)} %collective-permute-done.lam_theirs, bf16[4,2,272,128]{3,2,1,0:T(8,128)(2,1)} %bitcast.17, ...), custom_call_target="tpu_custom_call" | custom-call | flops 268435456 | bytes 3145728 | tf_op jit(solution)/shard_map/finish/pallas_call | solution.py:372
  153.1 2.4 %collective-permute-start.5 = (bf16[32,2048]{1,0:T(8,128)(2,1)}, bf16[32,2048]{1,0:T(8,128)(2,1)S(1)}, u32[]{:S(2)}, u32[]{:S(2)}) collective-permute-start(bf16[32,2048]{1,0:T(8,128)(2,1)} %get-tuple-element.28), channel_id=1, source_target_pairs={{0,4},{2,6},{4,0},{6,2},{1,5},{3,7},{5,1},{7,3},{8,12},{10,14},{12... | collective-permute-start | bytes 393224 | tf_op jit(solution)/shard_map/ppermute | solution.py:491
  155.5 3.5 %collective-permute-start.6 = (bf16[32,2048]{1,0:T(8,128)(2,1)}, bf16[32,2048]{1,0:T(8,128)(2,1)S(1)}, u32[]{:S(2)}, u32[]{:S(2)}) collective-permute-start(bf16[32,2048]{1,0:T(8,128)(2,1)} %get-tuple-element.29), channel_id=1, source_target_pairs={{0,2},{2,0},{4,6},{6,4},{1,3},{3,1},{5,7},{7,5},{8,10},{10,8},{12,... | collective-permute-start | bytes 393224 | tf_op jit(solution)/shard_map/ppermute | solution.py:491
  159.0 4.0 %collective-permute-start.7 = (bf16[32,2048]{1,0:T(8,128)(2,1)}, bf16[32,2048]{1,0:T(8,128)(2,1)S(1)}, u32[]{:S(2)}, u32[]{:S(2)}) collective-permute-start(bf16[32,2048]{1,0:T(8,128)(2,1)} %get-tuple-element.30), channel_id=1, source_target_pairs={{0,6},{2,4},{4,2},{6,0},{1,7},{3,5},{5,3},{7,1},{8,14},{10,12},{12... | collective-permute-start | bytes 393224 | tf_op jit(solution)/shard_map/ppermute | solution.py:491
  163.0 0.1 collective-permute-done.6
  163.1 4.2 %collective-permute-done.7 = bf16[32,2048]{1,0:T(8,128)(2,1)S(1)} collective-permute-done((bf16[32,2048]{1,0:T(8,128)(2,1)}, bf16[32,2048]{1,0:T(8,128)(2,1)S(1)}, u32[]{:S(2)}, u32[]{:S(2)}) %collective-permute-start.7) | collective-permute-done | bytes 131104 | tf_op jit(solution)/shard_map/ppermute | solution.py:491
  167.3 1.6 add_convert_fusion
  (32 shorter events, 0.2 us)
Async XLA Ops:
  0.0 3.9 %copy-start = (bf16[2048,128]{1,0:T(8,128)(2,1)S(1)}, bf16[2048,128]{1,0:T(8,128)(2,1)}, u32[]{:S(2)}) copy-start(bf16[2048,128]{1,0:T(8,128)(2,1)} %param.21) | copy-start | bytes 1572868
  7.0 10.9 %copy-start.4 = (bf16[32,2048]{1,0:T(8,128)(2,1)S(1)}, bf16[32,2048]{1,0:T(8,128)(2,1)}, u32[]{:S(2)}) copy-start(bf16[32,2048]{1,0:T(8,128)(2,1)} %normalized.1) | copy-start | bytes 393220
  7.0 77.0 %copy-start.6 = (bf16[128,2048]{1,0:T(8,128)(2,1)S(1)}, bf16[128,2048]{1,0:T(8,128)(2,1)}, u32[]{:S(2)}) copy-start(bf16[128,2048]{1,0:T(8,128)(2,1)} %param.32) | copy-start | bytes 1572868
  7.0 98.1 %all-to-all-start = ((bf16[64,64,256]{2,1,0:T(8,128)(2,1)}), bf16[64,64,256]{2,1,0:T(8,128)(2,1)}, u32[]{:S(2)}, u32[]{:S(2)}) async-start(bf16[64,64,256]{2,1,0:T(8,128)(2,1)} %broadcast_in_dim.20), calls=%async_computation | async-start | bytes 4194304 | tf_op jit(solution)/shard_map/all_to_all | solution.py:25
  17.9 66.1 %copy-start.7 = (bf16[128,2048]{1,0:T(8,128)(2,1)S(1)}, bf16[128,2048]{1,0:T(8,128)(2,1)}, u32[]{:S(2)}) copy-start(bf16[128,2048]{1,0:T(8,128)(2,1)} %param.33) | copy-start | bytes 1572868
  17.9 68.6 %copy-start.10 = (f32[128]{0:T(128)S(1)}, f32[128]{0:T(128)}, u32[]{:S(2)}) copy-start(f32[128]{0:T(128)} %param.27) | copy-start | bytes 1540
  18.0 49.9 %collective-permute-start.1 = (bf16[8,2048]{1,0:T(8,128)(2,1)S(1)}, bf16[8,2048]{1,0:T(8,128)(2,1)S(1)}, u32[]{:S(2)}, u32[]{:S(2)}) collective-permute-start(bf16[8,2048]{1,0:T(8,128)(2,1)S(1)} %slice.4), channel_id=1, source_target_pairs={{0,8},{8,16},{16,24},{24,32},{32,40},{40,48},{48,56},{56,64},{64,7... | collective-permute-start | bytes 98312 | tf_op jit(solution)/shard_map/ppermute | solution.py:31
  82.0 5.6 %copy-start.1 = (bf16[160,2048]{1,0:T(8,128)(2,1)}, bf16[160,2048]{1,0:T(8,128)(2,1)S(1)}, u32[]{:S(2)}) copy-start(bf16[160,2048]{1,0:T(8,128)(2,1)S(1)} %all_gather.13.mine) | copy-start | bytes 1966084
  82.0 5.6 %collective-permute-start.2 = (bf16[160,2048]{1,0:T(8,128)(2,1)S(1)}, bf16[160,2048]{1,0:T(8,128)(2,1)}, u32[]{:S(2)}, u32[]{:S(2)}) collective-permute-start(bf16[160,2048]{1,0:T(8,128)(2,1)S(1)} %all_gather.13.mine), channel_id=1, source_target_pairs={{0,1},{1,0},{2,3},{3,2},{4,5},{5,4},{6,7},{7,6},{8,9},{9,8},{10,11... | collective-permute-start | bytes 1966088 | tf_op jit(solution)/shard_map/ppermute | solution.py:439
  84.1 49.4 %copy-start.2 = (bf16[256,2048]{1,0:T(8,128)(2,1)}, bf16[256,2048]{1,0:T(8,128)(2,1)S(1)}, u32[]{:S(2)}) copy-start(bf16[256,2048]{1,0:T(8,128)(2,1)S(1)} %constant_dynamic-update-slice_fusion.w_mine_far) | copy-start | bytes 3145732
  84.1 60.4 %collective-permute-start.4 = (bf16[256,2048]{1,0:T(8,128)(2,1)S(1)}, bf16[256,2048]{1,0:T(8,128)(2,1)S(1)}, u32[]{:S(2)}, u32[]{:S(2)}) collective-permute-start(bf16[256,2048]{1,0:T(8,128)(2,1)S(1)} %constant_dynamic-update-slice_fusion.w_mine_far), channel_id=1, source_target_pairs={{0,1},{1,0},{2,3},{3,2},{4,5},{5,4},{6,7},{7,6},{8,9},{9,8},{10,11... | collective-permute-start | bytes 3145736 | tf_op jit(solution)/shard_map/ppermute | solution.py:462
  106.4 27.0 %all-to-all-start.2 = ((f32[64,2,128]{2,1,0:T(2,128)}), f32[64,2,128]{2,1,0:T(2,128)S(1)}, u32[]{:S(2)}, u32[]{:S(2)}) async-start(f32[64,2,128]{2,1,0:T(2,128)} %broadcast_in_dim.22), calls=%async_computation.2 | async-start | bytes 131072 | tf_op jit(solution)/shard_map/all_to_all | solution.py:25
  133.5 3.6 %copy-start.8 = (f32[64,2,128]{2,1,0:T(2,128)}, f32[64,2,128]{2,1,0:T(2,128)S(1)}, u32[]{:S(2)}) copy-start(f32[64,2,128]{2,1,0:T(2,128)S(1)} %all-to-all-done.2.pieces) | copy-start | bytes 196612
  133.5 14.1 %all-to-all-start.1 = ((bf16[8,272,128]{2,1,0:T(8,128)(2,1)}), bf16[8,272,128]{2,1,0:T(8,128)(2,1)S(1)}, u32[]{:S(2)}, u32[]{:S(2)}) async-start(bf16[8,272,128]{2,1,0:T(8,128)(2,1)} %bitcast.18), calls=%async_computation.1 | async-start | bytes 1114112 | tf_op jit(solution)/shard_map/all_to_all | solution.py:468
  138.9 5.6 %collective-permute-start.3 = (bf16[128,128]{1,0:T(8,128)(2,1)}, bf16[128,128]{1,0:T(8,128)(2,1)S(1)}, u32[]{:S(2)}, u32[]{:S(2)}) collective-permute-start(bf16[128,128]{1,0:T(8,128)(2,1)} %get-tuple-element.26), channel_id=1, source_target_pairs={{0,1},{1,0},{2,3},{3,2},{4,5},{5,4},{6,7},{7,6},{8,9},{9,8},{10,11... | collective-permute-start | bytes 98312 | tf_op jit(solution)/shard_map/ppermute | solution.py:474
  141.2 3.3 %collective-permute-start = (f32[1]{0:T(128)}, f32[1]{0:T(128)}, u32[]{:S(2)}, u32[]{:S(2)}) collective-permute-start(f32[1]{0:T(128)} %param.30), channel_id=1, source_target_pairs={{0,1},{1,0},{2,3},{3,2},{4,5},{5,4},{6,7},{7,6},{8,9},{9,8},{10,11... | collective-permute-start | bytes 20 | tf_op jit(solution)/shard_map/ppermute | solution.py:463
  144.5 3.2 %copy-start.9 = (bf16[128,128]{1,0:T(8,128)(2,1)}, bf16[128,128]{1,0:T(8,128)(2,1)S(1)}, u32[]{:S(2)}) copy-start(bf16[128,128]{1,0:T(8,128)(2,1)S(1)} %collective-permute-done.3.lru_theirs) | copy-start | bytes 98308
  144.5 3.2 %copy-start.5 = (bf16[256,2048]{1,0:T(8,128)(2,1)}, bf16[256,2048]{1,0:T(8,128)(2,1)S(1)}, u32[]{:S(2)}) copy-start(bf16[256,2048]{1,0:T(8,128)(2,1)S(1)} %collective-permute-done.4.w_theirs_far) | copy-start | bytes 3145732
  147.6 0.8 copy-start.3
  153.1 9.8 %collective-permute-start.5 = (bf16[32,2048]{1,0:T(8,128)(2,1)}, bf16[32,2048]{1,0:T(8,128)(2,1)S(1)}, u32[]{:S(2)}, u32[]{:S(2)}) collective-permute-start(bf16[32,2048]{1,0:T(8,128)(2,1)} %get-tuple-element.28), channel_id=1, source_target_pairs={{0,4},{2,6},{4,0},{6,2},{1,5},{3,7},{5,1},{7,3},{8,12},{10,14},{12... | collective-permute-start | bytes 393224 | tf_op jit(solution)/shard_map/ppermute | solution.py:491
  155.5 7.6 %collective-permute-start.6 = (bf16[32,2048]{1,0:T(8,128)(2,1)}, bf16[32,2048]{1,0:T(8,128)(2,1)S(1)}, u32[]{:S(2)}, u32[]{:S(2)}) collective-permute-start(bf16[32,2048]{1,0:T(8,128)(2,1)} %get-tuple-element.29), channel_id=1, source_target_pairs={{0,2},{2,0},{4,6},{6,4},{1,3},{3,1},{5,7},{7,5},{8,10},{10,8},{12,... | collective-permute-start | bytes 393224 | tf_op jit(solution)/shard_map/ppermute | solution.py:491
  159.0 8.3 %collective-permute-start.7 = (bf16[32,2048]{1,0:T(8,128)(2,1)}, bf16[32,2048]{1,0:T(8,128)(2,1)S(1)}, u32[]{:S(2)}, u32[]{:S(2)}) collective-permute-start(bf16[32,2048]{1,0:T(8,128)(2,1)} %get-tuple-element.30), channel_id=1, source_target_pairs={{0,6},{2,4},{4,2},{6,0},{1,7},{3,5},{5,3},{7,1},{8,14},{10,12},{12... | collective-permute-start | bytes 393224 | tf_op jit(solution)/shard_map/ppermute | solution.py:491

commit v7 on v6

--- a/solution.py
+++ b/solution.py
@@ -43,18 +43,22 @@
     return pl.BlockSpec(memory_space=pltpu.SMEM)
 
 
-def norm_kernel(tokens, gain, out):
+def norm_kernel(tokens, gain, out, last):
     floats = tokens[...].astype(jnp.float32)
     level = lax.rsqrt(jnp.mean(floats * floats, axis=1, keepdims=True) + input_eps)
     out[...] = (floats * level * gain[...]).astype(jnp.bfloat16)
-
-
-def normalized(tokens, gain):
+    last[...] = out[out.shape[0] - last.shape[0] :, :]
+
+
+def normalized(tokens, gain, margin):
     return pl.pallas_call(
         norm_kernel,
-        out_shape=jax.ShapeDtypeStruct(tokens.shape, jnp.bfloat16),
+        out_shape=(
+            jax.ShapeDtypeStruct(tokens.shape, jnp.bfloat16),
+            jax.ShapeDtypeStruct((margin, tokens.shape[1]), jnp.bfloat16),
+        ),
         in_specs=[vmem(), vmem()],
-        out_specs=vmem(),
+        out_specs=(vmem(), vmem()),
         cost_estimate=pl.CostEstimate(
             flops=4 * tokens.size, bytes_accessed=1 << 18, transcendentals=0
         ),
@@ -136,11 +140,13 @@
     decays[...] = decay
     states[...] = drive
     last = decay.shape[0] - 1
-    ends[0:1, :] = decay[last:]
-    ends[1:2, :] = drive[last:]
-
-
-def project(place, mine, theirs, weights, taps, w_recur, w_admit, rate, scale, fs_count, rows):
+    both = jnp.concatenate([decay[last:], drive[last:]], axis=0)
+    ends[...] = jnp.broadcast_to(both[None], ends.shape)
+
+
+def project(
+    place, mine, theirs, weights, taps, w_recur, w_admit, rate, scale, blocks, fs_count, rows
+):
     channels = scale.shape[1]
     block = jax.ShapeDtypeStruct(scale.shape, jnp.float32)
     return pl.pallas_call(
@@ -150,7 +156,7 @@
             block,
             block,
             block,
-            jax.ShapeDtypeStruct((2, channels), jnp.float32),
+            jax.ShapeDtypeStruct((blocks, 2, channels), jnp.float32),
         ),
         in_specs=[smem()] + [vmem()] * 10,
         out_specs=(vmem(),) * 5,
@@ -208,10 +214,11 @@
 
 
 def attention_kernel(
-    place, group, kv_far, packed, query, peak, values, value_t, kv, arrivals,
-    *, block_rows, part_rows,
+    place, group, kv_far, *refs, block_rows, part_rows, start, stop
 ):
-    heads, size, rows = group.shape
+    packed, query, peak, values, value_t, kv, arrivals = refs[-7:]
+    heads = stop - start
+    _, size, rows = group.shape
     chunk_keys = kv.shape[1]
     z, y, member = (place[0], place[1], place[2])
 
@@ -227,7 +234,7 @@
     lax.fori_loop(0, z, begin, 0)
     line = lax.broadcasted_iota(jnp.int32, (size, rows), 0)
     for h in range(heads):
-        whole = group[h]
+        whole = group[start + h]
         zero = jnp.zeros_like(whole)
         query[2 * h] = jnp.where(line < size // 2, whole, zero)
         query[2 * h + 1] = jnp.where(line < size // 2, zero, whole)
@@ -277,6 +284,8 @@
 
     lax.fori_loop(0, z, earlier, 0)
 
+    if start:
+        packed[:start] = refs[0][...]
     half = rows // 2
     line = lax.broadcasted_iota(jnp.int32, (16, rows), 0)
     for h in range(heads):
@@ -291,20 +300,24 @@
             tail = jnp.where(line == 2 * m, coarse, tail)
             tail = jnp.where(line == 2 * m + 1, level - coarse, tail)
             for t in range(2):
-                packed[h, t, m * size : (m + 1) * size, :] = shares[:, t * half : (t + 1) * half]
+                packed[start + h, t, m * size : (m + 1) * size, :] = shares[:, t * half : (t + 1) * half]
         rounded = tail.astype(jnp.bfloat16)
         for t in range(2):
-            packed[h, t, 2 * size : 2 * size + 16, :] = rounded[:, t * half : (t + 1) * half]
-
-
-def attention(place, group, kv, block_rows, part_rows):
-    heads, size, rows = group.shape
+            packed[start + h, t, 2 * size : 2 * size + 16, :] = rounded[:, t * half : (t + 1) * half]
+
+
+def attention(place, group, kv, earlier, stop, block_rows, part_rows):
+    start = 0 if earlier is None else earlier.shape[0]
+    heads = stop - start
+    _, size, rows = group.shape
     z_count, chunk_keys, _ = kv.shape
     keys = chunk_keys * z_count
     return pl.pallas_call(
-        functools.partial(attention_kernel, block_rows=block_rows, part_rows=part_rows),
-        out_shape=jax.ShapeDtypeStruct((heads, 2, 2 * size + 16, rows // 2), jnp.bfloat16),
-        in_specs=[smem(), vmem(), anywhere()],
+        functools.partial(
+            attention_kernel, block_rows=block_rows, part_rows=part_rows, start=start, stop=stop
+        ),
+        out_shape=jax.ShapeDtypeStruct((stop, 2, 2 * size + 16, rows // 2), jnp.bfloat16),
+        in_specs=[smem(), vmem(), anywhere()] + [vmem()] * (start > 0),
         out_specs=vmem(),
         scratch_shapes=[
             pltpu.VMEM((2 * heads, size, rows), jnp.bfloat16),
@@ -320,20 +333,10 @@
             transcendentals=2 * heads * rows * keys,
         ),
         name="attention",
-    )(place, group, kv)
-
-
-def finish_kernel(
-    place, lam, lam_theirs, parts, gain, lru_mine, lru_theirs, w_mine_far, w_theirs_far, *refs,
-):
-    outs = refs[:-4]
-    w_mine, w_theirs, whole, arrivals = refs[-4:]
-    copies = [
-        pltpu.make_async_copy(w_mine_far, w_mine, arrivals.at[0]),
-        pltpu.make_async_copy(w_theirs_far, w_theirs, arrivals.at[1]),
-    ]
-    for copy in copies:
-        copy.start()
+    )(place, group, kv, *(() if earlier is None else (earlier,)))
+
+
+def finish_kernel(place, lam, lam_theirs, parts, gain, lru_mine, lru_theirs, w_mine, w_theirs, out):
     count, _, lines, _ = parts.shape
     size = (lines - 16) // 2
     core = place[3]
@@ -358,28 +361,18 @@
 
     mine = jnp.concatenate([lru_mine[...], head_output(core, lam[0])], axis=1)
     theirs = jnp.concatenate([lru_theirs[...], head_output(1 - core, lam_theirs[0])], axis=1)
-    for copy in copies:
-        copy.wait()
     result = jnp.dot(mine, w_mine[...], preferred_element_type=jnp.float32)
     result = result + jnp.dot(theirs, w_theirs[...], preferred_element_type=jnp.float32)
-    whole[...] = result.astype(jnp.bfloat16).reshape(whole.shape)
-    for by, out in enumerate(outs):
-        out[...] = whole[place[2] ^ by]
-
-
-def finish(place, lam, lam_theirs, parts, gain, lru_mine, lru_theirs, w_mine, w_theirs, slots):
+    out[...] = result.astype(jnp.bfloat16)
+
+
+def finish(place, lam, lam_theirs, parts, gain, lru_mine, lru_theirs, w_mine, w_theirs):
     rows, wide = (lru_mine.shape[0], w_mine.shape[1])
     return pl.pallas_call(
         finish_kernel,
-        out_shape=(jax.ShapeDtypeStruct((rows // slots, wide), jnp.bfloat16),) * slots,
-        in_specs=[smem()] * 3 + [vmem()] * 4 + [anywhere()] * 2,
-        out_specs=(vmem(),) * slots,
-        scratch_shapes=[
-            pltpu.VMEM(w_mine.shape, w_mine.dtype),
-            pltpu.VMEM(w_theirs.shape, w_theirs.dtype),
-            pltpu.VMEM((slots, rows // slots, wide), jnp.bfloat16),
-            pltpu.SemaphoreType.DMA((2,)),
-        ],
+        out_shape=jax.ShapeDtypeStruct((rows, wide), jnp.bfloat16),
+        in_specs=[smem()] * 3 + [vmem()] * 6,
+        out_specs=vmem(),
         cost_estimate=pl.CostEstimate(
             flops=2 * rows * wide * 512, bytes_accessed=3 << 20, transcendentals=rows * 16
         ),
@@ -406,7 +399,7 @@
     w_out_lru,
     w_out_attn,
 ):
-    member_rows, _ = tokens.shape
+    member_rows, wide = tokens.shape
     fs_count = lax.axis_size("fs")
     tp_count = lax.axis_size("tp")
     row_count = member_rows * fs_count * tp_count
@@ -416,10 +409,9 @@
     z_count, z = (lax.axis_size("sp_0"), lax.axis_index("sp_0"))
     y_count, y = (lax.axis_size("sp_1"), lax.axis_index("sp_1"))
 
-    normed = normalized(tokens, norm_gain[None])
-
-    margin = 8
-    before_rows = passed_along(normed[member_rows - margin :], SP, 1)
+    normed, last_rows = normalized(tokens, norm_gain[None], 8)
+
+    before_rows = passed_along(last_rows, SP, 1)
 
     chip_rows = lax.all_gather(normed, "tp", axis=0, tiled=True)
     kv_here = jnp.concatenate(
@@ -450,19 +442,22 @@
         w_admit,
         rate[None],
         decay_scale,
+        z_count * y_count,
         fs_count,
         member_rows,
     )
 
     group = lax.all_gather(query_t, "fs")
 
-    everywhere = from_everyone(ends, SP)
-
     w_mine = jnp.concatenate([w_out_lru, w_out_attn], axis=0)
     w_theirs = lax.ppermute(w_mine, "tp", swap)
     lam_theirs = lax.ppermute(diff_lambda, "tp", swap)
 
-    carried = attention(place, group, everyone, row_count, share_rows)
+    half_heads = fs_count // 2
+    part = attention(place, group, everyone, None, half_heads, row_count, share_rows)
+    ends, part = lax.optimization_barrier((ends, part))
+    everywhere = lax.all_to_all(ends, SP, split_axis=0, concat_axis=0, tiled=True)
+    carried = attention(place, group, everyone, part, fs_count, row_count, share_rows)
     lines, half_rows = carried.shape[2:]
     carried = carried.reshape(fs_count * tp_count, lines, half_rows)
     packed = lax.all_to_all(carried, ("fs", "tp"), split_axis=0, concat_axis=0, tiled=True)
@@ -483,13 +478,10 @@
         lru_theirs,
         w_mine,
         w_theirs,
-        fs_count,
     )
-    mixed = partial[0].astype(jnp.float32)
-    for by in (2, 1, 3):
-        pairs = [(i, i ^ by) for i in range(fs_count)]
-        mixed = mixed + lax.ppermute(partial[by], "fs", pairs).astype(jnp.float32)
-    return mixed.astype(jnp.bfloat16)
+    partial = partial.reshape(fs_count, member_rows, wide)
+    arrived = lax.all_to_all(partial, "fs", split_axis=0, concat_axis=0, tiled=True)
+    return arrived.astype(jnp.float32).sum(axis=0).astype(jnp.bfloat16)
 
 
 def solution(mesh):

time: 170 us -> 174 us (1.024)
  the two profiles are of different devices: /device:TPU:448 before, /device:TPU:1 now
where the time goes in v7:
time: 174 us; the launch traced here: 173 us
  starting transfers between devices  54.8 us (31%)
  waiting for transfers between devices  49.3 us (28%)
  blocking collectives  42.8 us (25%)
  Pallas kernels  19.4 us (11%)
  local copies, waits for them, and re-layouts  2.49 us (1%)
  other arithmetic  1.97 us (1%)
    ppermute x1, waiting for transfers between devices, passed_along(): return lax.ppermute(value, axis, pairs)  39.2 us
    all_to_all x1, starting transfers between devices, body(): lax.all_to_all(ends, SP, split_axis=0, concat_axis=0, tiled=True)  19.2 us
    all_to_all x1, blocking collectives, body(): lax.all_to_all(partial, 'fs', split_axis=0, concat_axis=0, tiled=True)  12.1 us
    all_to_all x1, starting transfers between devices, from_everyone(): return lax.all_to_all(copies, axis, split_axis=0, concat_axis=0, tiled=True)  11.4 us
    all_gather x1, blocking collectives, body(): mine = lax.all_gather(sent, 'fs', axis=0, tiled=True)  11.3 us
    all_gather x1, blocking collectives, body(): group = lax.all_gather(query_t, 'fs')  10.8 us
    all_gather x1, blocking collectives, body(): chip_rows = lax.all_gather(normed, 'tp', axis=0, tiled=True)  8.67 us
    all_to_all x1, starting transfers between devices, body(): lax.all_to_all(carried, ('fs', 'tp'), split_axis=0, concat_axis=0, tiled=...  8 us
  transfers between devices with their start and end apart: 8, of which 4 were waited for; matrix products, arithmetic and copies ran while one was open for 1% of the time, Pallas kernels for 8%

profile of v7, /device:TPU:1, one launch (start us, length us, event | category | flops | bytes accessed | tf_op | source)
XLA Modules:
  0.0 173.1 jit_solution(5695374090199633155)
XLA Ops:
  0.0 1.8 %normalized.1 = (bf16[32,2048]{1,0:T(8,128)(2,1)}, bf16[8,2048]{1,0:T(8,128)(2,1)}) custom-call(bf16[32,2048]{1,0:T(8,128)(2,1)} %tokens.1, f32[1,2048]{1,0:T(1,128)} %bitcast.23), custom_call_target="tpu_custom_call" | custom-call | flops 262144 | bytes 262144 | tf_op jit(solution)/shard_map/normalized/pallas_call | solution.py:54
  1.8 8.7 %all_gather.12 = bf16[64,2048]{1,0:T(8,128)(2,1)S(1)} all-gather(bf16[32,2048]{1,0:T(8,128)(2,1)} %get-tuple-element.19), channel_id=1, replica_groups=mesh['sp_0'=8,'sp_1'=8,'fs'=4,'tp'=2] {'tp'}, dimensions={0}, use_global_device_ids=true | all-gather | bytes 393216 | tf_op jit(solution)/shard_map/all_gather | solution.py:416
  10.4 0.2 convolution_convert_fusion
  10.7 1.3 convolution_convert_fusion.1
  11.9 1.5 broadcast_in_dim.17
  13.5 11.4 %all-to-all-start = ((bf16[64,64,256]{2,1,0:T(8,128)(2,1)}), bf16[64,64,256]{2,1,0:T(8,128)(2,1)}, u32[]{:S(2)}, u32[]{:S(2)}) async-start(bf16[64,64,256]{2,1,0:T(8,128)(2,1)} %broadcast_in_dim.17), calls=%async_computation | async-start | bytes 4194304 | tf_op jit(solution)/shard_map/all_to_all | solution.py:25
  24.9 0.0 copy-start.7
  24.9 0.0 copy-start.11
  24.9 3.0 %collective-permute-start.1 = (bf16[8,2048]{1,0:T(8,128)(2,1)S(1)}, bf16[8,2048]{1,0:T(8,128)(2,1)S(1)}, u32[]{:S(2)}, u32[]{:S(2)}) collective-permute-start(bf16[8,2048]{1,0:T(8,128)(2,1)S(1)} %copy-done.10), channel_id=1, source_target_pairs={{0,8},{8,16},{16,24},{24,32},{32,40},{40,48},{48,56},{56,64},{64,7... | collective-permute-start | bytes 98312 | tf_op jit(solution)/shard_map/ppermute | solution.py:31
  27.9 39.2 %collective-permute-done.1 = bf16[8,2048]{1,0:T(8,128)(2,1)S(1)} collective-permute-done((bf16[8,2048]{1,0:T(8,128)(2,1)S(1)}, bf16[8,2048]{1,0:T(8,128)(2,1)S(1)}, u32[]{:S(2)}, u32[]{:S(2)}) %collective-permute-start.1) | collective-permute-done | bytes 32800 | tf_op jit(solution)/shard_map/ppermute | solution.py:31
  67.1 11.3 %all_gather.13.mine = bf16[160,2048]{1,0:T(8,128)(2,1)S(1)} all-gather(bf16[40,2048]{1,0:T(8,128)(2,1)S(1)} %pad_maximum_fusion), channel_id=1, replica_groups=mesh['sp_0'=8,'sp_1'=8,'fs'=4,'tp'=2] {'fs'}, dimensions={0}, use_global_device_ids=true | all-gather | bytes 819200 | tf_op jit(solution)/shard_map/all_gather | solution.py:429
  78.5 7.0 %collective-permute-start.2 = (bf16[160,2048]{1,0:T(8,128)(2,1)S(1)}, bf16[160,2048]{1,0:T(8,128)(2,1)}, u32[]{:S(2)}, u32[]{:S(2)}) collective-permute-start(bf16[160,2048]{1,0:T(8,128)(2,1)S(1)} %all_gather.13.mine), channel_id=1, source_target_pairs={{0,1},{1,0},{2,3},{3,2},{4,5},{5,4},{6,7},{7,6},{8,9},{9,8},{10,11... | collective-permute-start | bytes 1966088 | tf_op jit(solution)/shard_map/ppermute | solution.py:431
  85.6 1.9 %collective-permute-start.4 = (bf16[256,2048]{1,0:T(8,128)(2,1)S(1)}, bf16[256,2048]{1,0:T(8,128)(2,1)S(1)}, u32[]{:S(2)}, u32[]{:S(2)}) collective-permute-start(bf16[256,2048]{1,0:T(8,128)(2,1)S(1)} %constant_dynamic-update-slice_fusion.w_mine), channel_id=1, source_target_pairs={{0,1},{1,0},{2,3},{3,2},{4,5},{5,4},{6,7},{7,6},{8,9},{9,8},{10,11... | collective-permute-start | bytes 3145736 | tf_op jit(solution)/shard_map/ppermute | solution.py:453
  87.5 0.5 fusion.1.rate
  88.1 0.7 pad_add_fusion.place
  88.7 4.3 %project.1 = (bf16[128,256]{1,0:T(8,128)(2,1)}, f32[256,128]{1,0:T(8,128)}, f32[256,128]{1,0:T(8,128)}, f32[256,128]{1,0:T(8,128)}, f32[64,2,128]{2,1,0:T(2,128)}) custom-call(s32[4]{0:T(128)} %pad_add_fusion.place, bf16[160,2048]{1,0:T(8,128)(2,1)} %copy-done.1, bf16[160,2048]{1,0:T(8,128)(2,1)} %collective-permute-done.2.theirs, ...), custom_call_target="tpu_custom_call" | custom-call | flops 402653184 | bytes 4194304 | tf_op jit(solution)/shard_map/project/pallas_call | solution.py:152
  93.0 10.8 %all-gather = bf16[512,256]{1,0:T(8,128)(2,1)} all-gather(bf16[128,256]{1,0:T(8,128)(2,1)} %get-tuple-element.21), channel_id=2, replica_groups=mesh['sp_0'=8,'sp_1'=8,'fs'=4,'tp'=2] {'fs'}, dimensions={0}, use_global_device_ids=true | all-gather | bytes 327680 | tf_op jit(solution)/shard_map/all_gather | solution.py:450
  103.8 0.0 all-to-all-done
  103.8 3.8 %attention.2.refs_0_ = bf16[2,2,272,128]{3,2,1,0:T(8,128)(2,1)} custom-call(s32[4]{0:T(128)} %pad_add_fusion.place, bf16[4,128,256]{2,1,0:T(8,128)(2,1)} %bitcast.21, bf16[8,512,256]{2,1,0:T(8,128)(2,1)} %bitcast.7.kv_far), custom_call_target="tpu_custom_call" | custom-call | flops 2147483648 | bytes 4194304 | tf_op jit(solution)/shard_map/attention/pallas_call | solution.py:315
  107.6 19.2 %all-to-all-start.2 = ((f32[64,2,128]{2,1,0:T(2,128)}), f32[64,2,128]{2,1,0:T(2,128)S(1)}, u32[]{:S(2)}, u32[]{:S(2)}) async-start(f32[64,2,128]{2,1,0:T(2,128)} %get-tuple-element.25), calls=%async_computation.2 | async-start | bytes 131072 | tf_op jit(solution)/shard_map/all_to_all | solution.py:459
  126.8 3.9 %attention.3 = bf16[4,2,272,128]{3,2,1,0:T(8,128)(2,1)} custom-call(s32[4]{0:T(128)} %pad_add_fusion.place, bf16[4,128,256]{2,1,0:T(8,128)(2,1)} %bitcast.22, bf16[8,512,256]{2,1,0:T(8,128)(2,1)} %bitcast.7.kv_far, bf16[2,2,272,128]{3,2,1,0:T(8,128)(2,1)} %attention.2.refs_0_), custom_call_target="tpu_custom_call" | custom-call | flops 2147483648 | bytes 4194304 | tf_op jit(solution)/shard_map/attention/pallas_call | solution.py:315
  130.8 7.1 %all-to-all-done.2.pieces = f32[64,2,128]{2,1,0:T(2,128)S(1)} async-done(((f32[64,2,128]{2,1,0:T(2,128)}), f32[64,2,128]{2,1,0:T(2,128)S(1)}, u32[]{:S(2)}, u32[]{:S(2)}) %all-to-all-start.2) | async-done | bytes 65568 | tf_op jit(solution)/shard_map/all_to_all | solution.py:459
  137.9 8.0 %all-to-all-start.1 = ((bf16[8,272,128]{2,1,0:T(8,128)(2,1)}), bf16[8,272,128]{2,1,0:T(8,128)(2,1)S(1)}, u32[]{:S(2)}, u32[]{:S(2)}) async-start(bf16[8,272,128]{2,1,0:T(8,128)(2,1)} %bitcast.20), calls=%async_computation.1 | async-start | bytes 1114112 | tf_op jit(solution)/shard_map/all_to_all | solution.py:463
  145.9 1.8 %final_states.1 = (bf16[128,128]{1,0:T(8,128)(2,1)}, bf16[128,128]{1,0:T(8,128)(2,1)}) custom-call(s32[4]{0:T(128)} %pad_add_fusion.place, f32[64,2,128]{2,1,0:T(2,128)} %copy-done.8, f32[1,128]{1,0:T(1,128)} %bitcast.24, f32[256,128]{1,0:T(8,128)} %get-tuple-element.26.decays, f32[256,128]{1,0:T(8,128)} %get-tuple-element.27.states, ...), custom_call_target="tpu_custom_call" | custom-call | flops 1048576 | bytes 524288 | tf_op jit(solution)/shard_map/final_states/pallas_call | solution.py:202
  147.7 2.0 %collective-permute-start.3 = (bf16[128,128]{1,0:T(8,128)(2,1)}, bf16[128,128]{1,0:T(8,128)(2,1)S(1)}, u32[]{:S(2)}, u32[]{:S(2)}) collective-permute-start(bf16[128,128]{1,0:T(8,128)(2,1)} %get-tuple-element.30), channel_id=1, source_target_pairs={{0,1},{1,0},{2,3},{3,2},{4,5},{5,4},{6,7},{7,6},{8,9},{9,8},{10,11... | collective-permute-start | bytes 98312 | tf_op jit(solution)/shard_map/ppermute | solution.py:469
  149.7 2.3 %collective-permute-start = (f32[1]{0:T(128)}, f32[1]{0:T(128)}, u32[]{:S(2)}, u32[]{:S(2)}) collective-permute-start(f32[1]{0:T(128)} %param.30), channel_id=1, source_target_pairs={{0,1},{1,0},{2,3},{3,2},{4,5},{5,4},{6,7},{7,6},{8,9},{9,8},{10,11... | collective-permute-start | bytes 20 | tf_op jit(solution)/shard_map/ppermute | solution.py:454
  152.6 0.3 collective-permute-done.lam_theirs
  152.9 2.6 %all-to-all-done.1 = bf16[8,272,128]{2,1,0:T(8,128)(2,1)S(1)} async-done(((bf16[8,272,128]{2,1,0:T(8,128)(2,1)}), bf16[8,272,128]{2,1,0:T(8,128)(2,1)S(1)}, u32[]{:S(2)}, u32[]{:S(2)}) %all-to-all-start.1) | async-done | bytes 557088 | tf_op jit(solution)/shard_map/all_to_all | solution.py:463
  155.6 0.8 copy-done.3
  156.4 3.9 %finish.1 = bf16[128,2048]{1,0:T(8,128)(2,1)} custom-call(s32[4]{0:T(128)} %pad_add_fusion.place, f32[1]{0:T(128)S(6)} %copy.19.lam, f32[1]{0:T(128)} %collective-permute-done.lam_theirs, bf16[4,2,272,128]{3,2,1,0:T(8,128)(2,1)} %bitcast.18, f32[1,128]{1,0:T(1,128)} %bitcast.25, bf16[128,128]{1,0:T(8,128)(2,1)} %get-tuple-element.29.lru_mine, ...), custom_call_target="tpu_custom_call" | custom-call | flops 268435456 | bytes 3145728 | tf_op jit(solution)/shard_map/finish/pallas_call | solution.py:371
  160.3 12.1 %all_to_all.20 = bf16[4,32,2048]{2,1,0:T(8,128)(2,1)S(1)} all-to-all(bf16[4,32,2048]{2,1,0:T(8,128)(2,1)} %bitcast.19), channel_id=1, replica_groups=mesh['sp_0'=8,'sp_1'=8,'fs'=4,'tp'=2] {'fs'}, dimensions={0} | all-to-all | bytes 1048576 | tf_op jit(solution)/shard_map/all_to_all | solution.py:483
  172.3 0.7 reduce_sum.12
  (28 shorter events, 0.1 us)
Async XLA Ops:
  0.0 10.4 %copy-start = (bf16[2048,128]{1,0:T(8,128)(2,1)S(1)}, bf16[2048,128]{1,0:T(8,128)(2,1)}, u32[]{:S(2)}) copy-start(bf16[2048,128]{1,0:T(8,128)(2,1)} %param.21) | copy-start | bytes 1572868
  13.5 11.4 %copy-start.10 = (bf16[8,2048]{1,0:T(8,128)(2,1)S(1)}, bf16[8,2048]{1,0:T(8,128)(2,1)}, u32[]{:S(2)}) copy-start(bf16[8,2048]{1,0:T(8,128)(2,1)} %get-tuple-element.20) | copy-start | bytes 98308
  13.5 53.6 %copy-start.5 = (bf16[32,2048]{1,0:T(8,128)(2,1)S(1)}, bf16[32,2048]{1,0:T(8,128)(2,1)}, u32[]{:S(2)}) copy-start(bf16[32,2048]{1,0:T(8,128)(2,1)} %get-tuple-element.19) | copy-start | bytes 393220
  13.5 72.0 %copy-start.6 = (bf16[128,2048]{1,0:T(8,128)(2,1)S(1)}, bf16[128,2048]{1,0:T(8,128)(2,1)}, u32[]{:S(2)}) copy-start(bf16[128,2048]{1,0:T(8,128)(2,1)} %param.32) | copy-start | bytes 1572868
  13.5 90.3 %all-to-all-start = ((bf16[64,64,256]{2,1,0:T(8,128)(2,1)}), bf16[64,64,256]{2,1,0:T(8,128)(2,1)}, u32[]{:S(2)}, u32[]{:S(2)}) async-start(bf16[64,64,256]{2,1,0:T(8,128)(2,1)} %broadcast_in_dim.17), calls=%async_computation | async-start | bytes 4194304 | tf_op jit(solution)/shard_map/all_to_all | solution.py:25
  24.9 60.7 %copy-start.7 = (bf16[128,2048]{1,0:T(8,128)(2,1)S(1)}, bf16[128,2048]{1,0:T(8,128)(2,1)}, u32[]{:S(2)}) copy-start(bf16[128,2048]{1,0:T(8,128)(2,1)} %param.33) | copy-start | bytes 1572868
  24.9 62.6 %copy-start.11 = (f32[128]{0:T(128)S(1)}, f32[128]{0:T(128)}, u32[]{:S(2)}) copy-start(f32[128]{0:T(128)} %param.27) | copy-start | bytes 1540
  24.9 42.2 %collective-permute-start.1 = (bf16[8,2048]{1,0:T(8,128)(2,1)S(1)}, bf16[8,2048]{1,0:T(8,128)(2,1)S(1)}, u32[]{:S(2)}, u32[]{:S(2)}) collective-permute-start(bf16[8,2048]{1,0:T(8,128)(2,1)S(1)} %copy-done.10), channel_id=1, source_target_pairs={{0,8},{8,16},{16,24},{24,32},{32,40},{40,48},{48,56},{56,64},{64,7... | collective-permute-start | bytes 98312 | tf_op jit(solution)/shard_map/ppermute | solution.py:31
  78.5 10.3 %copy-start.1 = (bf16[160,2048]{1,0:T(8,128)(2,1)}, bf16[160,2048]{1,0:T(8,128)(2,1)S(1)}, u32[]{:S(2)}) copy-start(bf16[160,2048]{1,0:T(8,128)(2,1)S(1)} %all_gather.13.mine) | copy-start | bytes 1966084
  78.5 10.3 %collective-permute-start.2 = (bf16[160,2048]{1,0:T(8,128)(2,1)S(1)}, bf16[160,2048]{1,0:T(8,128)(2,1)}, u32[]{:S(2)}, u32[]{:S(2)}) collective-permute-start(bf16[160,2048]{1,0:T(8,128)(2,1)S(1)} %all_gather.13.mine), channel_id=1, source_target_pairs={{0,1},{1,0},{2,3},{3,2},{4,5},{5,4},{6,7},{7,6},{8,9},{9,8},{10,11... | collective-permute-start | bytes 1966088 | tf_op jit(solution)/shard_map/ppermute | solution.py:431
  85.6 22.0 %copy-start.2 = (bf16[256,2048]{1,0:T(8,128)(2,1)}, bf16[256,2048]{1,0:T(8,128)(2,1)S(1)}, u32[]{:S(2)}) copy-start(bf16[256,2048]{1,0:T(8,128)(2,1)S(1)} %constant_dynamic-update-slice_fusion.w_mine) | copy-start | bytes 3145732
  85.6 67.3 %collective-permute-start.4 = (bf16[256,2048]{1,0:T(8,128)(2,1)S(1)}, bf16[256,2048]{1,0:T(8,128)(2,1)S(1)}, u32[]{:S(2)}, u32[]{:S(2)}) collective-permute-start(bf16[256,2048]{1,0:T(8,128)(2,1)S(1)} %constant_dynamic-update-slice_fusion.w_mine), channel_id=1, source_target_pairs={{0,1},{1,0},{2,3},{3,2},{4,5},{5,4},{6,7},{7,6},{8,9},{9,8},{10,11... | collective-permute-start | bytes 3145736 | tf_op jit(solution)/shard_map/ppermute | solution.py:453
  107.6 30.3 %all-to-all-start.2 = ((f32[64,2,128]{2,1,0:T(2,128)}), f32[64,2,128]{2,1,0:T(2,128)S(1)}, u32[]{:S(2)}, u32[]{:S(2)}) async-start(f32[64,2,128]{2,1,0:T(2,128)} %get-tuple-element.25), calls=%async_computation.2 | async-start | bytes 131072 | tf_op jit(solution)/shard_map/all_to_all | solution.py:459
  137.9 8.0 %copy-start.8 = (f32[64,2,128]{2,1,0:T(2,128)}, f32[64,2,128]{2,1,0:T(2,128)S(1)}, u32[]{:S(2)}) copy-start(f32[64,2,128]{2,1,0:T(2,128)S(1)} %all-to-all-done.2.pieces) | copy-start | bytes 196612
  137.9 17.7 %all-to-all-start.1 = ((bf16[8,272,128]{2,1,0:T(8,128)(2,1)}), bf16[8,272,128]{2,1,0:T(8,128)(2,1)S(1)}, u32[]{:S(2)}, u32[]{:S(2)}) async-start(bf16[8,272,128]{2,1,0:T(8,128)(2,1)} %bitcast.20), calls=%async_computation.1 | async-start | bytes 1114112 | tf_op jit(solution)/shard_map/all_to_all | solution.py:463
  147.7 5.3 %collective-permute-start.3 = (bf16[128,128]{1,0:T(8,128)(2,1)}, bf16[128,128]{1,0:T(8,128)(2,1)S(1)}, u32[]{:S(2)}, u32[]{:S(2)}) collective-permute-start(bf16[128,128]{1,0:T(8,128)(2,1)} %get-tuple-element.30), channel_id=1, source_target_pairs={{0,1},{1,0},{2,3},{3,2},{4,5},{5,4},{6,7},{7,6},{8,9},{9,8},{10,11... | collective-permute-start | bytes 98312 | tf_op jit(solution)/shard_map/ppermute | solution.py:469
  149.7 3.2 %collective-permute-start = (f32[1]{0:T(128)}, f32[1]{0:T(128)}, u32[]{:S(2)}, u32[]{:S(2)}) collective-permute-start(f32[1]{0:T(128)} %param.30), channel_id=1, source_target_pairs={{0,1},{1,0},{2,3},{3,2},{4,5},{5,4},{6,7},{7,6},{8,9},{9,8},{10,11... | collective-permute-start | bytes 20 | tf_op jit(solution)/shard_map/ppermute | solution.py:454
  152.9 2.7 %copy-start.4 = (bf16[256,2048]{1,0:T(8,128)(2,1)}, bf16[256,2048]{1,0:T(8,128)(2,1)S(1)}, u32[]{:S(2)}) copy-start(bf16[256,2048]{1,0:T(8,128)(2,1)S(1)} %collective-permute-done.4.w_theirs) | copy-start | bytes 3145732
  152.9 2.7 %copy-start.9 = (bf16[128,128]{1,0:T(8,128)(2,1)}, bf16[128,128]{1,0:T(8,128)(2,1)S(1)}, u32[]{:S(2)}) copy-start(bf16[128,128]{1,0:T(8,128)(2,1)S(1)} %collective-permute-done.3.lru_theirs) | copy-start | bytes 98308
  155.6 0.8 copy-start.3

commit v8 on v7

--- a/solution.py
+++ b/solution.py
@@ -29,6 +29,12 @@
     devices = lax.axis_size(axis)
     pairs = [(i, i + by) for i in range(devices) if 0 <= i + by < devices]
     return lax.ppermute(value, axis, pairs)
+
+
+def pair_combine(earlier, later):
+    decay_early, state_early = earlier
+    decay_late, state_late = later
+    return (decay_early * decay_late, decay_late * state_early + state_late)
 
 
 def vmem():
@@ -140,12 +146,12 @@
     decays[...] = decay
     states[...] = drive
     last = decay.shape[0] - 1
-    both = jnp.concatenate([decay[last:], drive[last:]], axis=0)
-    ends[...] = jnp.broadcast_to(both[None], ends.shape)
+    ends[0:1, :] = decay[last:]
+    ends[1:2, :] = drive[last:]
 
 
 def project(
-    place, mine, theirs, weights, taps, w_recur, w_admit, rate, scale, blocks, fs_count, rows
+    place, mine, theirs, weights, taps, w_recur, w_admit, rate, scale, fs_count, rows
 ):
     channels = scale.shape[1]
     block = jax.ShapeDtypeStruct(scale.shape, jnp.float32)
@@ -156,7 +162,7 @@
             block,
             block,
             block,
-            jax.ShapeDtypeStruct((blocks, 2, channels), jnp.float32),
+            jax.ShapeDtypeStruct((2, channels), jnp.float32),
         ),
         in_specs=[smem()] + [vmem()] * 10,
         out_specs=(vmem(),) * 5,
@@ -170,24 +176,21 @@
 
 
 def states_kernel(
-    place, pieces, start, decays, states, gates, mine, theirs, *, y_count, fs_count, member_rows
+    place, near, far, start, decays, states, gates, mine, theirs, *, fs_count, member_rows
 ):
-    here, core = (place[0] * y_count + place[1], place[3])
-
-    count = pieces.shape[0]
-    decay, state = (pieces[:, 0, :], pieces[:, 1, :])
-    row = lax.broadcasted_iota(jnp.int32, decay.shape, 0)
-    decay = jnp.where(row < here, decay, 1.0)
-    state = jnp.where(row < here, state, 0.0)
-    by = 1
-    while by < count:
-        inside = row >= by
-        decay_before = jnp.where(inside, pltpu.roll(decay, by, 0), 1.0)
-        state_before = jnp.where(inside, pltpu.roll(state, by, 0), 0.0)
-        state = decay * state_before + state
-        decay = decay * decay_before
-        by *= 2
-    entering = decay[count - 1 :] * start[...] + state[count - 1 :]
+    z, y, core = (place[0], place[1], place[3])
+
+    def before(pieces, here):
+        decay, state = (jnp.ones_like(pieces[0, 0:1]), jnp.zeros_like(pieces[0, 1:2]))
+        for k in range(pieces.shape[0]):
+            passed = k < here
+            new_decay, new_state = pair_combine((decay, state), (pieces[k, 0:1], pieces[k, 1:2]))
+            decay = jnp.where(passed, new_decay, decay)
+            state = jnp.where(passed, new_state, state)
+        return decay, state
+
+    decay, state = pair_combine(before(far, z), before(near, y))
+    entering = decay * start[...] + state
     out = ((states[...] + decays[...] * entering) * gates[...]).astype(jnp.bfloat16)
     for f in range(fs_count):
         at = 2 * f * member_rows
@@ -197,20 +200,18 @@
         theirs[f * member_rows : (f + 1) * member_rows] = jnp.where(core == 0, odd, even)
 
 
-def final_states(place, pieces, start, decays, states, gates, y_count, fs_count, member_rows):
+def final_states(place, near, far, start, decays, states, gates, fs_count, member_rows):
     half = jax.ShapeDtypeStruct((fs_count * member_rows, decays.shape[1]), jnp.bfloat16)
     return pl.pallas_call(
-        functools.partial(
-            states_kernel, y_count=y_count, fs_count=fs_count, member_rows=member_rows
-        ),
+        functools.partial(states_kernel, fs_count=fs_count, member_rows=member_rows),
         out_shape=(half, half),
-        in_specs=[smem()] + [vmem()] * 5,
+        in_specs=[smem()] + [vmem()] * 6,
         out_specs=(vmem(), vmem()),
         cost_estimate=pl.CostEstimate(
             flops=1 << 20, bytes_accessed=1 << 19, transcendentals=0
         ),
         name="final_states",
-    )(place, pieces, start, decays, states, gates)
+    )(place, near, far, start, decays, states, gates)
 
 
 def attention_kernel(
@@ -406,7 +407,7 @@
     share_rows = member_rows * tp_count
     member = lax.axis_index("fs")
     core = lax.axis_index("tp")
-    z_count, z = (lax.axis_size("sp_0"), lax.axis_index("sp_0"))
+    z = lax.axis_index("sp_0")
     y_count, y = (lax.axis_size("sp_1"), lax.axis_index("sp_1"))
 
     normed, last_rows = normalized(tokens, norm_gain[None], 8)
@@ -421,11 +422,11 @@
         ],
         axis=1,
     )
-    kv_here, normed = lax.optimization_barrier((kv_here, normed))
-    everyone = from_everyone(kv_here, SP)
-    everyone = everyone.reshape(z_count, y_count * share_rows, kv_here.shape[1])
+    chunk = from_everyone(kv_here, "sp_1").reshape(y_count * share_rows, kv_here.shape[1])
 
     sent = jnp.concatenate([normed, before_rows], axis=0)
+    sent, chunk = lax.optimization_barrier((sent, chunk))
+    everyone = lax.all_gather(chunk, "sp_0")
     mine = lax.all_gather(sent, "fs", axis=0, tiled=True)
     swap = [(0, 1), (1, 0)]
     theirs = lax.ppermute(mine, "tp", swap)
@@ -442,7 +443,6 @@
         w_admit,
         rate[None],
         decay_scale,
-        z_count * y_count,
         fs_count,
         member_rows,
     )
@@ -453,18 +453,20 @@
     w_theirs = lax.ppermute(w_mine, "tp", swap)
     lam_theirs = lax.ppermute(diff_lambda, "tp", swap)
 
-    half_heads = fs_count // 2
-    part = attention(place, group, everyone, None, half_heads, row_count, share_rows)
-    ends, part = lax.optimization_barrier((ends, part))
-    everywhere = lax.all_to_all(ends, SP, split_axis=0, concat_axis=0, tiled=True)
-    carried = attention(place, group, everyone, part, fs_count, row_count, share_rows)
+    near = lax.all_gather(ends, "sp_1")
+    row = (near[0, 0], near[0, 1])
+    for k in range(1, y_count):
+        row = pair_combine(row, (near[k, 0], near[k, 1]))
+    far = from_everyone(jnp.stack(row), "sp_0")
+
+    carried = attention(place, group, everyone, None, fs_count, row_count, share_rows)
     lines, half_rows = carried.shape[2:]
     carried = carried.reshape(fs_count * tp_count, lines, half_rows)
     packed = lax.all_to_all(carried, ("fs", "tp"), split_axis=0, concat_axis=0, tiled=True)
     packed = packed.reshape(fs_count, tp_count, lines, half_rows)
 
     lru_mine, lru_other = final_states(
-        place, everywhere, init_state[None], decays, states, gates, y_count, fs_count, member_rows
+        place, near, far, init_state[None], decays, states, gates, fs_count, member_rows
     )
     lru_theirs = lax.ppermute(lru_other, "tp", swap)
 

time: 174 us -> 149 us (0.86)
  the two profiles are of different devices: /device:TPU:1 before, /device:TPU:448 now
where the time goes in v8:
time: 149 us; the launch traced here: 148 us
  blocking collectives  56.2 us (38%)
  Pallas kernels  29 us (19%)
  starting transfers between devices  27.8 us (19%)
  between operations  14.2 us (10%)
  waiting for transfers between devices  12.4 us (8%)
  local copies, waits for them, and re-layouts  5.05 us (3%)
  other arithmetic  1.95 us (1%)
    pallas_call x1, Pallas kernels, attention(): pl.pallas_call(functools.partial(attention_kernel, block_rows=block_rows,...  17.4 us
    all_gather x1, blocking collectives, body(): mine = lax.all_gather(sent, 'fs', axis=0, tiled=True)  14.1 us
    all_gather x1, blocking collectives, body(): near = lax.all_gather(ends, 'sp_1')  13.7 us
    all_gather x1, blocking collectives, body(): group = lax.all_gather(query_t, 'fs')  13.2 us
    all_to_all x1, blocking collectives, body(): lax.all_to_all(partial, 'fs', split_axis=0, concat_axis=0, tiled=True)  12.9 us
    all_to_all x2, starting transfers between devices, from_everyone(): return lax.all_to_all(copies, axis, split_axis=0, concat_axis=0, tiled=True)  11.7 us
    ppermute x1, waiting for transfers between devices, passed_along(): return lax.ppermute(value, axis, pairs)  5.18 us
    pallas_call x1, Pallas kernels, project(): pl.pallas_call(functools.partial(project_kernel, fs_count=fs_count, membe...  4.3 us
  transfers between devices with their start and end apart: 9, of which 4 were waited for; matrix products, arithmetic and copies ran while one was open for 3% of the time, Pallas kernels for 16%

profile of v8, /device:TPU:448, one launch (start us, length us, event | category | flops | bytes accessed | tf_op | source)
XLA Modules:
  0.0 148.2 jit_solution(11632638816638451091)
XLA Ops:
  6.5 1.8 %normalized.1 = (bf16[32,2048]{1,0:T(8,128)(2,1)}, bf16[8,2048]{1,0:T(8,128)(2,1)}) custom-call(bf16[32,2048]{1,0:T(8,128)(2,1)} %tokens.1, f32[1,2048]{1,0:T(1,128)} %bitcast.29), custom_call_target="tpu_custom_call" | custom-call | flops 262144 | bytes 262144 | tf_op jit(solution)/shard_map/normalized/pallas_call | solution.py:60
  8.3 2.3 %all_gather.24 = bf16[64,2048]{1,0:T(8,128)(2,1)S(1)} all-gather(bf16[32,2048]{1,0:T(8,128)(2,1)} %get-tuple-element.16), channel_id=1, replica_groups=mesh['sp_0'=8,'sp_1'=8,'fs'=4,'tp'=2] {'tp'}, dimensions={0}, use_global_device_ids=true | all-gather | bytes 393216 | tf_op jit(solution)/shard_map/all_gather | solution.py:417
  10.9 1.3 convolution_convert_fusion.1
  12.1 0.7 broadcast_in_dim.19
  12.9 7.2 %all-to-all-start = ((bf16[8,64,256]{2,1,0:T(8,128)(2,1)}), bf16[8,64,256]{2,1,0:T(8,128)(2,1)S(1)}, u32[]{:S(2)}, u32[]{:S(2)}) async-start(bf16[8,64,256]{2,1,0:T(8,128)(2,1)} %broadcast_in_dim.19), calls=%async_computation | async-start | bytes 524288 | tf_op jit(solution)/shard_map/all_to_all | solution.py:25
  20.2 3.9 %collective-permute-start.1 = (bf16[8,2048]{1,0:T(8,128)(2,1)S(1)}, bf16[8,2048]{1,0:T(8,128)(2,1)S(1)}, u32[]{:S(2)}, u32[]{:S(2)}) collective-permute-start(bf16[8,2048]{1,0:T(8,128)(2,1)S(1)} %copy-done.10), channel_id=1, source_target_pairs={{0,8},{8,16},{16,24},{24,32},{32,40},{40,48},{48,56},{56,64},{64,7... | collective-permute-start | bytes 98312 | tf_op jit(solution)/shard_map/ppermute | solution.py:31
  24.0 5.2 %collective-permute-done.1 = bf16[8,2048]{1,0:T(8,128)(2,1)S(1)} collective-permute-done((bf16[8,2048]{1,0:T(8,128)(2,1)S(1)}, bf16[8,2048]{1,0:T(8,128)(2,1)S(1)}, u32[]{:S(2)}, u32[]{:S(2)}) %collective-permute-start.1) | collective-permute-done | bytes 32800 | tf_op jit(solution)/shard_map/ppermute | solution.py:31
  29.2 3.4 %all-to-all-done = bf16[8,64,256]{2,1,0:T(8,128)(2,1)S(1)} async-done(((bf16[8,64,256]{2,1,0:T(8,128)(2,1)}), bf16[8,64,256]{2,1,0:T(8,128)(2,1)S(1)}, u32[]{:S(2)}, u32[]{:S(2)}) %all-to-all-start) | async-done | bytes 262176 | tf_op jit(solution)/shard_map/all_to_all | solution.py:25
  32.6 0.7 copy-done.4
  33.4 14.1 %all_gather.25.mine = bf16[160,2048]{1,0:T(8,128)(2,1)S(1)} all-gather(bf16[40,2048]{1,0:T(8,128)(2,1)S(1)} %pad_maximum_fusion), channel_id=1, replica_groups=mesh['sp_0'=8,'sp_1'=8,'fs'=4,'tp'=2] {'fs'}, dimensions={0}, use_global_device_ids=true | all-gather | bytes 819200 | tf_op jit(solution)/shard_map/all_gather | solution.py:430
  47.5 1.9 %collective-permute-start.2 = (bf16[160,2048]{1,0:T(8,128)(2,1)S(1)}, bf16[160,2048]{1,0:T(8,128)(2,1)}, u32[]{:S(2)}, u32[]{:S(2)}) collective-permute-start(bf16[160,2048]{1,0:T(8,128)(2,1)S(1)} %all_gather.25.mine), channel_id=1, source_target_pairs={{0,1},{1,0},{2,3},{3,2},{4,5},{5,4},{6,7},{7,6},{8,9},{9,8},{10,11... | collective-permute-start | bytes 1966088 | tf_op jit(solution)/shard_map/ppermute | solution.py:432
  49.4 1.1 constant_dynamic-update-slice_fusion.1
  50.5 1.1 constant_dynamic-update-slice_fusion.w_mine
  51.6 2.4 %collective-permute-start.4 = (bf16[256,2048]{1,0:T(8,128)(2,1)S(1)}, bf16[256,2048]{1,0:T(8,128)(2,1)S(1)}, u32[]{:S(2)}, u32[]{:S(2)}) collective-permute-start(bf16[256,2048]{1,0:T(8,128)(2,1)S(1)} %constant_dynamic-update-slice_fusion.w_mine), channel_id=1, source_target_pairs={{0,1},{1,0},{2,3},{3,2},{4,5},{5,4},{6,7},{7,6},{8,9},{9,8},{10,11... | collective-permute-start | bytes 3145736 | tf_op jit(solution)/shard_map/ppermute | solution.py:453
  54.0 0.6 pad_add_fusion.place
  54.6 0.6 fusion.10.rate
  55.2 4.3 %project.1 = (bf16[128,256]{1,0:T(8,128)(2,1)}, f32[256,128]{1,0:T(8,128)}, f32[256,128]{1,0:T(8,128)}, f32[256,128]{1,0:T(8,128)}, f32[2,128]{1,0:T(2,128)}) custom-call(s32[4]{0:T(128)} %pad_add_fusion.place, bf16[160,2048]{1,0:T(8,128)(2,1)} %copy-done.1, bf16[160,2048]{1,0:T(8,128)(2,1)} %collective-permute-done.2.theirs, bf16[2048,128]{1,0:T(8,128)(2,1)} %w_query.1, ...), custom_call_target="tpu_custom_call" | custom-call | flops 402653184 | bytes 4194304 | tf_op jit(solution)/shard_map/project/pallas_call | solution.py:158
  59.5 13.7 %all-gather.3.near = f32[8,2,128]{2,1,0:T(2,128)S(1)} all-gather(f32[1,2,128]{2,1,0:T(2,128)} %bitcast.30), channel_id=4, replica_groups=mesh['sp_0'=8,'sp_1'=8,'fs'=4,'tp'=2] {'sp_1'}, dimensions={0}, use_global_device_ids=true | all-gather | bytes 9216 | tf_op jit(solution)/shard_map/all_gather | solution.py:456
  73.2 0.6 broadcast_in_dim.22
  73.8 4.5 %all-to-all-start.2 = ((f32[8,2,128]{2,1,0:T(2,128)}), f32[8,2,128]{2,1,0:T(2,128)S(1)}, u32[]{:S(2)}, u32[]{:S(2)}) async-start(f32[8,2,128]{2,1,0:T(2,128)} %broadcast_in_dim.22), calls=%async_computation.2 | async-start | bytes 16384 | tf_op jit(solution)/shard_map/all_to_all | solution.py:25
  78.3 13.2 %all-gather = bf16[512,256]{1,0:T(8,128)(2,1)} all-gather(bf16[128,256]{1,0:T(8,128)(2,1)} %get-tuple-element.19), channel_id=2, replica_groups=mesh['sp_0'=8,'sp_1'=8,'fs'=4,'tp'=2] {'fs'}, dimensions={0}, use_global_device_ids=true | all-gather | bytes 327680 | tf_op jit(solution)/shard_map/all_gather | solution.py:450
  91.5 17.4 %attention.1 = bf16[4,2,272,128]{3,2,1,0:T(8,128)(2,1)} custom-call(s32[4]{0:T(128)} %pad_add_fusion.place, bf16[4,128,256]{2,1,0:T(8,128)(2,1)} %bitcast.28, bf16[8,512,256]{2,1,0:T(8,128)(2,1)} %bitcast.33), custom_call_target="tpu_custom_call" | custom-call | flops 4294967296 | bytes 4194304 | tf_op jit(solution)/shard_map/attention/pallas_call | solution.py:316
  109.0 3.5 %all-to-all-start.1 = ((bf16[8,272,128]{2,1,0:T(8,128)(2,1)}), bf16[8,272,128]{2,1,0:T(8,128)(2,1)S(1)}, u32[]{:S(2)}, u32[]{:S(2)}) async-start(bf16[8,272,128]{2,1,0:T(8,128)(2,1)} %bitcast.27), calls=%async_computation.1 | async-start | bytes 1114112 | tf_op jit(solution)/shard_map/all_to_all | solution.py:465
  112.5 1.8 %final_states.1 = (bf16[128,128]{1,0:T(8,128)(2,1)}, bf16[128,128]{1,0:T(8,128)(2,1)}) custom-call(s32[4]{0:T(128)} %pad_add_fusion.place, f32[8,2,128]{2,1,0:T(2,128)} %copy-done.7, f32[8,2,128]{2,1,0:T(2,128)} %copy-done.9, f32[1,128]{1,0:T(1,128)} %bitcast.31, f32[256,128]{1,0:T(8,128)} %get-tuple-element.22.decays, f32[256,128]{1,0:T(8,128)} %get-tuple-element.23.states, ...), custom_call_target="tpu_custom_call" | custom-call | flops 1048576 | bytes 524288 | tf_op jit(solution)/shard_map/final_states/pallas_call | solution.py:205
  114.3 2.3 %collective-permute-start.3 = (bf16[128,128]{1,0:T(8,128)(2,1)}, bf16[128,128]{1,0:T(8,128)(2,1)S(1)}, u32[]{:S(2)}, u32[]{:S(2)}) collective-permute-start(bf16[128,128]{1,0:T(8,128)(2,1)} %get-tuple-element.26), channel_id=1, source_target_pairs={{0,1},{1,0},{2,3},{3,2},{4,5},{5,4},{6,7},{7,6},{8,9},{9,8},{10,11... | collective-permute-start | bytes 98312 | tf_op jit(solution)/shard_map/ppermute | solution.py:471
  116.6 2.0 %collective-permute-start = (f32[1]{0:T(128)}, f32[1]{0:T(128)}, u32[]{:S(2)}, u32[]{:S(2)}) collective-permute-start(f32[1]{0:T(128)} %param.30), channel_id=1, source_target_pairs={{0,1},{1,0},{2,3},{3,2},{4,5},{5,4},{6,7},{7,6},{8,9},{9,8},{10,11... | collective-permute-start | bytes 20 | tf_op jit(solution)/shard_map/ppermute | solution.py:454
  119.3 0.5 collective-permute-done.lam_theirs
  119.8 3.3 %all-to-all-done.1 = bf16[8,272,128]{2,1,0:T(8,128)(2,1)S(1)} async-done(((bf16[8,272,128]{2,1,0:T(8,128)(2,1)}), bf16[8,272,128]{2,1,0:T(8,128)(2,1)S(1)}, u32[]{:S(2)}, u32[]{:S(2)}) %all-to-all-start.1) | async-done | bytes 557088 | tf_op jit(solution)/shard_map/all_to_all | solution.py:465
  123.1 0.8 copy-done.3
  123.9 3.8 %finish.1 = bf16[128,2048]{1,0:T(8,128)(2,1)} custom-call(s32[4]{0:T(128)} %pad_add_fusion.place, f32[1]{0:T(128)S(6)} %copy.19.lam, f32[1]{0:T(128)} %collective-permute-done.lam_theirs, bf16[4,2,272,128]{3,2,1,0:T(8,128)(2,1)} %bitcast.24, f32[1,128]{1,0:T(1,128)} %bitcast.32, bf16[128,128]{1,0:T(8,128)(2,1)} %get-tuple-element.25.lru_mine, ...), custom_call_target="tpu_custom_call" | custom-call | flops 268435456 | bytes 3145728 | tf_op jit(solution)/shard_map/finish/pallas_call | solution.py:372
  127.7 12.9 %all_to_all.20 = bf16[4,32,2048]{2,1,0:T(8,128)(2,1)S(1)} all-to-all(bf16[4,32,2048]{2,1,0:T(8,128)(2,1)} %bitcast.25), channel_id=1, replica_groups=mesh['sp_0'=8,'sp_1'=8,'fs'=4,'tp'=2] {'fs'}, dimensions={0} | all-to-all | bytes 1048576 | tf_op jit(solution)/shard_map/all_to_all | solution.py:485
  140.6 0.7 reduce_sum.12
  (35 shorter events, 0.4 us)
Async XLA Ops:
  6.5 4.1 %copy-start = (bf16[2048,128]{1,0:T(8,128)(2,1)S(1)}, bf16[2048,128]{1,0:T(8,128)(2,1)}, u32[]{:S(2)}) copy-start(bf16[2048,128]{1,0:T(8,128)(2,1)} %param.21) | copy-start | bytes 1572868
  8.3 11.8 %copy-start.10 = (bf16[8,2048]{1,0:T(8,128)(2,1)S(1)}, bf16[8,2048]{1,0:T(8,128)(2,1)}, u32[]{:S(2)}) copy-start(bf16[8,2048]{1,0:T(8,128)(2,1)} %get-tuple-element.17) | copy-start | bytes 98308
  8.3 20.9 %copy-start.6 = (bf16[32,2048]{1,0:T(8,128)(2,1)S(1)}, bf16[32,2048]{1,0:T(8,128)(2,1)}, u32[]{:S(2)}) copy-start(bf16[32,2048]{1,0:T(8,128)(2,1)} %get-tuple-element.16) | copy-start | bytes 393220
  12.9 41.7 %copy-start.11 = (f32[128]{0:T(128)S(1)}, f32[128]{0:T(128)}, u32[]{:S(2)}) copy-start(f32[128]{0:T(128)} %param.27) | copy-start | bytes 1540
  12.9 19.8 %all-to-all-start = ((bf16[8,64,256]{2,1,0:T(8,128)(2,1)}), bf16[8,64,256]{2,1,0:T(8,128)(2,1)S(1)}, u32[]{:S(2)}, u32[]{:S(2)}) async-start(bf16[8,64,256]{2,1,0:T(8,128)(2,1)} %broadcast_in_dim.19), calls=%async_computation | async-start | bytes 524288 | tf_op jit(solution)/shard_map/all_to_all | solution.py:25
  20.1 71.4 %all-gather.6.cloned.1.call-start = ((), (), s32[]{:S(2)}) async-start(), calls=%async_computation.4 | async-start | bytes 2359296 | tf_op jit(solution)/shard_map/all_gather | solution.py:429
  20.2 9.1 %collective-permute-start.1 = (bf16[8,2048]{1,0:T(8,128)(2,1)S(1)}, bf16[8,2048]{1,0:T(8,128)(2,1)S(1)}, u32[]{:S(2)}, u32[]{:S(2)}) collective-permute-start(bf16[8,2048]{1,0:T(8,128)(2,1)S(1)} %copy-done.10), channel_id=1, source_target_pairs={{0,8},{8,16},{16,24},{24,32},{32,40},{40,48},{48,56},{56,64},{64,7... | collective-permute-start | bytes 98312 | tf_op jit(solution)/shard_map/ppermute | solution.py:31
  32.6 0.7 copy-start.4
  47.5 7.7 %copy-start.1 = (bf16[160,2048]{1,0:T(8,128)(2,1)}, bf16[160,2048]{1,0:T(8,128)(2,1)S(1)}, u32[]{:S(2)}) copy-start(bf16[160,2048]{1,0:T(8,128)(2,1)S(1)} %all_gather.25.mine) | copy-start | bytes 1966084
  47.5 7.7 %collective-permute-start.2 = (bf16[160,2048]{1,0:T(8,128)(2,1)S(1)}, bf16[160,2048]{1,0:T(8,128)(2,1)}, u32[]{:S(2)}, u32[]{:S(2)}) collective-permute-start(bf16[160,2048]{1,0:T(8,128)(2,1)S(1)} %all_gather.25.mine), channel_id=1, source_target_pairs={{0,1},{1,0},{2,3},{3,2},{4,5},{5,4},{6,7},{7,6},{8,9},{9,8},{10,11... | collective-permute-start | bytes 1966088 | tf_op jit(solution)/shard_map/ppermute | solution.py:432
  51.6 57.3 %copy-start.2 = (bf16[256,2048]{1,0:T(8,128)(2,1)}, bf16[256,2048]{1,0:T(8,128)(2,1)S(1)}, u32[]{:S(2)}) copy-start(bf16[256,2048]{1,0:T(8,128)(2,1)S(1)} %constant_dynamic-update-slice_fusion.w_mine) | copy-start | bytes 3145732
  51.6 68.2 %collective-permute-start.4 = (bf16[256,2048]{1,0:T(8,128)(2,1)S(1)}, bf16[256,2048]{1,0:T(8,128)(2,1)S(1)}, u32[]{:S(2)}, u32[]{:S(2)}) collective-permute-start(bf16[256,2048]{1,0:T(8,128)(2,1)S(1)} %constant_dynamic-update-slice_fusion.w_mine), channel_id=1, source_target_pairs={{0,1},{1,0},{2,3},{3,2},{4,5},{5,4},{6,7},{7,6},{8,9},{9,8},{10,11... | collective-permute-start | bytes 3145736 | tf_op jit(solution)/shard_map/ppermute | solution.py:453
  73.1 35.8 %copy-start.7 = (f32[8,2,128]{2,1,0:T(2,128)}, f32[8,2,128]{2,1,0:T(2,128)S(1)}, u32[]{:S(2)}) copy-start(f32[8,2,128]{2,1,0:T(2,128)S(1)} %all-gather.3.near) | copy-start | bytes 24580
  73.8 35.2 %all-to-all-start.2 = ((f32[8,2,128]{2,1,0:T(2,128)}), f32[8,2,128]{2,1,0:T(2,128)S(1)}, u32[]{:S(2)}, u32[]{:S(2)}) async-start(f32[8,2,128]{2,1,0:T(2,128)} %broadcast_in_dim.22), calls=%async_computation.2 | async-start | bytes 16384 | tf_op jit(solution)/shard_map/all_to_all | solution.py:25
  109.0 3.6 %copy-start.9 = (f32[8,2,128]{2,1,0:T(2,128)}, f32[8,2,128]{2,1,0:T(2,128)S(1)}, u32[]{:S(2)}) copy-start(f32[8,2,128]{2,1,0:T(2,128)S(1)} %all-to-all-done.2.far) | copy-start | bytes 24580
  109.0 14.1 %all-to-all-start.1 = ((bf16[8,272,128]{2,1,0:T(8,128)(2,1)}), bf16[8,272,128]{2,1,0:T(8,128)(2,1)S(1)}, u32[]{:S(2)}, u32[]{:S(2)}) async-start(bf16[8,272,128]{2,1,0:T(8,128)(2,1)} %bitcast.27), calls=%async_computation.1 | async-start | bytes 1114112 | tf_op jit(solution)/shard_map/all_to_all | solution.py:465
  114.3 5.5 %collective-permute-start.3 = (bf16[128,128]{1,0:T(8,128)(2,1)}, bf16[128,128]{1,0:T(8,128)(2,1)S(1)}, u32[]{:S(2)}, u32[]{:S(2)}) collective-permute-start(bf16[128,128]{1,0:T(8,128)(2,1)} %get-tuple-element.26), channel_id=1, source_target_pairs={{0,1},{1,0},{2,3},{3,2},{4,5},{5,4},{6,7},{7,6},{8,9},{9,8},{10,11... | collective-permute-start | bytes 98312 | tf_op jit(solution)/shard_map/ppermute | solution.py:471
  116.6 3.2 %collective-permute-start = (f32[1]{0:T(128)}, f32[1]{0:T(128)}, u32[]{:S(2)}, u32[]{:S(2)}) collective-permute-start(f32[1]{0:T(128)} %param.30), channel_id=1, source_target_pairs={{0,1},{1,0},{2,3},{3,2},{4,5},{5,4},{6,7},{7,6},{8,9},{9,8},{10,11... | collective-permute-start | bytes 20 | tf_op jit(solution)/shard_map/ppermute | solution.py:454
  119.8 3.3 %copy-start.5 = (bf16[256,2048]{1,0:T(8,128)(2,1)}, bf16[256,2048]{1,0:T(8,128)(2,1)S(1)}, u32[]{:S(2)}) copy-start(bf16[256,2048]{1,0:T(8,128)(2,1)S(1)} %collective-permute-done.4.w_theirs) | copy-start | bytes 3145732
  119.8 3.3 %copy-start.8 = (bf16[128,128]{1,0:T(8,128)(2,1)}, bf16[128,128]{1,0:T(8,128)(2,1)S(1)}, u32[]{:S(2)}) copy-start(bf16[128,128]{1,0:T(8,128)(2,1)S(1)} %collective-permute-done.3.lru_theirs) | copy-start | bytes 98308
  123.1 0.8 copy-start.3
Sparse Core Ops, SparseCore 0:
  33.5 36.7 all-gather.5

commit v9 on v7

--- a/solution.py
+++ b/solution.py
@@ -216,15 +216,18 @@
 def attention_kernel(
     place, group, kv_far, *refs, block_rows, part_rows, start, stop
 ):
-    packed, query, peak, values, value_t, kv, arrivals = refs[-7:]
+    packed, query, peak, values, value_t, kv, arrivals = refs[-10:-3]
+    plain, held = (refs[-3], refs[-2:])
     heads = stop - start
     _, size, rows = group.shape
-    chunk_keys = kv.shape[1]
+    z_count, chunk_keys, _ = kv.shape
     z, y, member = (place[0], place[1], place[2])
 
     def arrival(at):
         return pltpu.make_async_copy(kv_far.at[at], kv.at[at], arrivals.at[at])
 
+    queries = pltpu.make_async_copy(group.at[pl.ds(start, heads)], plain, arrivals.at[z_count])
+    queries.start()
     arrival(z).start()
 
     def begin(at, _):
@@ -232,12 +235,6 @@
         return 0
 
     lax.fori_loop(0, z, begin, 0)
-    line = lax.broadcasted_iota(jnp.int32, (size, rows), 0)
-    for h in range(heads):
-        whole = group[start + h]
-        zero = jnp.zeros_like(whole)
-        query[2 * h] = jnp.where(line < size // 2, whole, zero)
-        query[2 * h + 1] = jnp.where(line < size // 2, zero, whole)
     peak[...] = jnp.full(peak.shape, far_below, jnp.float32)
     value_t[size:, :] = jnp.ones((16, chunk_keys), jnp.bfloat16)
     values[...] = jnp.zeros(values.shape, jnp.float32)
@@ -261,9 +258,11 @@
             found = jnp.dot(keys, query[i], preferred_element_type=jnp.float32)
             return jnp.where(visible, found, far_below) if masked else found
 
-        scores = scores_of(0)
+        held[0][...] = scores_of(0)
         for i in range(2 * heads):
-            following = scores_of(i + 1) if i + 1 < 2 * heads else None
+            if i + 1 < 2 * heads:
+                held[(i + 1) % 2][...] = scores_of(i + 1)
+            scores = held[i % 2][...]
             old = peak[i]
             now = jnp.maximum(old, jnp.max(scores, axis=0, keepdims=True))
             expos = jnp.exp2(scores - now)
@@ -274,8 +273,14 @@
             values[i] = values[i] * fade + jnp.dot(
                 value_t[...], expos.astype(jnp.bfloat16), preferred_element_type=jnp.float32
             )
-            scores = following
-
+
+    queries.wait()
+    line = lax.broadcasted_iota(jnp.int32, (size, rows), 0)
+    for h in range(heads):
+        whole = plain[h]
+        zero = jnp.zeros_like(whole)
+        query[2 * h] = jnp.where(line < size // 2, whole, zero)
+        query[2 * h + 1] = jnp.where(line < size // 2, zero, whole)
     one_chunk(z, True)
 
     def earlier(at, _):
@@ -317,7 +322,7 @@
             attention_kernel, block_rows=block_rows, part_rows=part_rows, start=start, stop=stop
         ),
         out_shape=jax.ShapeDtypeStruct((stop, 2, 2 * size + 16, rows // 2), jnp.bfloat16),
-        in_specs=[smem(), vmem(), anywhere()] + [vmem()] * (start > 0),
+        in_specs=[smem(), anywhere(), anywhere()] + [vmem()] * (start > 0),
         out_specs=vmem(),
         scratch_shapes=[
             pltpu.VMEM((2 * heads, size, rows), jnp.bfloat16),
@@ -325,7 +330,10 @@
             pltpu.VMEM((2 * heads, size + 16, rows), jnp.float32),
             pltpu.VMEM((size + 16, chunk_keys), jnp.bfloat16),
             pltpu.VMEM(kv.shape, kv.dtype),
-            pltpu.SemaphoreType.DMA((z_count,)),
+            pltpu.SemaphoreType.DMA((z_count + 1,)),
+            pltpu.VMEM((heads, size, rows), jnp.bfloat16),
+            pltpu.VMEM((chunk_keys, rows), jnp.float32),
+            pltpu.VMEM((chunk_keys, rows), jnp.float32),
         ],
         cost_estimate=pl.CostEstimate(
             flops=4 * 2 * heads * rows * keys * size,
@@ -453,11 +461,9 @@
     w_theirs = lax.ppermute(w_mine, "tp", swap)
     lam_theirs = lax.ppermute(diff_lambda, "tp", swap)
 
-    half_heads = fs_count // 2
-    part = attention(place, group, everyone, None, half_heads, row_count, share_rows)
-    ends, part = lax.optimization_barrier((ends, part))
     everywhere = lax.all_to_all(ends, SP, split_axis=0, concat_axis=0, tiled=True)
-    carried = attention(place, group, everyone, part, fs_count, row_count, share_rows)
+
+    carried = attention(place, group, everyone, None, fs_count, row_count, share_rows)
     lines, half_rows = carried.shape[2:]
     carried = carried.reshape(fs_count * tp_count, lines, half_rows)
     packed = lax.all_to_all(carried, ("fs", "tp"), split_axis=0, concat_axis=0, tiled=True)

time: 174 us -> 166 us (0.954)
  the two profiles are of different devices: /device:TPU:1 before, /device:TPU:448 now
where the time goes in v9:
time: 166 us; the launch traced here: 163 us
  waiting for transfers between devices  50.1 us (30%)
  blocking collectives  42.5 us (26%)
  starting transfers between devices  36.2 us (22%)
  Pallas kernels  27.6 us (17%)
  local copies, waits for them, and re-layouts  2.49 us (2%)
  other arithmetic  1.97 us (1%)
    ppermute x1, waiting for transfers between devices, passed_along(): return lax.ppermute(value, axis, pairs)  46.4 us
    pallas_call x1, Pallas kernels, attention(): pl.pallas_call(functools.partial(attention_kernel, block_rows=block_rows,...  15.9 us
    all_gather x1, blocking collectives, body(): mine = lax.all_gather(sent, 'fs', axis=0, tiled=True)  14.2 us
    all_gather x1, blocking collectives, body(): group = lax.all_gather(query_t, 'fs')  13.2 us
    all_to_all x1, blocking collectives, body(): lax.all_to_all(partial, 'fs', split_axis=0, concat_axis=0, tiled=True)  12.9 us
    all_to_all x1, starting transfers between devices, from_everyone(): return lax.all_to_all(copies, axis, split_axis=0, concat_axis=0, tiled=True)  10.9 us
    all_to_all x1, starting transfers between devices, body(): lax.all_to_all(ends, SP, split_axis=0, concat_axis=0, tiled=True)  9.6 us
    pallas_call x1, Pallas kernels, project(): pl.pallas_call(functools.partial(project_kernel, fs_count=fs_count, membe...  4.27 us
  transfers between devices with their start and end apart: 8, of which 3 were waited for; matrix products, arithmetic and copies ran while one was open for 1% of the time, Pallas kernels for 13%

profile of v9, /device:TPU:448, one launch (start us, length us, event | category | flops | bytes accessed | tf_op | source)
XLA Modules:
  0.0 163.3 jit_solution(2610464081816818100)
XLA Ops:
  0.0 1.8 %normalized.1 = (bf16[32,2048]{1,0:T(8,128)(2,1)}, bf16[8,2048]{1,0:T(8,128)(2,1)}) custom-call(bf16[32,2048]{1,0:T(8,128)(2,1)} %tokens.1, f32[1,2048]{1,0:T(1,128)} %bitcast.22), custom_call_target="tpu_custom_call" | custom-call | flops 262144 | bytes 262144 | tf_op jit(solution)/shard_map/normalized/pallas_call | solution.py:54
  1.8 2.2 %all_gather.12 = bf16[64,2048]{1,0:T(8,128)(2,1)S(1)} all-gather(bf16[32,2048]{1,0:T(8,128)(2,1)} %get-tuple-element.17), channel_id=1, replica_groups=mesh['sp_0'=8,'sp_1'=8,'fs'=4,'tp'=2] {'tp'}, dimensions={0}, use_global_device_ids=true | all-gather | bytes 393216 | tf_op jit(solution)/shard_map/all_gather | solution.py:424
  4.0 0.2 convolution_convert_fusion
  4.2 1.3 convolution_convert_fusion.1
  5.5 1.5 broadcast_in_dim.17
  7.0 10.9 %all-to-all-start = ((bf16[64,64,256]{2,1,0:T(8,128)(2,1)}), bf16[64,64,256]{2,1,0:T(8,128)(2,1)}, u32[]{:S(2)}, u32[]{:S(2)}) async-start(bf16[64,64,256]{2,1,0:T(8,128)(2,1)} %broadcast_in_dim.17), calls=%async_computation | async-start | bytes 4194304 | tf_op jit(solution)/shard_map/all_to_all | solution.py:25
  17.9 0.0 copy-start.7
  18.0 0.0 copy-start.11
  18.0 3.5 %collective-permute-start.1 = (bf16[8,2048]{1,0:T(8,128)(2,1)S(1)}, bf16[8,2048]{1,0:T(8,128)(2,1)S(1)}, u32[]{:S(2)}, u32[]{:S(2)}) collective-permute-start(bf16[8,2048]{1,0:T(8,128)(2,1)S(1)} %copy-done.10), channel_id=1, source_target_pairs={{0,8},{8,16},{16,24},{24,32},{32,40},{40,48},{48,56},{56,64},{64,7... | collective-permute-start | bytes 98312 | tf_op jit(solution)/shard_map/ppermute | solution.py:31
  21.5 46.4 %collective-permute-done.1 = bf16[8,2048]{1,0:T(8,128)(2,1)S(1)} collective-permute-done((bf16[8,2048]{1,0:T(8,128)(2,1)S(1)}, bf16[8,2048]{1,0:T(8,128)(2,1)S(1)}, u32[]{:S(2)}, u32[]{:S(2)}) %collective-permute-start.1) | collective-permute-done | bytes 32800 | tf_op jit(solution)/shard_map/ppermute | solution.py:31
  67.9 14.2 %all_gather.13.mine = bf16[160,2048]{1,0:T(8,128)(2,1)S(1)} all-gather(bf16[40,2048]{1,0:T(8,128)(2,1)S(1)} %pad_maximum_fusion), channel_id=1, replica_groups=mesh['sp_0'=8,'sp_1'=8,'fs'=4,'tp'=2] {'fs'}, dimensions={0}, use_global_device_ids=true | all-gather | bytes 819200 | tf_op jit(solution)/shard_map/all_gather | solution.py:437
  82.1 1.9 %collective-permute-start.2 = (bf16[160,2048]{1,0:T(8,128)(2,1)S(1)}, bf16[160,2048]{1,0:T(8,128)(2,1)}, u32[]{:S(2)}, u32[]{:S(2)}) collective-permute-start(bf16[160,2048]{1,0:T(8,128)(2,1)S(1)} %all_gather.13.mine), channel_id=1, source_target_pairs={{0,1},{1,0},{2,3},{3,2},{4,5},{5,4},{6,7},{7,6},{8,9},{9,8},{10,11... | collective-permute-start | bytes 1966088 | tf_op jit(solution)/shard_map/ppermute | solution.py:439
  84.1 2.4 %collective-permute-start.4 = (bf16[256,2048]{1,0:T(8,128)(2,1)S(1)}, bf16[256,2048]{1,0:T(8,128)(2,1)S(1)}, u32[]{:S(2)}, u32[]{:S(2)}) collective-permute-start(bf16[256,2048]{1,0:T(8,128)(2,1)S(1)} %constant_dynamic-update-slice_fusion.w_mine), channel_id=1, source_target_pairs={{0,1},{1,0},{2,3},{3,2},{4,5},{5,4},{6,7},{7,6},{8,9},{9,8},{10,11... | collective-permute-start | bytes 3145736 | tf_op jit(solution)/shard_map/ppermute | solution.py:461
  86.5 0.5 fusion.1.rate
  87.1 0.7 pad_add_fusion.place
  87.8 4.3 %project.1 = (bf16[128,256]{1,0:T(8,128)(2,1)}, f32[256,128]{1,0:T(8,128)}, f32[256,128]{1,0:T(8,128)}, f32[256,128]{1,0:T(8,128)}, f32[64,2,128]{2,1,0:T(2,128)}) custom-call(s32[4]{0:T(128)} %pad_add_fusion.place, bf16[160,2048]{1,0:T(8,128)(2,1)} %copy-done.1, bf16[160,2048]{1,0:T(8,128)(2,1)} %collective-permute-done.2.theirs, ...), custom_call_target="tpu_custom_call" | custom-call | flops 402653184 | bytes 4194304 | tf_op jit(solution)/shard_map/project/pallas_call | solution.py:152
  92.0 13.2 %all-gather = bf16[512,256]{1,0:T(8,128)(2,1)} all-gather(bf16[128,256]{1,0:T(8,128)(2,1)} %get-tuple-element.19), channel_id=2, replica_groups=mesh['sp_0'=8,'sp_1'=8,'fs'=4,'tp'=2] {'fs'}, dimensions={0}, use_global_device_ids=true | all-gather | bytes 327680 | tf_op jit(solution)/shard_map/all_gather | solution.py:458
  105.2 0.0 all-to-all-done
  105.2 9.6 %all-to-all-start.2 = ((f32[64,2,128]{2,1,0:T(2,128)}), f32[64,2,128]{2,1,0:T(2,128)S(1)}, u32[]{:S(2)}, u32[]{:S(2)}) async-start(f32[64,2,128]{2,1,0:T(2,128)} %get-tuple-element.21), calls=%async_computation.2 | async-start | bytes 131072 | tf_op jit(solution)/shard_map/all_to_all | solution.py:464
  114.8 15.9 %attention.1 = bf16[4,2,272,128]{3,2,1,0:T(8,128)(2,1)} custom-call(s32[4]{0:T(128)} %pad_add_fusion.place, bf16[4,128,256]{2,1,0:T(8,128)(2,1)} %bitcast.21, bf16[8,512,256]{2,1,0:T(8,128)(2,1)} %bitcast.7.kv_far), custom_call_target="tpu_custom_call" | custom-call | flops 4294967296 | bytes 4194304 | tf_op jit(solution)/shard_map/attention/pallas_call | solution.py:320
  130.8 3.5 %all-to-all-start.1 = ((bf16[8,272,128]{2,1,0:T(8,128)(2,1)}), bf16[8,272,128]{2,1,0:T(8,128)(2,1)S(1)}, u32[]{:S(2)}, u32[]{:S(2)}) async-start(bf16[8,272,128]{2,1,0:T(8,128)(2,1)} %bitcast.20), calls=%async_computation.1 | async-start | bytes 1114112 | tf_op jit(solution)/shard_map/all_to_all | solution.py:469
  134.4 1.8 %final_states.1 = (bf16[128,128]{1,0:T(8,128)(2,1)}, bf16[128,128]{1,0:T(8,128)(2,1)}) custom-call(s32[4]{0:T(128)} %pad_add_fusion.place, f32[64,2,128]{2,1,0:T(2,128)} %copy-done.8, f32[1,128]{1,0:T(1,128)} %bitcast.23, f32[256,128]{1,0:T(8,128)} %get-tuple-element.22.decays, f32[256,128]{1,0:T(8,128)} %get-tuple-element.23.states, ...), custom_call_target="tpu_custom_call" | custom-call | flops 1048576 | bytes 524288 | tf_op jit(solution)/shard_map/final_states/pallas_call | solution.py:202
  136.2 2.3 %collective-permute-start.3 = (bf16[128,128]{1,0:T(8,128)(2,1)}, bf16[128,128]{1,0:T(8,128)(2,1)S(1)}, u32[]{:S(2)}, u32[]{:S(2)}) collective-permute-start(bf16[128,128]{1,0:T(8,128)(2,1)} %get-tuple-element.26), channel_id=1, source_target_pairs={{0,1},{1,0},{2,3},{3,2},{4,5},{5,4},{6,7},{7,6},{8,9},{9,8},{10,11... | collective-permute-start | bytes 98312 | tf_op jit(solution)/shard_map/ppermute | solution.py:475
  138.5 2.0 %collective-permute-start = (f32[1]{0:T(128)}, f32[1]{0:T(128)}, u32[]{:S(2)}, u32[]{:S(2)}) collective-permute-start(f32[1]{0:T(128)} %param.30), channel_id=1, source_target_pairs={{0,1},{1,0},{2,3},{3,2},{4,5},{5,4},{6,7},{7,6},{8,9},{9,8},{10,11... | collective-permute-start | bytes 20 | tf_op jit(solution)/shard_map/ppermute | solution.py:462
  141.1 0.5 collective-permute-done.lam_theirs
  141.6 0.0 collective-permute-done.3.lru_theirs
  141.6 0.0 collective-permute-done.4.w_theirs
  141.7 3.3 %all-to-all-done.1 = bf16[8,272,128]{2,1,0:T(8,128)(2,1)S(1)} async-done(((bf16[8,272,128]{2,1,0:T(8,128)(2,1)}), bf16[8,272,128]{2,1,0:T(8,128)(2,1)S(1)}, u32[]{:S(2)}, u32[]{:S(2)}) %all-to-all-start.1) | async-done | bytes 557088 | tf_op jit(solution)/shard_map/all_to_all | solution.py:469
  144.9 0.8 copy-done.3
  145.8 3.9 %finish.1 = bf16[128,2048]{1,0:T(8,128)(2,1)} custom-call(s32[4]{0:T(128)} %pad_add_fusion.place, f32[1]{0:T(128)S(6)} %copy.19.lam, f32[1]{0:T(128)} %collective-permute-done.lam_theirs, bf16[4,2,272,128]{3,2,1,0:T(8,128)(2,1)} %bitcast.18, f32[1,128]{1,0:T(1,128)} %bitcast.24, bf16[128,128]{1,0:T(8,128)(2,1)} %get-tuple-element.25.lru_mine, ...), custom_call_target="tpu_custom_call" | custom-call | flops 268435456 | bytes 3145728 | tf_op jit(solution)/shard_map/finish/pallas_call | solution.py:379
  149.6 12.9 %all_to_all.20 = bf16[4,32,2048]{2,1,0:T(8,128)(2,1)S(1)} all-to-all(bf16[4,32,2048]{2,1,0:T(8,128)(2,1)} %bitcast.19), channel_id=1, replica_groups=mesh['sp_0'=8,'sp_1'=8,'fs'=4,'tp'=2] {'fs'}, dimensions={0} | all-to-all | bytes 1048576 | tf_op jit(solution)/shard_map/all_to_all | solution.py:489
  162.5 0.7 reduce_sum.12
  (27 shorter events, 0.1 us)
Async XLA Ops:
  0.0 4.0 %copy-start = (bf16[2048,128]{1,0:T(8,128)(2,1)S(1)}, bf16[2048,128]{1,0:T(8,128)(2,1)}, u32[]{:S(2)}) copy-start(bf16[2048,128]{1,0:T(8,128)(2,1)} %param.21) | copy-start | bytes 1572868
  7.0 11.0 %copy-start.10 = (bf16[8,2048]{1,0:T(8,128)(2,1)S(1)}, bf16[8,2048]{1,0:T(8,128)(2,1)}, u32[]{:S(2)}) copy-start(bf16[8,2048]{1,0:T(8,128)(2,1)} %get-tuple-element.18) | copy-start | bytes 98308
  7.0 60.8 %copy-start.5 = (bf16[32,2048]{1,0:T(8,128)(2,1)S(1)}, bf16[32,2048]{1,0:T(8,128)(2,1)}, u32[]{:S(2)}) copy-start(bf16[32,2048]{1,0:T(8,128)(2,1)} %get-tuple-element.17) | copy-start | bytes 393220
  7.0 77.0 %copy-start.6 = (bf16[128,2048]{1,0:T(8,128)(2,1)S(1)}, bf16[128,2048]{1,0:T(8,128)(2,1)}, u32[]{:S(2)}) copy-start(bf16[128,2048]{1,0:T(8,128)(2,1)} %param.32) | copy-start | bytes 1572868
  7.0 98.2 %all-to-all-start = ((bf16[64,64,256]{2,1,0:T(8,128)(2,1)}), bf16[64,64,256]{2,1,0:T(8,128)(2,1)}, u32[]{:S(2)}, u32[]{:S(2)}) async-start(bf16[64,64,256]{2,1,0:T(8,128)(2,1)} %broadcast_in_dim.17), calls=%async_computation | async-start | bytes 4194304 | tf_op jit(solution)/shard_map/all_to_all | solution.py:25
  17.9 66.1 %copy-start.7 = (bf16[128,2048]{1,0:T(8,128)(2,1)S(1)}, bf16[128,2048]{1,0:T(8,128)(2,1)}, u32[]{:S(2)}) copy-start(bf16[128,2048]{1,0:T(8,128)(2,1)} %param.33) | copy-start | bytes 1572868
  18.0 68.6 %copy-start.11 = (f32[128]{0:T(128)S(1)}, f32[128]{0:T(128)}, u32[]{:S(2)}) copy-start(f32[128]{0:T(128)} %param.27) | copy-start | bytes 1540
  18.0 49.9 %collective-permute-start.1 = (bf16[8,2048]{1,0:T(8,128)(2,1)S(1)}, bf16[8,2048]{1,0:T(8,128)(2,1)S(1)}, u32[]{:S(2)}, u32[]{:S(2)}) collective-permute-start(bf16[8,2048]{1,0:T(8,128)(2,1)S(1)} %copy-done.10), channel_id=1, source_target_pairs={{0,8},{8,16},{16,24},{24,32},{32,40},{40,48},{48,56},{56,64},{64,7... | collective-permute-start | bytes 98312 | tf_op jit(solution)/shard_map/ppermute | solution.py:31
  82.1 5.7 %copy-start.1 = (bf16[160,2048]{1,0:T(8,128)(2,1)}, bf16[160,2048]{1,0:T(8,128)(2,1)S(1)}, u32[]{:S(2)}) copy-start(bf16[160,2048]{1,0:T(8,128)(2,1)S(1)} %all_gather.13.mine) | copy-start | bytes 1966084
  82.1 5.7 %collective-permute-start.2 = (bf16[160,2048]{1,0:T(8,128)(2,1)S(1)}, bf16[160,2048]{1,0:T(8,128)(2,1)}, u32[]{:S(2)}, u32[]{:S(2)}) collective-permute-start(bf16[160,2048]{1,0:T(8,128)(2,1)S(1)} %all_gather.13.mine), channel_id=1, source_target_pairs={{0,1},{1,0},{2,3},{3,2},{4,5},{5,4},{6,7},{7,6},{8,9},{9,8},{10,11... | collective-permute-start | bytes 1966088 | tf_op jit(solution)/shard_map/ppermute | solution.py:439
  84.1 46.7 %copy-start.2 = (bf16[256,2048]{1,0:T(8,128)(2,1)}, bf16[256,2048]{1,0:T(8,128)(2,1)S(1)}, u32[]{:S(2)}) copy-start(bf16[256,2048]{1,0:T(8,128)(2,1)S(1)} %constant_dynamic-update-slice_fusion.w_mine) | copy-start | bytes 3145732
  84.1 57.5 %collective-permute-start.4 = (bf16[256,2048]{1,0:T(8,128)(2,1)S(1)}, bf16[256,2048]{1,0:T(8,128)(2,1)S(1)}, u32[]{:S(2)}, u32[]{:S(2)}) collective-permute-start(bf16[256,2048]{1,0:T(8,128)(2,1)S(1)} %constant_dynamic-update-slice_fusion.w_mine), channel_id=1, source_target_pairs={{0,1},{1,0},{2,3},{3,2},{4,5},{5,4},{6,7},{7,6},{8,9},{9,8},{10,11... | collective-permute-start | bytes 3145736 | tf_op jit(solution)/shard_map/ppermute | solution.py:461
  105.2 25.5 %all-to-all-start.2 = ((f32[64,2,128]{2,1,0:T(2,128)}), f32[64,2,128]{2,1,0:T(2,128)S(1)}, u32[]{:S(2)}, u32[]{:S(2)}) async-start(f32[64,2,128]{2,1,0:T(2,128)} %get-tuple-element.21), calls=%async_computation.2 | async-start | bytes 131072 | tf_op jit(solution)/shard_map/all_to_all | solution.py:464
  130.8 3.6 %copy-start.8 = (f32[64,2,128]{2,1,0:T(2,128)}, f32[64,2,128]{2,1,0:T(2,128)S(1)}, u32[]{:S(2)}) copy-start(f32[64,2,128]{2,1,0:T(2,128)S(1)} %all-to-all-done.2.pieces) | copy-start | bytes 196612
  130.8 14.1 %all-to-all-start.1 = ((bf16[8,272,128]{2,1,0:T(8,128)(2,1)}), bf16[8,272,128]{2,1,0:T(8,128)(2,1)S(1)}, u32[]{:S(2)}, u32[]{:S(2)}) async-start(bf16[8,272,128]{2,1,0:T(8,128)(2,1)} %bitcast.20), calls=%async_computation.1 | async-start | bytes 1114112 | tf_op jit(solution)/shard_map/all_to_all | solution.py:469
  136.2 5.5 %collective-permute-start.3 = (bf16[128,128]{1,0:T(8,128)(2,1)}, bf16[128,128]{1,0:T(8,128)(2,1)S(1)}, u32[]{:S(2)}, u32[]{:S(2)}) collective-permute-start(bf16[128,128]{1,0:T(8,128)(2,1)} %get-tuple-element.26), channel_id=1, source_target_pairs={{0,1},{1,0},{2,3},{3,2},{4,5},{5,4},{6,7},{7,6},{8,9},{9,8},{10,11... | collective-permute-start | bytes 98312 | tf_op jit(solution)/shard_map/ppermute | solution.py:475
  138.5 3.2 %collective-permute-start = (f32[1]{0:T(128)}, f32[1]{0:T(128)}, u32[]{:S(2)}, u32[]{:S(2)}) collective-permute-start(f32[1]{0:T(128)} %param.30), channel_id=1, source_target_pairs={{0,1},{1,0},{2,3},{3,2},{4,5},{5,4},{6,7},{7,6},{8,9},{9,8},{10,11... | collective-permute-start | bytes 20 | tf_op jit(solution)/shard_map/ppermute | solution.py:462
  141.6 3.3 %copy-start.9 = (bf16[128,128]{1,0:T(8,128)(2,1)}, bf16[128,128]{1,0:T(8,128)(2,1)S(1)}, u32[]{:S(2)}) copy-start(bf16[128,128]{1,0:T(8,128)(2,1)S(1)} %collective-permute-done.3.lru_theirs) | copy-start | bytes 98308
  141.6 3.3 %copy-start.4 = (bf16[256,2048]{1,0:T(8,128)(2,1)}, bf16[256,2048]{1,0:T(8,128)(2,1)S(1)}, u32[]{:S(2)}) copy-start(bf16[256,2048]{1,0:T(8,128)(2,1)S(1)} %collective-permute-done.4.w_theirs) | copy-start | bytes 3145732
  144.9 0.8 copy-start.3

commit v10 on v7

--- a/solution.py
+++ b/solution.py
@@ -216,7 +216,8 @@
 def attention_kernel(
     place, group, kv_far, *refs, block_rows, part_rows, start, stop
 ):
-    packed, query, peak, values, value_t, kv, arrivals = refs[-7:]
+    packed, query, peak, values, value_t, kv, arrivals = refs[-9:-2]
+    held = refs[-2:]
     heads = stop - start
     _, size, rows = group.shape
     chunk_keys = kv.shape[1]
@@ -261,9 +262,11 @@
             found = jnp.dot(keys, query[i], preferred_element_type=jnp.float32)
             return jnp.where(visible, found, far_below) if masked else found
 
-        scores = scores_of(0)
+        held[0][...] = scores_of(0)
         for i in range(2 * heads):
-            following = scores_of(i + 1) if i + 1 < 2 * heads else None
+            if i + 1 < 2 * heads:
+                held[(i + 1) % 2][...] = scores_of(i + 1)
+            scores = held[i % 2][...]
             old = peak[i]
             now = jnp.maximum(old, jnp.max(scores, axis=0, keepdims=True))
             expos = jnp.exp2(scores - now)
@@ -274,7 +277,6 @@
             values[i] = values[i] * fade + jnp.dot(
                 value_t[...], expos.astype(jnp.bfloat16), preferred_element_type=jnp.float32
             )
-            scores = following
 
     one_chunk(z, True)
 
@@ -326,6 +328,8 @@
             pltpu.VMEM((size + 16, chunk_keys), jnp.bfloat16),
             pltpu.VMEM(kv.shape, kv.dtype),
             pltpu.SemaphoreType.DMA((z_count,)),
+            pltpu.VMEM((chunk_keys, rows), jnp.float32),
+            pltpu.VMEM((chunk_keys, rows), jnp.float32),
         ],
         cost_estimate=pl.CostEstimate(
             flops=4 * 2 * heads * rows * keys * size,
@@ -453,11 +457,9 @@
     w_theirs = lax.ppermute(w_mine, "tp", swap)
     lam_theirs = lax.ppermute(diff_lambda, "tp", swap)
 
-    half_heads = fs_count // 2
-    part = attention(place, group, everyone, None, half_heads, row_count, share_rows)
-    ends, part = lax.optimization_barrier((ends, part))
     everywhere = lax.all_to_all(ends, SP, split_axis=0, concat_axis=0, tiled=True)
-    carried = attention(place, group, everyone, part, fs_count, row_count, share_rows)
+
+    carried = attention(place, group, everyone, None, fs_count, row_count, share_rows)
     lines, half_rows = carried.shape[2:]
     carried = carried.reshape(fs_count * tp_count, lines, half_rows)
     packed = lax.all_to_all(carried, ("fs", "tp"), split_axis=0, concat_axis=0, tiled=True)

time: 174 us -> 166 us (0.954)
  the two profiles are of different devices: /device:TPU:1 before, /device:TPU:448 now
where the time goes in v10:
time: 166 us; the launch traced here: 163 us
  waiting for transfers between devices  50.1 us (30%)
  blocking collectives  42.5 us (26%)
  starting transfers between devices  36.2 us (22%)
  Pallas kernels  27.8 us (17%)
  local copies, waits for them, and re-layouts  2.49 us (2%)
  other arithmetic  1.97 us (1%)
    ppermute x1, waiting for transfers between devices, passed_along(): return lax.ppermute(value, axis, pairs)  46.4 us
    pallas_call x1, Pallas kernels, attention(): pl.pallas_call(functools.partial(attention_kernel, block_rows=block_rows,...  16.1 us
    all_gather x1, blocking collectives, body(): mine = lax.all_gather(sent, 'fs', axis=0, tiled=True)  14.2 us
    all_gather x1, blocking collectives, body(): group = lax.all_gather(query_t, 'fs')  13.2 us
    all_to_all x1, blocking collectives, body(): lax.all_to_all(partial, 'fs', split_axis=0, concat_axis=0, tiled=True)  12.9 us
    all_to_all x1, starting transfers between devices, from_everyone(): return lax.all_to_all(copies, axis, split_axis=0, concat_axis=0, tiled=True)  10.9 us
    all_to_all x1, starting transfers between devices, body(): lax.all_to_all(ends, SP, split_axis=0, concat_axis=0, tiled=True)  9.6 us
    pallas_call x1, Pallas kernels, project(): pl.pallas_call(functools.partial(project_kernel, fs_count=fs_count, membe...  4.27 us
  transfers between devices with their start and end apart: 8, of which 3 were waited for; matrix products, arithmetic and copies ran while one was open for 1% of the time, Pallas kernels for 14%

profile of v10, /device:TPU:448, one launch (start us, length us, event | category | flops | bytes accessed | tf_op | source)
XLA Modules:
  0.0 163.5 jit_solution(8575960524565518773)
XLA Ops:
  0.0 1.8 %normalized.1 = (bf16[32,2048]{1,0:T(8,128)(2,1)}, bf16[8,2048]{1,0:T(8,128)(2,1)}) custom-call(bf16[32,2048]{1,0:T(8,128)(2,1)} %tokens.1, f32[1,2048]{1,0:T(1,128)} %bitcast.22), custom_call_target="tpu_custom_call" | custom-call | flops 262144 | bytes 262144 | tf_op jit(solution)/shard_map/normalized/pallas_call | solution.py:54
  1.8 2.2 %all_gather.12 = bf16[64,2048]{1,0:T(8,128)(2,1)S(1)} all-gather(bf16[32,2048]{1,0:T(8,128)(2,1)} %get-tuple-element.17), channel_id=1, replica_groups=mesh['sp_0'=8,'sp_1'=8,'fs'=4,'tp'=2] {'tp'}, dimensions={0}, use_global_device_ids=true | all-gather | bytes 393216 | tf_op jit(solution)/shard_map/all_gather | solution.py:420
  4.0 0.2 convolution_convert_fusion
  4.2 1.3 convolution_convert_fusion.1
  5.5 1.5 broadcast_in_dim.17
  7.0 10.9 %all-to-all-start = ((bf16[64,64,256]{2,1,0:T(8,128)(2,1)}), bf16[64,64,256]{2,1,0:T(8,128)(2,1)}, u32[]{:S(2)}, u32[]{:S(2)}) async-start(bf16[64,64,256]{2,1,0:T(8,128)(2,1)} %broadcast_in_dim.17), calls=%async_computation | async-start | bytes 4194304 | tf_op jit(solution)/shard_map/all_to_all | solution.py:25
  17.9 0.0 copy-start.7
  18.0 0.0 copy-start.11
  18.0 3.5 %collective-permute-start.1 = (bf16[8,2048]{1,0:T(8,128)(2,1)S(1)}, bf16[8,2048]{1,0:T(8,128)(2,1)S(1)}, u32[]{:S(2)}, u32[]{:S(2)}) collective-permute-start(bf16[8,2048]{1,0:T(8,128)(2,1)S(1)} %copy-done.10), channel_id=1, source_target_pairs={{0,8},{8,16},{16,24},{24,32},{32,40},{40,48},{48,56},{56,64},{64,7... | collective-permute-start | bytes 98312 | tf_op jit(solution)/shard_map/ppermute | solution.py:31
  21.5 46.4 %collective-permute-done.1 = bf16[8,2048]{1,0:T(8,128)(2,1)S(1)} collective-permute-done((bf16[8,2048]{1,0:T(8,128)(2,1)S(1)}, bf16[8,2048]{1,0:T(8,128)(2,1)S(1)}, u32[]{:S(2)}, u32[]{:S(2)}) %collective-permute-start.1) | collective-permute-done | bytes 32800 | tf_op jit(solution)/shard_map/ppermute | solution.py:31
  67.9 14.2 %all_gather.13.mine = bf16[160,2048]{1,0:T(8,128)(2,1)S(1)} all-gather(bf16[40,2048]{1,0:T(8,128)(2,1)S(1)} %pad_maximum_fusion), channel_id=1, replica_groups=mesh['sp_0'=8,'sp_1'=8,'fs'=4,'tp'=2] {'fs'}, dimensions={0}, use_global_device_ids=true | all-gather | bytes 819200 | tf_op jit(solution)/shard_map/all_gather | solution.py:433
  82.1 1.9 %collective-permute-start.2 = (bf16[160,2048]{1,0:T(8,128)(2,1)S(1)}, bf16[160,2048]{1,0:T(8,128)(2,1)}, u32[]{:S(2)}, u32[]{:S(2)}) collective-permute-start(bf16[160,2048]{1,0:T(8,128)(2,1)S(1)} %all_gather.13.mine), channel_id=1, source_target_pairs={{0,1},{1,0},{2,3},{3,2},{4,5},{5,4},{6,7},{7,6},{8,9},{9,8},{10,11... | collective-permute-start | bytes 1966088 | tf_op jit(solution)/shard_map/ppermute | solution.py:435
  84.1 2.4 %collective-permute-start.4 = (bf16[256,2048]{1,0:T(8,128)(2,1)S(1)}, bf16[256,2048]{1,0:T(8,128)(2,1)S(1)}, u32[]{:S(2)}, u32[]{:S(2)}) collective-permute-start(bf16[256,2048]{1,0:T(8,128)(2,1)S(1)} %constant_dynamic-update-slice_fusion.w_mine), channel_id=1, source_target_pairs={{0,1},{1,0},{2,3},{3,2},{4,5},{5,4},{6,7},{7,6},{8,9},{9,8},{10,11... | collective-permute-start | bytes 3145736 | tf_op jit(solution)/shard_map/ppermute | solution.py:457
  86.5 0.5 fusion.1.rate
  87.1 0.7 pad_add_fusion.place
  87.8 4.3 %project.1 = (bf16[128,256]{1,0:T(8,128)(2,1)}, f32[256,128]{1,0:T(8,128)}, f32[256,128]{1,0:T(8,128)}, f32[256,128]{1,0:T(8,128)}, f32[64,2,128]{2,1,0:T(2,128)}) custom-call(s32[4]{0:T(128)} %pad_add_fusion.place, bf16[160,2048]{1,0:T(8,128)(2,1)} %copy-done.1, bf16[160,2048]{1,0:T(8,128)(2,1)} %collective-permute-done.2.theirs, ...), custom_call_target="tpu_custom_call" | custom-call | flops 402653184 | bytes 4194304 | tf_op jit(solution)/shard_map/project/pallas_call | solution.py:152
  92.0 13.2 %all-gather = bf16[512,256]{1,0:T(8,128)(2,1)} all-gather(bf16[128,256]{1,0:T(8,128)(2,1)} %get-tuple-element.19), channel_id=2, replica_groups=mesh['sp_0'=8,'sp_1'=8,'fs'=4,'tp'=2] {'fs'}, dimensions={0}, use_global_device_ids=true | all-gather | bytes 327680 | tf_op jit(solution)/shard_map/all_gather | solution.py:454
  105.2 0.0 all-to-all-done
  105.2 9.6 %all-to-all-start.2 = ((f32[64,2,128]{2,1,0:T(2,128)}), f32[64,2,128]{2,1,0:T(2,128)S(1)}, u32[]{:S(2)}, u32[]{:S(2)}) async-start(f32[64,2,128]{2,1,0:T(2,128)} %get-tuple-element.21), calls=%async_computation.2 | async-start | bytes 131072 | tf_op jit(solution)/shard_map/all_to_all | solution.py:460
  114.8 16.1 %attention.1 = bf16[4,2,272,128]{3,2,1,0:T(8,128)(2,1)} custom-call(s32[4]{0:T(128)} %pad_add_fusion.place, bf16[4,128,256]{2,1,0:T(8,128)(2,1)} %bitcast.21, bf16[8,512,256]{2,1,0:T(8,128)(2,1)} %bitcast.7.kv_far), custom_call_target="tpu_custom_call" | custom-call | flops 4294967296 | bytes 4194304 | tf_op jit(solution)/shard_map/attention/pallas_call | solution.py:317
  131.0 3.5 %all-to-all-start.1 = ((bf16[8,272,128]{2,1,0:T(8,128)(2,1)}), bf16[8,272,128]{2,1,0:T(8,128)(2,1)S(1)}, u32[]{:S(2)}, u32[]{:S(2)}) async-start(bf16[8,272,128]{2,1,0:T(8,128)(2,1)} %bitcast.20), calls=%async_computation.1 | async-start | bytes 1114112 | tf_op jit(solution)/shard_map/all_to_all | solution.py:465
  134.6 1.8 %final_states.1 = (bf16[128,128]{1,0:T(8,128)(2,1)}, bf16[128,128]{1,0:T(8,128)(2,1)}) custom-call(s32[4]{0:T(128)} %pad_add_fusion.place, f32[64,2,128]{2,1,0:T(2,128)} %copy-done.8, f32[1,128]{1,0:T(1,128)} %bitcast.23, f32[256,128]{1,0:T(8,128)} %get-tuple-element.22.decays, f32[256,128]{1,0:T(8,128)} %get-tuple-element.23.states, ...), custom_call_target="tpu_custom_call" | custom-call | flops 1048576 | bytes 524288 | tf_op jit(solution)/shard_map/final_states/pallas_call | solution.py:202
  136.4 2.3 %collective-permute-start.3 = (bf16[128,128]{1,0:T(8,128)(2,1)}, bf16[128,128]{1,0:T(8,128)(2,1)S(1)}, u32[]{:S(2)}, u32[]{:S(2)}) collective-permute-start(bf16[128,128]{1,0:T(8,128)(2,1)} %get-tuple-element.26), channel_id=1, source_target_pairs={{0,1},{1,0},{2,3},{3,2},{4,5},{5,4},{6,7},{7,6},{8,9},{9,8},{10,11... | collective-permute-start | bytes 98312 | tf_op jit(solution)/shard_map/ppermute | solution.py:471
  138.7 2.0 %collective-permute-start = (f32[1]{0:T(128)}, f32[1]{0:T(128)}, u32[]{:S(2)}, u32[]{:S(2)}) collective-permute-start(f32[1]{0:T(128)} %param.30), channel_id=1, source_target_pairs={{0,1},{1,0},{2,3},{3,2},{4,5},{5,4},{6,7},{7,6},{8,9},{9,8},{10,11... | collective-permute-start | bytes 20 | tf_op jit(solution)/shard_map/ppermute | solution.py:458
  141.3 0.5 collective-permute-done.lam_theirs
  141.8 0.0 collective-permute-done.3.lru_theirs
  141.8 0.0 collective-permute-done.4.w_theirs
  141.9 3.3 %all-to-all-done.1 = bf16[8,272,128]{2,1,0:T(8,128)(2,1)S(1)} async-done(((bf16[8,272,128]{2,1,0:T(8,128)(2,1)}), bf16[8,272,128]{2,1,0:T(8,128)(2,1)S(1)}, u32[]{:S(2)}, u32[]{:S(2)}) %all-to-all-start.1) | async-done | bytes 557088 | tf_op jit(solution)/shard_map/all_to_all | solution.py:465
  145.1 0.8 copy-done.3
  146.0 3.9 %finish.1 = bf16[128,2048]{1,0:T(8,128)(2,1)} custom-call(s32[4]{0:T(128)} %pad_add_fusion.place, f32[1]{0:T(128)S(6)} %copy.19.lam, f32[1]{0:T(128)} %collective-permute-done.lam_theirs, bf16[4,2,272,128]{3,2,1,0:T(8,128)(2,1)} %bitcast.18, f32[1,128]{1,0:T(1,128)} %bitcast.24, bf16[128,128]{1,0:T(8,128)(2,1)} %get-tuple-element.25.lru_mine, ...), custom_call_target="tpu_custom_call" | custom-call | flops 268435456 | bytes 3145728 | tf_op jit(solution)/shard_map/finish/pallas_call | solution.py:375
  149.8 12.9 %all_to_all.20 = bf16[4,32,2048]{2,1,0:T(8,128)(2,1)S(1)} all-to-all(bf16[4,32,2048]{2,1,0:T(8,128)(2,1)} %bitcast.19), channel_id=1, replica_groups=mesh['sp_0'=8,'sp_1'=8,'fs'=4,'tp'=2] {'fs'}, dimensions={0} | all-to-all | bytes 1048576 | tf_op jit(solution)/shard_map/all_to_all | solution.py:485
  162.7 0.7 reduce_sum.12
  (27 shorter events, 0.1 us)
Async XLA Ops:
  0.0 4.0 %copy-start = (bf16[2048,128]{1,0:T(8,128)(2,1)S(1)}, bf16[2048,128]{1,0:T(8,128)(2,1)}, u32[]{:S(2)}) copy-start(bf16[2048,128]{1,0:T(8,128)(2,1)} %param.21) | copy-start | bytes 1572868
  7.0 11.0 %copy-start.10 = (bf16[8,2048]{1,0:T(8,128)(2,1)S(1)}, bf16[8,2048]{1,0:T(8,128)(2,1)}, u32[]{:S(2)}) copy-start(bf16[8,2048]{1,0:T(8,128)(2,1)} %get-tuple-element.18) | copy-start | bytes 98308
  7.0 60.8 %copy-start.5 = (bf16[32,2048]{1,0:T(8,128)(2,1)S(1)}, bf16[32,2048]{1,0:T(8,128)(2,1)}, u32[]{:S(2)}) copy-start(bf16[32,2048]{1,0:T(8,128)(2,1)} %get-tuple-element.17) | copy-start | bytes 393220
  7.0 77.0 %copy-start.6 = (bf16[128,2048]{1,0:T(8,128)(2,1)S(1)}, bf16[128,2048]{1,0:T(8,128)(2,1)}, u32[]{:S(2)}) copy-start(bf16[128,2048]{1,0:T(8,128)(2,1)} %param.32) | copy-start | bytes 1572868
  7.0 98.2 %all-to-all-start = ((bf16[64,64,256]{2,1,0:T(8,128)(2,1)}), bf16[64,64,256]{2,1,0:T(8,128)(2,1)}, u32[]{:S(2)}, u32[]{:S(2)}) async-start(bf16[64,64,256]{2,1,0:T(8,128)(2,1)} %broadcast_in_dim.17), calls=%async_computation | async-start | bytes 4194304 | tf_op jit(solution)/shard_map/all_to_all | solution.py:25
  17.9 66.1 %copy-start.7 = (bf16[128,2048]{1,0:T(8,128)(2,1)S(1)}, bf16[128,2048]{1,0:T(8,128)(2,1)}, u32[]{:S(2)}) copy-start(bf16[128,2048]{1,0:T(8,128)(2,1)} %param.33) | copy-start | bytes 1572868
  18.0 68.6 %copy-start.11 = (f32[128]{0:T(128)S(1)}, f32[128]{0:T(128)}, u32[]{:S(2)}) copy-start(f32[128]{0:T(128)} %param.27) | copy-start | bytes 1540
  18.0 49.9 %collective-permute-start.1 = (bf16[8,2048]{1,0:T(8,128)(2,1)S(1)}, bf16[8,2048]{1,0:T(8,128)(2,1)S(1)}, u32[]{:S(2)}, u32[]{:S(2)}) collective-permute-start(bf16[8,2048]{1,0:T(8,128)(2,1)S(1)} %copy-done.10), channel_id=1, source_target_pairs={{0,8},{8,16},{16,24},{24,32},{32,40},{40,48},{48,56},{56,64},{64,7... | collective-permute-start | bytes 98312 | tf_op jit(solution)/shard_map/ppermute | solution.py:31
  82.1 5.7 %copy-start.1 = (bf16[160,2048]{1,0:T(8,128)(2,1)}, bf16[160,2048]{1,0:T(8,128)(2,1)S(1)}, u32[]{:S(2)}) copy-start(bf16[160,2048]{1,0:T(8,128)(2,1)S(1)} %all_gather.13.mine) | copy-start | bytes 1966084
  82.1 5.7 %collective-permute-start.2 = (bf16[160,2048]{1,0:T(8,128)(2,1)S(1)}, bf16[160,2048]{1,0:T(8,128)(2,1)}, u32[]{:S(2)}, u32[]{:S(2)}) collective-permute-start(bf16[160,2048]{1,0:T(8,128)(2,1)S(1)} %all_gather.13.mine), channel_id=1, source_target_pairs={{0,1},{1,0},{2,3},{3,2},{4,5},{5,4},{6,7},{7,6},{8,9},{9,8},{10,11... | collective-permute-start | bytes 1966088 | tf_op jit(solution)/shard_map/ppermute | solution.py:435
  84.1 46.9 %copy-start.2 = (bf16[256,2048]{1,0:T(8,128)(2,1)}, bf16[256,2048]{1,0:T(8,128)(2,1)S(1)}, u32[]{:S(2)}) copy-start(bf16[256,2048]{1,0:T(8,128)(2,1)S(1)} %constant_dynamic-update-slice_fusion.w_mine) | copy-start | bytes 3145732
  84.1 57.7 %collective-permute-start.4 = (bf16[256,2048]{1,0:T(8,128)(2,1)S(1)}, bf16[256,2048]{1,0:T(8,128)(2,1)S(1)}, u32[]{:S(2)}, u32[]{:S(2)}) collective-permute-start(bf16[256,2048]{1,0:T(8,128)(2,1)S(1)} %constant_dynamic-update-slice_fusion.w_mine), channel_id=1, source_target_pairs={{0,1},{1,0},{2,3},{3,2},{4,5},{5,4},{6,7},{7,6},{8,9},{9,8},{10,11... | collective-permute-start | bytes 3145736 | tf_op jit(solution)/shard_map/ppermute | solution.py:457
  105.2 25.7 %all-to-all-start.2 = ((f32[64,2,128]{2,1,0:T(2,128)}), f32[64,2,128]{2,1,0:T(2,128)S(1)}, u32[]{:S(2)}, u32[]{:S(2)}) async-start(f32[64,2,128]{2,1,0:T(2,128)} %get-tuple-element.21), calls=%async_computation.2 | async-start | bytes 131072 | tf_op jit(solution)/shard_map/all_to_all | solution.py:460
  131.0 3.6 %copy-start.8 = (f32[64,2,128]{2,1,0:T(2,128)}, f32[64,2,128]{2,1,0:T(2,128)S(1)}, u32[]{:S(2)}) copy-start(f32[64,2,128]{2,1,0:T(2,128)S(1)} %all-to-all-done.2.pieces) | copy-start | bytes 196612
  131.0 14.1 %all-to-all-start.1 = ((bf16[8,272,128]{2,1,0:T(8,128)(2,1)}), bf16[8,272,128]{2,1,0:T(8,128)(2,1)S(1)}, u32[]{:S(2)}, u32[]{:S(2)}) async-start(bf16[8,272,128]{2,1,0:T(8,128)(2,1)} %bitcast.20), calls=%async_computation.1 | async-start | bytes 1114112 | tf_op jit(solution)/shard_map/all_to_all | solution.py:465
  136.4 5.5 %collective-permute-start.3 = (bf16[128,128]{1,0:T(8,128)(2,1)}, bf16[128,128]{1,0:T(8,128)(2,1)S(1)}, u32[]{:S(2)}, u32[]{:S(2)}) collective-permute-start(bf16[128,128]{1,0:T(8,128)(2,1)} %get-tuple-element.26), channel_id=1, source_target_pairs={{0,1},{1,0},{2,3},{3,2},{4,5},{5,4},{6,7},{7,6},{8,9},{9,8},{10,11... | collective-permute-start | bytes 98312 | tf_op jit(solution)/shard_map/ppermute | solution.py:471
  138.7 3.2 %collective-permute-start = (f32[1]{0:T(128)}, f32[1]{0:T(128)}, u32[]{:S(2)}, u32[]{:S(2)}) collective-permute-start(f32[1]{0:T(128)} %param.30), channel_id=1, source_target_pairs={{0,1},{1,0},{2,3},{3,2},{4,5},{5,4},{6,7},{7,6},{8,9},{9,8},{10,11... | collective-permute-start | bytes 20 | tf_op jit(solution)/shard_map/ppermute | solution.py:458
  141.8 3.3 %copy-start.9 = (bf16[128,128]{1,0:T(8,128)(2,1)}, bf16[128,128]{1,0:T(8,128)(2,1)S(1)}, u32[]{:S(2)}) copy-start(bf16[128,128]{1,0:T(8,128)(2,1)S(1)} %collective-permute-done.3.lru_theirs) | copy-start | bytes 98308
  141.8 3.3 %copy-start.4 = (bf16[256,2048]{1,0:T(8,128)(2,1)}, bf16[256,2048]{1,0:T(8,128)(2,1)S(1)}, u32[]{:S(2)}) copy-start(bf16[256,2048]{1,0:T(8,128)(2,1)S(1)} %collective-permute-done.4.w_theirs) | copy-start | bytes 3145732
  145.1 0.8 copy-start.3
